TPU v7x, 1024 devices: a whole 8x8x8 slice. The times are simulated.
1024 devices in a mesh: ep: 64 (over z, y), tp: 16 (over x, core).
Axes of the slice: x: 8, y: 8, z: 8, core: 2. Of those that a mesh axis runs over, the one named last changes fastest.
Arguments:
- tokens: bfloat16 [16384, 2048], P('ep', 'tp'), may hold values from -72 to 72
- norm_gain: bfloat16 [2048], P('tp'), may hold values from 0.099609375 to 1.8984375
- expert_ids: int32 [16384, 2], P('ep'), may hold values from 0 to 63, all different within a row; in each aligned block of 256 rows (0 to 255, 256 to 511, ...) at most 16 rows name the same one
- gate_share: float32 [16384, 2], P('ep'), may hold values from 0.1 to 1
- gate_weight: bfloat16 [64, 2048, 4096], P('ep', None, 'tp'), may hold values from -0.125 to 0.125
- up_weight: bfloat16 [64, 2048, 4096], P('ep', None, 'tp'), may hold values from -0.125 to 0.125
- down_weight: bfloat16 [64, 4096, 2048], P('ep', 'tp'), may hold values from -0.09375 to 0.09375
Outputs:
- mixed: bfloat16 [16384, 2048], P('ep', 'tp')
Inputs may be any that keep to these rules, and one draw needn't show every extreme that they name: `expert_ids`: each token names two different experts; among the 256 tokens of one index of ep no expert is named more than 16 times, a bound that some block reaches.
All inputs are finite; a program needn't handle non-finite values.
Results may differ from a plain program's by a relative error of at most 0.019.
Values may be sent and summed in bfloat16 or wider, within the bound.
No kernel may reach another device: no remote copies, remote signals or barrier semaphores. Data moves between devices by JAX's collectives and lax.ppermute only.
A program may use at most 64 MiB of HBM per device.

v0:
```python
import jax
import jax.numpy as jnp
from jax import lax
from jax.sharding import PartitionSpec as P

D = 2048


EPS = 1e-06


def from_everyone(x, axis):
    copies = jnp.broadcast_to(x, (lax.axis_size(axis), *x.shape))
    return lax.all_to_all(copies, axis, split_axis=0, concat_axis=0, tiled=True)


def of_everyone(x, axis):
    return from_everyone(x, axis).sum(axis=0)


def shards(tokens, norm_gain, expert_ids, gate_share, gate_weight, up_weight, down_weight):
    n_expdev = lax.axis_size("ep")
    exp_local = gate_weight.shape[0]
    experts = exp_local * n_expdev
    tok_rows = tokens.shape[0]
    slot_cap = 4 * tok_rows // experts
    flat_ids = expert_ids.reshape(-1)
    onehot = (flat_ids[:, None] == jnp.arange(experts, dtype=jnp.int32)[None, :]).astype(jnp.int32)
    slots = jnp.sum((jnp.cumsum(onehot, axis=0) - onehot) * onehot, axis=1)
    target = flat_ids * slot_cap + slots
    values = tokens.astype(jnp.float32)
    squares = of_everyone(jnp.sum(values * values, axis=1), "tp")
    factor = lax.rsqrt(squares / D + EPS)
    normed = (values * factor[:, None] * norm_gain.astype(jnp.float32)[None, :]).astype(
        jnp.bfloat16
    )
    rows = jnp.repeat(normed, 2, axis=0)
    buffer = jnp.zeros((experts * slot_cap, normed.shape[1]), jnp.bfloat16).at[target].set(rows)
    buffer = buffer.reshape(n_expdev, exp_local, slot_cap, normed.shape[1])
    arrived = lax.all_to_all(buffer, "ep", split_axis=0, concat_axis=0, tiled=True)
    piece = lax.all_gather(arrived, "tp", axis=3, tiled=True)
    first = jnp.einsum("secd,edf->secf", piece, gate_weight, preferred_element_type=jnp.float32)
    second = jnp.einsum("secd,edf->secf", piece, up_weight, preferred_element_type=jnp.float32)
    hidden = (jax.nn.silu(first) * second).astype(jnp.bfloat16)
    width_local = D // lax.axis_size("tp")
    term = jnp.einsum("secf,efd->dsec", hidden, down_weight, preferred_element_type=jnp.float32)
    summed = lax.psum_scatter(
        term.reshape(lax.axis_size("tp") * width_local, n_expdev * exp_local * slot_cap).astype(
            jnp.bfloat16
        ),
        "tp",
        scatter_dimension=0,
        tiled=True,
    )
    results = summed.reshape(width_local, n_expdev, exp_local, slot_cap)
    results = jnp.transpose(results, (1, 2, 3, 0))
    returned = lax.all_to_all(results, "ep", split_axis=0, concat_axis=0, tiled=True)
    flat_back = returned.reshape(experts * slot_cap, width_local)
    picked = flat_back[target].astype(jnp.float32).reshape(tok_rows, 2, width_local)
    return jnp.sum(picked * gate_share[:, :, None], axis=1).astype(jnp.bfloat16)


def solution(mesh):
    in_specs = (
        P("ep", "tp"),
        P("tp"),
        P("ep", None),
        P("ep", None),
        P("ep", None, "tp"),
        P("ep", None, "tp"),
        P("ep", "tp", None),
    )
    out_specs = P("ep", "tp")
    return jax.shard_map(shards, mesh=mesh, in_specs=in_specs, out_specs=out_specs, check_vma=False)
```

profile of v0, /device:TPU:15, one launch (start us, length us, event | category | flops | bytes accessed | tf_op | source)
XLA Modules:
  0.0 227.7 jit_solution(13968484402092088935)
XLA Ops:
  6.5 0.0 copy-start
  6.5 1.0 fusion.20
  7.6 0.6 broadcast_in_dim.7
  8.2 16.6 %all-to-all-start = ((f32[16,1,256]{2,1,0:T(1,128)}), f32[16,1,256]{2,1,0:T(1,128)S(1)}, u32[]{:S(2)}, u32[]{:S(2)}) async-start(f32[16,1,256]{2,1,0:T(1,128)} %broadcast_in_dim.7), calls=%async_computation | async-start | bytes 32768 | tf_op jit(solution)/shard_map/all_to_all | solution.py:14
  24.8 0.0 all-gather.2.cloned.1.call-start
  24.9 0.8 copy.29
  25.7 0.1 eq.29
  25.9 0.1 eq.25
  26.0 0.7 broadcast_multiply_fusion
  26.7 1.2 reduce-window.6
  27.9 0.2 slice_reduce_fusion
  28.2 0.1 copy.28
  28.3 0.1 mul.55
  28.5 0.1 fusion.25
  28.6 0.7 convert_element_type.38
  29.3 0.6 all-to-all-done
  29.9 0.9 fusion.22
  30.8 0.1 broadcast_in_dim.8
  30.9 0.0 copy-start.3
  30.9 1.8 scatter_custom_fusion
  32.8 26.9 %all_to_all.16 = bf16[64,1,16,128]{3,2,1,0:T(8,128)(2,1)} all-to-all(bf16[64,1,16,128]{3,2,1,0:T(8,128)(2,1)S(1)} %bitcast.80), channel_id=1, replica_groups=mesh['ep'=64,'tp'=16] {'ep'}, dimensions={0} | all-to-all | bytes 524288 | tf_op jit(solution)/shard_map/all_to_all | solution.py:40
  59.6 0.0 all-gather.2.cloned.1.call-update
  59.7 0.0 reduce-scatter.4.cloned.1.call-start
  59.7 47.6 %all-gather.2.cloned.1.call-done = bf16[64,1,16,2048]{3,2,0,1:T(8,128)(2,1)} async-done(((bf16[64,1,16,128]{3,2,0,1:T(8,128)(2,1)}), bf16[64,1,16,2048]{3,2,0,1:T(8,128)(2,1)}) %all-gather.2.cloned.1.call-update) | async-done | bytes 4194320 | tf_op jit(solution)/shard_map/all_gather | solution.py:41
  107.3 0.0 copy-start.2
  107.3 3.9 %fusion.4 = f32[64,1,16,256]{3,2,0,1:T(8,128)S(1)} fusion(bf16[64,1,16,2048]{3,2,0,1:T(8,128)(2,1)} %all-gather.2.cloned.1.call-done, bf16[1,2048,256]{2,1,0:T(8,128)(2,1)} %param.11), kind=kOutput, calls=%fused_computation.7 | convolution fusion | flops 1073741824 | bytes 6291456 | tf_op jit(solution)/shard_map/secd,edf->secf/dot_general | solution.py:42
  111.2 0.0 copy-done.3
  111.2 0.0 copy-done.2
  111.2 1.3 fusion.13
  112.5 0.0 copy-done
  112.5 3.2 %convert_bitcast_fusion = bf16[2048,1024]{0,1:T(8,128)(2,1)} fusion(bf16[1024,256]{1,0:T(8,128)(2,1)S(1)} %bitcast.78, bf16[1,256,2048]{2,1,0:T(8,128)(2,1)S(1)} %copy-done), kind=kOutput, calls=%fused_computation.6 | convolution fusion | flops 1075838976 | bytes 5767168 | tf_op jit(solution)/shard_map/secf,efd->dsec/dot_general | solution.py:46
  115.7 6.4 %copy.36 = bf16[2048,1024]{1,0:T(8,128)(2,1)} copy(bf16[2048,1024]{0,1:T(8,128)(2,1)} %convert_bitcast_fusion) | data formatting | bytes 8388608
  122.1 0.0 copy-start.1
  122.1 0.0 reduce-scatter.4.cloned.1.call-update
  122.1 68.7 %reduce-scatter.4.cloned.1.call-done = bf16[128,1024]{1,0:T(8,128)(2,1)} async-done(((bf16[2048,1024]{1,0:T(8,128)(2,1)}), bf16[128,1024]{1,0:T(8,128)(2,1)}) %reduce-scatter.4.cloned.1.call-update) | async-done | bytes 262160
  190.9 1.8 copy.37
  192.7 11.4 %all-to-all-start.2 = ((bf16[64,1,16,128]{3,2,1,0:T(8,128)(2,1)}), bf16[64,1,16,128]{3,2,1,0:T(8,128)(2,1)S(1)}, u32[]{:S(2)}, u32[]{:S(2)}) async-start(bf16[64,1,16,128]{3,2,1,0:T(8,128)(2,1)} %bitcast.24), calls=%async_computation.2 | async-start | bytes 524288 | tf_op jit(solution)/shard_map/all_to_all | solution.py:57
  204.0 0.0 copy-done.1
  204.0 0.1 copy.35
  204.2 14.3 %all-to-all-done.2 = bf16[64,1,16,128]{3,2,1,0:T(8,128)(2,1)S(1)} async-done(((bf16[64,1,16,128]{3,2,1,0:T(8,128)(2,1)}), bf16[64,1,16,128]{3,2,1,0:T(8,128)(2,1)S(1)}, u32[]{:S(2)}, u32[]{:S(2)}) %all-to-all-start.2) | async-done | bytes 262176 | tf_op jit(solution)/shard_map/all_to_all | solution.py:57
  218.5 1.3 gather_fusion
  219.8 1.1 fusion.19
  (7 shorter events, 0.1 us)
Async XLA Ops:
  6.5 105.9 %copy-start = (bf16[1,256,2048]{2,1,0:T(8,128)(2,1)S(1)}, bf16[1,256,2048]{2,1,0:T(8,128)(2,1)}, u32[]{:S(2)}) copy-start(bf16[1,256,2048]{2,1,0:T(8,128)(2,1)} %param.13) | copy-start | bytes 3145732
  8.2 21.6 %all-to-all-start = ((f32[16,1,256]{2,1,0:T(1,128)}), f32[16,1,256]{2,1,0:T(1,128)S(1)}, u32[]{:S(2)}, u32[]{:S(2)}) async-start(f32[16,1,256]{2,1,0:T(1,128)} %broadcast_in_dim.7), calls=%async_computation | async-start | bytes 32768 | tf_op jit(solution)/shard_map/all_to_all | solution.py:14
  24.8 82.4 %all-gather.2.cloned.1.call-start = ((), (), s32[]{:S(2)}) async-start(), calls=%async_computation.4 | async-start | bytes 4456448 | tf_op jit(solution)/shard_map/all_gather | solution.py:41
  30.9 80.3 %copy-start.3 = (bf16[1,2048,256]{2,1,0:T(8,128)(2,1)S(1)}, bf16[1,2048,256]{2,1,0:T(8,128)(2,1)}, u32[]{:S(2)}) copy-start(bf16[1,2048,256]{2,1,0:T(8,128)(2,1)} %param.12) | copy-start | bytes 3145732
  59.7 131.2 %reduce-scatter.4.cloned.1.call-start = ((), (), s32[]{:S(2)}) async-start(), calls=%async_computation.5 | async-start | bytes 4456448
  107.3 3.9 %copy-start.2 = (bf16[64,1,16,2048]{3,2,0,1:T(8,128)(2,1)S(1)}, bf16[64,1,16,2048]{3,2,0,1:T(8,128)(2,1)}, u32[]{:S(2)}) copy-start(bf16[64,1,16,2048]{3,2,0,1:T(8,128)(2,1)} %all-gather.2.cloned.1.call-done) | copy-start | bytes 12582916
  122.1 81.9 %copy-start.1 = (f32[256,2]{0,1:T(2,128)S(1)}, f32[256,2]{0,1:T(2,128)}, u32[]{:S(2)}) copy-start(f32[256,2]{0,1:T(2,128)} %param.10) | copy-start | bytes 6148
  192.7 25.8 %all-to-all-start.2 = ((bf16[64,1,16,128]{3,2,1,0:T(8,128)(2,1)}), bf16[64,1,16,128]{3,2,1,0:T(8,128)(2,1)S(1)}, u32[]{:S(2)}, u32[]{:S(2)}) async-start(bf16[64,1,16,128]{3,2,1,0:T(8,128)(2,1)} %bitcast.24), calls=%async_computation.2 | async-start | bytes 524288 | tf_op jit(solution)/shard_map/all_to_all | solution.py:57
Sparse Core Ops, SparseCore 0:
  59.8 47.4 all-gather.1
  122.3 68.5 reduce-scatter.3
where the time goes:
time: 229 us; the launch traced here: 228 us
  waiting for transfers between devices  131 us (57%)
  starting transfers between devices  28.1 us (12%)
  blocking collectives  26.9 us (12%)
  local copies, waits for them, and re-layouts  13.8 us (6%)
  between operations  13.6 us (6%)
  matrix products  8.39 us (4%)
  other arithmetic  5.82 us (3%)
    unnamed x3, waiting for transfers between devices  68.8 us
    all_gather x1, waiting for transfers between devices, shards(): piece = lax.all_gather(arrived, 'tp', axis=3, tiled=True)  47.6 us
    all_to_all x1, blocking collectives, shards(): lax.all_to_all(buffer, 'ep', split_axis=0, concat_axis=0, tiled=True)  26.9 us
    all_to_all x1, starting transfers between devices, from_everyone(): return lax.all_to_all(copies, axis, split_axis=0, concat_axis=0, tiled=True)  16.6 us
    all_to_all x1, waiting for transfers between devices, shards(): lax.all_to_all(results, 'ep', split_axis=0, concat_axis=0, tiled=True)  14.3 us
    all_to_all x1, starting transfers between devices, shards(): lax.all_to_all(results, 'ep', split_axis=0, concat_axis=0, tiled=True)  11.4 us
    unnamed x12, local copies, waits for them, and re-layouts  9.14 us
  transfers between devices with their start and end apart: 4, of which 4 were waited for; matrix products, arithmetic and copies ran while one was open for 2% of the time, Pallas kernels for 0%

commit v1 on v0

v1 whole, which is shorter than its diff:
```python
import functools

import jax
import jax.numpy as jnp
from jax import lax
from jax.experimental import pallas as pl
from jax.experimental.pallas import tpu as pltpu
from jax.sharding import Mesh, PartitionSpec as P

EPS = 1e-06
PAD = 16
EP = ("z", "y")
X = ("p", "q")
F32 = jnp.float32
BF16 = jnp.bfloat16
INTERPRET = False


def vmem(n):
    return [pl.BlockSpec(memory_space=pltpu.VMEM)] * n


SMEM = pl.BlockSpec(memory_space=pltpu.SMEM)


def call(body, outs, n_in, scalar, flops, name):
    return pl.pallas_call(
        body,
        out_shape=outs,
        in_specs=([SMEM] if scalar else []) + vmem(n_in),
        out_specs=tuple(vmem(len(outs))),
        cost_estimate=pl.CostEstimate(flops=flops, bytes_accessed=4 << 20, transcendentals=0),
        name=name,
        interpret=INTERPRET,
    )


def dispatch_body(experts, core, ids, own, other, buf, rows, gain):
    tok = ids.shape[1]
    half = buf.shape[0] // experts
    e_iota = lax.broadcasted_iota(jnp.int32, (experts, tok), 0)
    hit = [e_iota == ids[k : k + 1, :] for k in range(2)]
    named = (hit[0] | hit[1]).astype(F32).astype(BF16)
    before = lax.broadcasted_iota(jnp.int32, (tok, tok), 0) < lax.broadcasted_iota(
        jnp.int32, (tok, tok), 1
    )
    counts = jnp.dot(named, before.astype(F32).astype(BF16), preferred_element_type=F32)
    first = core[0] * half
    r_iota = lax.broadcasted_iota(jnp.int32, (buf.shape[0], tok), 0)
    place = None
    for k in range(2):
        slot = jnp.sum(jnp.where(hit[k], counts, 0.0), axis=0, keepdims=True).astype(jnp.int32)
        slot = slot - first
        row = jnp.where((slot >= 0) & (slot < half), ids[k : k + 1, :] * half + slot, -1)
        rows[k : k + 1, :] = row
        here = r_iota == row
        place = here if place is None else place | here
    place = place.astype(F32).astype(BF16)
    low = core[0] == 0
    for p in range(own.shape[0]):
        a = own[p]
        b = other[p]
        x = jnp.concatenate([jnp.where(low, a, b), jnp.where(low, b, a)], axis=1)
        buf[:, p * 256 : (p + 1) * 256] = jnp.dot(
            place, x[:tok], preferred_element_type=F32
        ).astype(BF16)
        gain[:, p * 256 : (p + 1) * 256] = x[tok:]


def expert_body(par, mine, gain, other_a, other_b, wg, wu, wd, wg2, wu2, wd2, keep, send_a, send_b):
    q = par[0]
    n = mine.shape[0]
    h = n // 2
    width = 2 * mine.shape[1]
    mine_x = mine[...].astype(F32)
    other_x = jnp.concatenate([other_a[:h], other_b[...]], axis=0).astype(F32)
    squares = jnp.sum(mine_x * mine_x, axis=1, keepdims=True) + jnp.sum(
        other_x * other_x, axis=1, keepdims=True
    )
    factor = lax.rsqrt(squares / width + EPS)
    mine_n = (mine_x * factor * gain[0:1, :].astype(F32)).astype(BF16)
    other_n = (other_x * factor * other_a[h : h + 1, :].astype(F32)).astype(BF16)

    def full(w):
        k = mine.shape[1]
        return jnp.dot(
            mine_n, w[:, pl.ds(q, 1)].reshape(k, w.shape[3]), preferred_element_type=F32
        ) + jnp.dot(
            other_n, w[:, pl.ds(1 - q, 1)].reshape(k, w.shape[3]), preferred_element_type=F32
        )

    def hidden(w_gate, w_up):
        gate = full(w_gate)
        up = full(w_up)
        return (gate / (1.0 + jnp.exp(-gate)) * up).astype(BF16)

    h1 = hidden(wg, wu)
    h2 = hidden(wg2, wu2)
    for p in range(mine.shape[1] // 256):
        cols = slice(p * 256, (p + 1) * 256)
        here = pl.ds(pl.multiple_of(p * 512 + q * 256, 256), 256)
        there = pl.ds(pl.multiple_of(p * 512 + (1 - q) * 256, 256), 256)
        keep[:, cols] = (
            jnp.dot(h1, wd[:, here], preferred_element_type=F32)
            + jnp.dot(h2, wd2[:, here], preferred_element_type=F32)
        ).astype(BF16)
        part = (
            jnp.dot(h1, wd[:, there], preferred_element_type=F32)
            + jnp.dot(h2, wd2[:, there], preferred_element_type=F32)
        ).astype(BF16)
        send_a[:, cols] = part[:h]
        send_b[:, cols] = part[h:]


def add_body(keep, got_a, got_b, out):
    h = got_a.shape[0]
    out[:h] = (keep[:h].astype(F32) + got_a[...].astype(F32)).astype(BF16)
    out[h:] = (keep[h:].astype(F32) + got_b[...].astype(F32)).astype(BF16)


def combine_body(core, rows, share, back, own, other):
    n = back.shape[0]
    tok = rows.shape[1]
    r_iota = lax.broadcasted_iota(jnp.int32, (n, tok), 0)
    weight = jnp.zeros((n, tok), F32)
    for k in range(2):
        weight = jnp.where(r_iota == rows[k : k + 1, :], share[k : k + 1, :], weight)
    high = weight.astype(BF16)
    low = (weight - high.astype(F32)).astype(BF16)
    dims = (((0,), (0,)), ((), ()))
    first = core[0] == 0
    for p in range(own.shape[0]):
        x = back[:, p * 256 : (p + 1) * 256]
        y = lax.dot_general(high, x, dims, preferred_element_type=F32) + lax.dot_general(
            low, x, dims, preferred_element_type=F32
        )
        a = y[:, :128]
        b = y[:, 128:]
        own[p] = jnp.where(first, a, b)
        other[p] = jnp.where(first, b, a)


def shards(tokens, norm_gain, expert_ids, gate_share, gate_weight, up_weight, down_weight):
    tok, width = tokens.shape
    n_ep = lax.axis_size("z") * lax.axis_size("y")
    n_p = lax.axis_size("p")
    slot_cap = 4 * tok // n_ep
    half = slot_cap // 2
    n = n_ep * half
    feats = n_p * 2 * width
    core = lax.axis_index("c").astype(jnp.int32).reshape(1)
    par = lax.axis_index("q").astype(jnp.int32).reshape(1)
    swap = [(0, 1), (1, 0)]
    n_x = 2 * n_p
    beside = [(x, (x + 1) % n_x if x % 2 else (x - 1) % n_x) for x in range(n_x)]

    hid = gate_weight.shape[2]
    wg = gate_weight.reshape(n_p, 2, 256, hid)
    wu = up_weight.reshape(n_p, 2, 256, hid)
    wd = down_weight.reshape(hid, down_weight.shape[2])
    wg2, wu2, wd2 = (lax.ppermute(w, "c", swap) for w in (wg, wu, wd))

    ids = expert_ids.T
    share = gate_share.T
    mine = jnp.concatenate([tokens, jnp.broadcast_to(norm_gain[None, :], (PAD, width))], axis=0)
    gathered = lax.all_gather(mine, "p", axis=0, tiled=False)
    other = lax.ppermute(gathered, "c", swap)
    buf, rows, gain = call(
        functools.partial(dispatch_body, n_ep),
        (
            jax.ShapeDtypeStruct((n, feats), BF16),
            jax.ShapeDtypeStruct((2, tok), jnp.int32),
            jax.ShapeDtypeStruct((PAD, feats), BF16),
        ),
        3,
        True,
        300_000_000,
        "dispatch",
    )(core, ids, gathered, other)
    arrived = lax.all_to_all(
        buf.reshape(n_ep, half, feats), EP, split_axis=0, concat_axis=0, tiled=True
    ).reshape(n, feats)
    h = n // 2
    other_a = lax.ppermute(jnp.concatenate([arrived[:h], gain], axis=0), "q", swap)
    other_b = lax.ppermute(arrived[h:], X, beside)
    piece = jax.ShapeDtypeStruct((h, feats), BF16)
    keep, send_a, send_b = call(
        expert_body,
        (jax.ShapeDtypeStruct((n, feats), BF16), piece, piece),
        10,
        True,
        3_200_000_000,
        "expert",
    )(par, arrived, gain, other_a, other_b, wg, wu, wd, wg2, wu2, wd2)
    got_a = lax.ppermute(send_a, "q", swap)
    got_b = lax.ppermute(send_b, X, beside)
    (sums,) = call(
        add_body, (jax.ShapeDtypeStruct((n, feats), BF16),), 3, False, 1_000_000, "pairsum"
    )(keep, got_a, got_b)
    returned = lax.all_to_all(
        sums.reshape(n_ep, half, feats), EP, split_axis=0, concat_axis=0, tiled=True
    ).reshape(n, feats)
    part = jax.ShapeDtypeStruct((n_p, tok, width), F32)
    own, away = call(combine_body, (part, part), 3, True, 600_000_000, "combine")(
        core, rows, share, returned
    )
    own = (own + lax.ppermute(away, "c", swap)).astype(BF16)
    parts = lax.all_to_all(own, "p", split_axis=0, concat_axis=0, tiled=True)
    return jnp.sum(parts.astype(F32), axis=0).astype(BF16)


def solution(mesh):
    n_ep, n_tp = mesh.devices.shape
    side = 8 if n_ep == 64 else n_ep
    fine = Mesh(
        mesh.devices.reshape(n_ep // side, side, n_tp // 4, 2, 2), ("z", "y", "p", "q", "c")
    )
    tp = ("p", "q", "c")
    in_specs = (
        P(EP, tp),
        P(tp),
        P(EP, None),
        P(EP, None),
        P(EP, None, tp),
        P(EP, None, tp),
        P(EP, tp, None),
    )
    return jax.shard_map(
        shards, mesh=fine, in_specs=in_specs, out_specs=P(EP, tp), check_vma=False
    )
```

time: 229 us -> 187 us (0.82)
  the two profiles are of different devices: /device:TPU:15 before, /device:TPU:16 now
where the time goes in v1:
time: 187 us; the launch traced here: 186 us
  blocking collectives  68.2 us (36%)
  waiting for transfers between devices  49.4 us (26%)
  starting transfers between devices  45 us (24%)
  Pallas kernels  16.8 us (9%)
  local copies, waits for them, and re-layouts  4.11 us (2%)
  other arithmetic  2.67 us (1%)
    all_to_all x1, blocking collectives, shards(): lax.all_to_all(sums.reshape(n_ep, half, feats), EP, split_axis=0, concat_...  35.5 us
    all_to_all x1, starting transfers between devices, shards(): lax.all_to_all(buf.reshape(n_ep, half, feats), EP, split_axis=0, concat_a...  23.5 us
    all_to_all x1, waiting for transfers between devices, shards(): lax.all_to_all(buf.reshape(n_ep, half, feats), EP, split_axis=0, concat_a...  23.3 us
    all_gather x1, blocking collectives, shards(): gathered = lax.all_gather(mine, 'p', axis=0, tiled=False)  17.1 us
    all_to_all x1, blocking collectives, shards(): parts = lax.all_to_all(own, 'p', split_axis=0, concat_axis=0, tiled=True)  15.6 us
    ppermute x1, waiting for transfers between devices, shards(): other_b = lax.ppermute(arrived[h:], X, beside)  11.5 us
    pallas_call x1, Pallas kernels, shards(): call(expert_body, (jax.ShapeDtypeStruct((n, feats), BF16), piece, piece),...  8.4 us
    ppermute x1, waiting for transfers between devices, shards(): got_a = lax.ppermute(send_a, 'q', swap)  7.85 us
  transfers between devices with their start and end apart: 10, of which 6 were waited for; matrix products, arithmetic and copies ran while one was open for 0% of the time, Pallas kernels for 0%

profile of v1, /device:TPU:16, one launch (start us, length us, event | category | flops | bytes accessed | tf_op | source)
XLA Modules:
  0.0 186.4 jit_solution(18346160247871551753)
XLA Ops:
  0.0 0.7 broadcast_in_dim.2
  0.7 0.8 pad_maximum_fusion.1
  1.5 17.1 %all-gather = bf16[1088,128]{1,0:T(8,128)(2,1)S(1)} all-gather(bf16[272,128]{1,0:T(8,128)(2,1)S(1)} %pad_maximum_fusion.1), channel_id=2, replica_groups=mesh['z'=8,'y'=8,'p'=4,'q'=2,'c'=2] {'p'}, dimensions={0}, use_global_device_ids=true | all-gather | bytes 348160 | tf_op jit(solution)/shard_map/all_gather | solution.py:166
  18.6 0.0 copy-start.3
  18.6 1.9 %collective-permute-start = (bf16[4,272,128]{2,1,0:T(8,128)(2,1)S(1)}, bf16[4,272,128]{2,1,0:T(8,128)(2,1)S(1)}, u32[]{:S(2)}, u32[]{:S(2)}) collective-permute-start(bf16[4,272,128]{2,1,0:T(8,128)(2,1)S(1)} %bitcast.20), channel_id=1, source_target_pairs={{0,1},{1,0},{2,3},{3,2},{4,5},{5,4},{6,7},{7,6},{8,9},{9,8},{10,11... | collective-permute-start | bytes 835592 | tf_op jit(solution)/shard_map/ppermute | solution.py:167
  20.6 1.5 collective-permute-done.other
  22.1 0.0 copy-start.8
  22.1 0.0 copy-done.3
  22.1 0.7 copy-done.8
  22.8 2.7 %dispatch.1 = (bf16[512,1024]{1,0:T(8,128)(2,1)}, s32[2,256]{1,0:T(2,128)}, bf16[16,1024]{1,0:T(8,128)(2,1)}) custom-call(s32[1]{0:T(128)} %bitcast.core, s32[2,256]{1,0:T(2,128)} %bitcast.28, bf16[4,272,128]{2,1,0:T(8,128)(2,1)} %bitcast.21, bf16[4,272,128]{2,1,0:T(8,128)(2,1)} %copy-done.8), custom_call_target="tpu_custom_call" | custom-call | flops 300000000 | bytes 4194304 | tf_op jit(solution)/shard_map/dispatch/pallas_call | solution.py:168
  25.4 0.0 copy-start.5
  25.4 23.5 %all-to-all-start = ((bf16[64,8,1024]{2,1,0:T(8,128)(2,1)}), bf16[64,8,1024]{2,1,0:T(8,128)(2,1)S(1)}, u32[]{:S(2)}, u32[]{:S(2)}) async-start(bf16[64,8,1024]{2,1,0:T(8,128)(2,1)} %bitcast.18), calls=%async_computation | async-start | bytes 2097152 | tf_op jit(solution)/shard_map/all_to_all | solution.py:180
  49.0 0.0 copy-done.5
  49.0 1.9 %collective-permute-start.3 = (bf16[4,2,256,256]{3,2,1,0:T(8,128)(2,1)S(1)}, bf16[4,2,256,256]{3,2,1,0:T(8,128)(2,1)}, u32[]{:S(2)}, u32[]{:S(2)}) collective-permute-start(bf16[4,2,256,256]{3,2,1,0:T(8,128)(2,1)S(1)} %bitcast.23), channel_id=1, source_target_pairs={{0,1},{1,0},{2,3},{3,2},{4,5},{5,4},{6,7},{7,6},{8,9},{9,8},{10,11... | collective-permute-start | bytes 3145736 | tf_op jit(solution)/shard_map/ppermute | solution.py:161
  50.9 2.4 %collective-permute-start.4 = (bf16[4,2,256,256]{3,2,1,0:T(8,128)(2,1)}, bf16[4,2,256,256]{3,2,1,0:T(8,128)(2,1)}, u32[]{:S(2)}, u32[]{:S(2)}) collective-permute-start(bf16[4,2,256,256]{3,2,1,0:T(8,128)(2,1)} %bitcast.24), channel_id=1, source_target_pairs={{0,1},{1,0},{2,3},{3,2},{4,5},{5,4},{6,7},{7,6},{8,9},{9,8},{10,11... | collective-permute-start | bytes 3145736 | tf_op jit(solution)/shard_map/ppermute | solution.py:161
  53.3 0.0 copy-start.4
  53.3 1.9 %collective-permute-start.5 = (bf16[256,2048]{1,0:T(8,128)(2,1)}, bf16[256,2048]{1,0:T(8,128)(2,1)}, u32[]{:S(2)}, u32[]{:S(2)}) collective-permute-start(bf16[256,2048]{1,0:T(8,128)(2,1)} %bitcast.26), channel_id=1, source_target_pairs={{0,1},{1,0},{2,3},{3,2},{4,5},{5,4},{6,7},{7,6},{8,9},{9,8},{10,11... | collective-permute-start | bytes 3145736 | tf_op jit(solution)/shard_map/ppermute | solution.py:161
  55.3 23.3 %all-to-all-done = bf16[64,8,1024]{2,1,0:T(8,128)(2,1)S(1)} async-done(((bf16[64,8,1024]{2,1,0:T(8,128)(2,1)}), bf16[64,8,1024]{2,1,0:T(8,128)(2,1)S(1)}, u32[]{:S(2)}, u32[]{:S(2)}) %all-to-all-start) | async-done | bytes 1048608 | tf_op jit(solution)/shard_map/all_to_all | solution.py:180
  78.6 0.0 copy-start
  78.6 0.1 slice_bitcast_fusion
  78.7 0.9 copy-done
  79.6 0.0 copy-done.4
  79.6 2.0 %collective-permute-start.1 = (bf16[272,1024]{1,0:T(8,128)(2,1)S(1)}, bf16[272,1024]{1,0:T(8,128)(2,1)S(1)}, u32[]{:S(2)}, u32[]{:S(2)}) collective-permute-start(bf16[272,1024]{1,0:T(8,128)(2,1)S(1)} %pad_maximum_fusion), channel_id=1, source_target_pairs={{0,2},{2,0},{1,3},{3,1},{4,6},{6,4},{5,7},{7,5},{8,10},{10,8},{9,1... | collective-permute-start | bytes 1671176 | tf_op jit(solution)/shard_map/ppermute | solution.py:184
  81.6 3.8 %collective-permute-start.2 = (bf16[256,1024]{1,0:T(8,128)(2,1)S(1)}, bf16[256,1024]{1,0:T(8,128)(2,1)S(1)}, u32[]{:S(2)}, u32[]{:S(2)}) collective-permute-start(bf16[256,1024]{1,0:T(8,128)(2,1)S(1)} %get-tuple-element.21), channel_id=1, source_target_pairs={{0,14},{2,4},{4,2},{6,8},{8,6},{10,12},{12,10},{14,0},{1,15},{3,5}... | collective-permute-start | bytes 1572872 | tf_op jit(solution)/shard_map/ppermute | solution.py:185
  85.4 0.0 collective-permute-done.3.wg2
  85.4 0.0 collective-permute-done.4.wu2
  85.4 0.0 collective-permute-done.5.wd2
  85.4 11.5 %collective-permute-done.2.other_b = bf16[256,1024]{1,0:T(8,128)(2,1)S(1)} collective-permute-done((bf16[256,1024]{1,0:T(8,128)(2,1)S(1)}, bf16[256,1024]{1,0:T(8,128)(2,1)S(1)}, u32[]{:S(2)}, u32[]{:S(2)}) %collective-permute-start.2) | collective-permute-done | bytes 524320 | tf_op jit(solution)/shard_map/ppermute | solution.py:185
  96.9 0.0 copy-start.7
  96.9 0.0 collective-permute-done.1.other_a
  96.9 0.0 copy-start.6
  96.9 0.8 copy-done.7
  97.7 0.2 copy-done.6
  97.9 8.4 %expert.1 = (bf16[512,1024]{1,0:T(8,128)(2,1)}, bf16[256,1024]{1,0:T(8,128)(2,1)}, bf16[256,1024]{1,0:T(8,128)(2,1)}) custom-call(s32[1]{0:T(128)} %bitcast.4.par, bf16[512,1024]{1,0:T(8,128)(2,1)} %bitcast.17, bf16[16,1024]{1,0:T(8,128)(2,1)} %get-tuple-element.15.gain, bf16[272,1024]{1,0:T(8,128)(2,1)} %copy-done.6, bf16[256,1024]{1,0:T(8,128)(2,1)} %copy-done.7, ...), custom_call_target="tpu_custom_call" | custom-call | flops 3200000000 | bytes 4194304 | tf_op jit(solution)/shard_map/expert/pallas_call | solution.py:187
  106.3 2.4 %collective-permute-start.6 = (bf16[256,1024]{1,0:T(8,128)(2,1)}, bf16[256,1024]{1,0:T(8,128)(2,1)S(1)}, u32[]{:S(2)}, u32[]{:S(2)}) collective-permute-start(bf16[256,1024]{1,0:T(8,128)(2,1)} %get-tuple-element.17), channel_id=1, source_target_pairs={{0,2},{2,0},{1,3},{3,1},{4,6},{6,4},{5,7},{7,5},{8,10},{10,8},{9,1... | collective-permute-start | bytes 1572872 | tf_op jit(solution)/shard_map/ppermute | solution.py:195
  108.8 3.2 %collective-permute-start.7 = (bf16[256,1024]{1,0:T(8,128)(2,1)}, bf16[256,1024]{1,0:T(8,128)(2,1)S(1)}, u32[]{:S(2)}, u32[]{:S(2)}) collective-permute-start(bf16[256,1024]{1,0:T(8,128)(2,1)} %get-tuple-element.18), channel_id=1, source_target_pairs={{0,14},{2,4},{4,2},{6,8},{8,6},{10,12},{12,10},{14,0},{1,15},{3,5}... | collective-permute-start | bytes 1572872 | tf_op jit(solution)/shard_map/ppermute | solution.py:196
  112.0 7.9 %collective-permute-done.6.got_a = bf16[256,1024]{1,0:T(8,128)(2,1)S(1)} collective-permute-done((bf16[256,1024]{1,0:T(8,128)(2,1)}, bf16[256,1024]{1,0:T(8,128)(2,1)S(1)}, u32[]{:S(2)}, u32[]{:S(2)}) %collective-permute-start.6) | collective-permute-done | bytes 524320 | tf_op jit(solution)/shard_map/ppermute | solution.py:195
  119.8 0.0 copy-start.1
  119.8 3.1 %collective-permute-done.7.got_b = bf16[256,1024]{1,0:T(8,128)(2,1)S(1)} collective-permute-done((bf16[256,1024]{1,0:T(8,128)(2,1)}, bf16[256,1024]{1,0:T(8,128)(2,1)S(1)}, u32[]{:S(2)}, u32[]{:S(2)}) %collective-permute-start.7) | collective-permute-done | bytes 524320 | tf_op jit(solution)/shard_map/ppermute | solution.py:196
  123.0 0.0 copy-start.2
  123.0 0.0 copy-done.1
  123.0 0.8 copy-done.2
  123.8 2.7 %pairsum.1 = bf16[512,1024]{1,0:T(8,128)(2,1)} custom-call(bf16[512,1024]{1,0:T(8,128)(2,1)} %get-tuple-element.16.keep, bf16[256,1024]{1,0:T(8,128)(2,1)} %copy-done.1, bf16[256,1024]{1,0:T(8,128)(2,1)} %copy-done.2), custom_call_target="tpu_custom_call" | custom-call | flops 1000000 | bytes 4194304 | tf_op jit(solution)/shard_map/pairsum/pallas_call | solution.py:197
  126.5 35.5 %all_to_all.15 = bf16[64,8,1024]{2,1,0:T(8,128)(2,1)} all-to-all(bf16[64,8,1024]{2,1,0:T(8,128)(2,1)} %bitcast.16), channel_id=1, replica_groups=mesh['z'=8,'y'=8,'p'=4,'q'=2,'c'=2] {'z','y'}, dimensions={0} | all-to-all | bytes 2097152 | tf_op jit(solution)/shard_map/all_to_all | solution.py:200
  162.0 3.0 %combine.1 = (f32[4,256,128]{2,1,0:T(8,128)}, f32[4,256,128]{2,1,0:T(8,128)}) custom-call(s32[1]{0:T(128)} %bitcast.core, s32[2,256]{1,0:T(2,128)} %get-tuple-element.13.rows, f32[2,256]{1,0:T(2,128)} %bitcast.29, bf16[512,1024]{1,0:T(8,128)(2,1)} %bitcast.19), custom_call_target="tpu_custom_call" | custom-call | flops 600000000 | bytes 4194304 | tf_op jit(solution)/shard_map/combine/pallas_call | solution.py:204
  165.0 1.9 %collective-permute-start.8 = (f32[4,256,128]{2,1,0:T(8,128)}, f32[4,256,128]{2,1,0:T(8,128)S(1)}, u32[]{:S(2)}, u32[]{:S(2)}) collective-permute-start(f32[4,256,128]{2,1,0:T(8,128)} %get-tuple-element.20), channel_id=1, source_target_pairs={{0,1},{1,0},{2,3},{3,2},{4,5},{5,4},{6,7},{7,6},{8,9},{9,8},{10,11... | collective-permute-start | bytes 1572872 | tf_op jit(solution)/shard_map/ppermute | solution.py:207
  166.9 2.1 %collective-permute-done.8 = f32[4,256,128]{2,1,0:T(8,128)S(1)} collective-permute-done((f32[4,256,128]{2,1,0:T(8,128)}, f32[4,256,128]{2,1,0:T(8,128)S(1)}, u32[]{:S(2)}, u32[]{:S(2)}) %collective-permute-start.8) | collective-permute-done | bytes 524320 | tf_op jit(solution)/shard_map/ppermute | solution.py:207
  169.0 1.1 add_convert_fusion
  170.2 15.6 %all_to_all.16 = bf16[4,256,128]{2,1,0:T(8,128)(2,1)S(1)} all-to-all(bf16[4,256,128]{2,1,0:T(8,128)(2,1)S(1)} %add_convert_fusion), channel_id=1, replica_groups=mesh['z'=8,'y'=8,'p'=4,'q'=2,'c'=2] {'p'}, dimensions={0} | all-to-all | bytes 524288 | tf_op jit(solution)/shard_map/all_to_all | solution.py:208
  185.7 0.7 reduce_sum.12
  (1 shorter events, 0.0 us)
Async XLA Ops:
  18.6 3.4 %copy-start.3 = (bf16[1088,128]{1,0:T(8,128)(2,1)}, bf16[1088,128]{1,0:T(8,128)(2,1)S(1)}, u32[]{:S(2)}) copy-start(bf16[1088,128]{1,0:T(8,128)(2,1)S(1)} %all-gather) | copy-start | bytes 835588
  18.6 3.4 %collective-permute-start = (bf16[4,272,128]{2,1,0:T(8,128)(2,1)S(1)}, bf16[4,272,128]{2,1,0:T(8,128)(2,1)S(1)}, u32[]{:S(2)}, u32[]{:S(2)}) collective-permute-start(bf16[4,272,128]{2,1,0:T(8,128)(2,1)S(1)} %bitcast.20), channel_id=1, source_target_pairs={{0,1},{1,0},{2,3},{3,2},{4,5},{5,4},{6,7},{7,6},{8,9},{9,8},{10,11... | collective-permute-start | bytes 835592 | tf_op jit(solution)/shard_map/ppermute | solution.py:167
  22.1 0.7 copy-start.8
  25.4 23.5 %copy-start.5 = (bf16[1,2048,256]{2,1,0:T(8,128)(2,1)S(1)}, bf16[1,2048,256]{2,1,0:T(8,128)(2,1)}, u32[]{:S(2)}) copy-start(bf16[1,2048,256]{2,1,0:T(8,128)(2,1)} %param.11) | copy-start | bytes 3145732
  25.4 53.1 %all-to-all-start = ((bf16[64,8,1024]{2,1,0:T(8,128)(2,1)}), bf16[64,8,1024]{2,1,0:T(8,128)(2,1)S(1)}, u32[]{:S(2)}, u32[]{:S(2)}) async-start(bf16[64,8,1024]{2,1,0:T(8,128)(2,1)} %bitcast.18), calls=%async_computation | async-start | bytes 2097152 | tf_op jit(solution)/shard_map/all_to_all | solution.py:180
  49.0 36.4 %collective-permute-start.3 = (bf16[4,2,256,256]{3,2,1,0:T(8,128)(2,1)S(1)}, bf16[4,2,256,256]{3,2,1,0:T(8,128)(2,1)}, u32[]{:S(2)}, u32[]{:S(2)}) collective-permute-start(bf16[4,2,256,256]{3,2,1,0:T(8,128)(2,1)S(1)} %bitcast.23), channel_id=1, source_target_pairs={{0,1},{1,0},{2,3},{3,2},{4,5},{5,4},{6,7},{7,6},{8,9},{9,8},{10,11... | collective-permute-start | bytes 3145736 | tf_op jit(solution)/shard_map/ppermute | solution.py:161
  50.9 34.5 %collective-permute-start.4 = (bf16[4,2,256,256]{3,2,1,0:T(8,128)(2,1)}, bf16[4,2,256,256]{3,2,1,0:T(8,128)(2,1)}, u32[]{:S(2)}, u32[]{:S(2)}) collective-permute-start(bf16[4,2,256,256]{3,2,1,0:T(8,128)(2,1)} %bitcast.24), channel_id=1, source_target_pairs={{0,1},{1,0},{2,3},{3,2},{4,5},{5,4},{6,7},{7,6},{8,9},{9,8},{10,11... | collective-permute-start | bytes 3145736 | tf_op jit(solution)/shard_map/ppermute | solution.py:161
  53.3 26.2 %copy-start.4 = (bf16[16,1024]{1,0:T(8,128)(2,1)S(1)}, bf16[16,1024]{1,0:T(8,128)(2,1)}, u32[]{:S(2)}) copy-start(bf16[16,1024]{1,0:T(8,128)(2,1)} %get-tuple-element.15.gain) | copy-start | bytes 98308
  53.3 32.1 %collective-permute-start.5 = (bf16[256,2048]{1,0:T(8,128)(2,1)}, bf16[256,2048]{1,0:T(8,128)(2,1)}, u32[]{:S(2)}, u32[]{:S(2)}) collective-permute-start(bf16[256,2048]{1,0:T(8,128)(2,1)} %bitcast.26), channel_id=1, source_target_pairs={{0,1},{1,0},{2,3},{3,2},{4,5},{5,4},{6,7},{7,6},{8,9},{9,8},{10,11... | collective-permute-start | bytes 3145736 | tf_op jit(solution)/shard_map/ppermute | solution.py:161
  78.6 1.0 copy-start
  79.6 17.3 %collective-permute-start.1 = (bf16[272,1024]{1,0:T(8,128)(2,1)S(1)}, bf16[272,1024]{1,0:T(8,128)(2,1)S(1)}, u32[]{:S(2)}, u32[]{:S(2)}) collective-permute-start(bf16[272,1024]{1,0:T(8,128)(2,1)S(1)} %pad_maximum_fusion), channel_id=1, source_target_pairs={{0,2},{2,0},{1,3},{3,1},{4,6},{6,4},{5,7},{7,5},{8,10},{10,8},{9,1... | collective-permute-start | bytes 1671176 | tf_op jit(solution)/shard_map/ppermute | solution.py:184
  81.6 15.4 %collective-permute-start.2 = (bf16[256,1024]{1,0:T(8,128)(2,1)S(1)}, bf16[256,1024]{1,0:T(8,128)(2,1)S(1)}, u32[]{:S(2)}, u32[]{:S(2)}) collective-permute-start(bf16[256,1024]{1,0:T(8,128)(2,1)S(1)} %get-tuple-element.21), channel_id=1, source_target_pairs={{0,14},{2,4},{4,2},{6,8},{8,6},{10,12},{12,10},{14,0},{1,15},{3,5}... | collective-permute-start | bytes 1572872 | tf_op jit(solution)/shard_map/ppermute | solution.py:185
  96.9 0.8 copy-start.7
  96.9 1.0 copy-start.6
  106.3 13.5 %collective-permute-start.6 = (bf16[256,1024]{1,0:T(8,128)(2,1)}, bf16[256,1024]{1,0:T(8,128)(2,1)S(1)}, u32[]{:S(2)}, u32[]{:S(2)}) collective-permute-start(bf16[256,1024]{1,0:T(8,128)(2,1)} %get-tuple-element.17), channel_id=1, source_target_pairs={{0,2},{2,0},{1,3},{3,1},{4,6},{6,4},{5,7},{7,5},{8,10},{10,8},{9,1... | collective-permute-start | bytes 1572872 | tf_op jit(solution)/shard_map/ppermute | solution.py:195
  108.8 14.2 %collective-permute-start.7 = (bf16[256,1024]{1,0:T(8,128)(2,1)}, bf16[256,1024]{1,0:T(8,128)(2,1)S(1)}, u32[]{:S(2)}, u32[]{:S(2)}) collective-permute-start(bf16[256,1024]{1,0:T(8,128)(2,1)} %get-tuple-element.18), channel_id=1, source_target_pairs={{0,14},{2,4},{4,2},{6,8},{8,6},{10,12},{12,10},{14,0},{1,15},{3,5}... | collective-permute-start | bytes 1572872 | tf_op jit(solution)/shard_map/ppermute | solution.py:196
  119.8 3.1 %copy-start.1 = (bf16[256,1024]{1,0:T(8,128)(2,1)}, bf16[256,1024]{1,0:T(8,128)(2,1)S(1)}, u32[]{:S(2)}) copy-start(bf16[256,1024]{1,0:T(8,128)(2,1)S(1)} %collective-permute-done.6.got_a) | copy-start | bytes 1572868
  123.0 0.8 copy-start.2
  165.0 4.0 %collective-permute-start.8 = (f32[4,256,128]{2,1,0:T(8,128)}, f32[4,256,128]{2,1,0:T(8,128)S(1)}, u32[]{:S(2)}, u32[]{:S(2)}) collective-permute-start(f32[4,256,128]{2,1,0:T(8,128)} %get-tuple-element.20), channel_id=1, source_target_pairs={{0,1},{1,0},{2,3},{3,2},{4,5},{5,4},{6,7},{7,6},{8,9},{9,8},{10,11... | collective-permute-start | bytes 1572872 | tf_op jit(solution)/shard_map/ppermute | solution.py:207

commit v2 on v1

v2 whole, which is shorter than its diff:
```python
import functools

import jax
import jax.numpy as jnp
from jax import lax
from jax.experimental import pallas as pl
from jax.experimental.pallas import tpu as pltpu
from jax.sharding import Mesh, PartitionSpec as P

EPS = 1e-06
PAD = 16
EP = ("z", "y")
X = ("p", "q")
F32 = jnp.float32
BF16 = jnp.bfloat16
INTERPRET = False


def vmem(n):
    return [pl.BlockSpec(memory_space=pltpu.VMEM)] * n


SMEM = pl.BlockSpec(memory_space=pltpu.SMEM)


def call(body, outs, n_in, scalar, flops, name, mib):
    return pl.pallas_call(
        body,
        out_shape=outs,
        in_specs=([SMEM] if scalar else []) + vmem(n_in),
        out_specs=tuple(vmem(len(outs))),
        cost_estimate=pl.CostEstimate(flops=flops, bytes_accessed=4 << 20, transcendentals=0),
        compiler_params=pltpu.CompilerParams(vmem_limit_bytes=mib << 20),
        name=name,
        interpret=INTERPRET,
    )


def dispatch_body(experts, pos, ids, own, other, buf, rows, gain):
    tok = ids.shape[1]
    n_p = own.shape[0]
    half = buf.shape[0] // experts
    core = pos[0]
    e_iota = lax.broadcasted_iota(jnp.int32, (experts, tok), 0)
    hit = [e_iota == ids[k : k + 1, :] for k in range(2)]
    named = (hit[0] | hit[1]).astype(F32).astype(BF16)
    before = lax.broadcasted_iota(jnp.int32, (tok, tok), 0) < lax.broadcasted_iota(
        jnp.int32, (tok, tok), 1
    )
    counts = jnp.dot(named, before.astype(F32).astype(BF16), preferred_element_type=F32)
    r_iota = lax.broadcasted_iota(jnp.int32, (buf.shape[0], tok), 0)
    place = None
    for k in range(2):
        slot = jnp.sum(jnp.where(hit[k], counts, 0.0), axis=0, keepdims=True).astype(jnp.int32)
        slot = slot - core * half
        row = jnp.where((slot >= 0) & (slot < half), ids[k : k + 1, :] * half + slot, -1)
        rows[k : k + 1, :] = row
        here = r_iota == row
        place = here if place is None else place | here
    place = place.astype(F32).astype(BF16)
    low = core == 0
    for s in range(n_p):
        cols = pl.ds(pl.multiple_of(((pos[1] + n_p - s) % n_p) * 256, 256), 256)
        a = own[s]
        b = other[s]
        x = jnp.concatenate([jnp.where(low, a, b), jnp.where(low, b, a)], axis=1)
        buf[:, cols] = jnp.dot(place, x[:tok], preferred_element_type=F32).astype(BF16)
        gain[:, cols] = x[tok:]


def product(x, half, w):
    k = x.shape[1]
    return jnp.dot(x, w[:, pl.ds(half, 1)].reshape(k, w.shape[3]), preferred_element_type=F32)


def near_body(par, mine, gain, wg, wu, wg2, wu2, gate, up, squares):
    x = mine[...].astype(F32)
    squares[...] = jnp.broadcast_to(jnp.sum(x * x, axis=1, keepdims=True), squares.shape)
    y = (x * gain[0:1, :].astype(F32)).astype(BF16)
    hid = wg.shape[3]
    for i, (w_gate, w_up) in enumerate(((wg, wu), (wg2, wu2))):
        cols = slice(i * hid, (i + 1) * hid)
        gate[:, cols] = product(y, par[0], w_gate)
        up[:, cols] = product(y, par[0], w_up)


def far_body(
    par, other_a, other_b, gate, up, squares, wg, wu, wg2, wu2, wd, wd2, send_a, send_b, hidden
):
    h = other_b.shape[0]
    n_in = other_b.shape[1]
    x = jnp.concatenate([other_a[:h], other_b[...]], axis=0).astype(F32)
    total = squares[:, 0:1] + jnp.sum(x * x, axis=1, keepdims=True)
    factor = lax.rsqrt(total / (2 * n_in) + EPS)
    y = (x * other_a[h : h + 1, :].astype(F32)).astype(BF16)
    hid = wg.shape[3]
    half = 1 - par[0]
    for i, (w_gate, w_up) in enumerate(((wg, wu), (wg2, wu2))):
        cols = slice(i * hid, (i + 1) * hid)
        g = (gate[:, cols] + product(y, half, w_gate)) * factor
        u = (up[:, cols] + product(y, half, w_up)) * factor
        hidden[:, cols] = (g / (1.0 + jnp.exp(-g)) * u).astype(BF16)
    down(hidden[...], wd, wd2, half, (send_a, send_b))


def down(hid, wd, wd2, half, outs):
    k = wd.shape[0]
    rows = hid.shape[0] // len(outs)
    for p in range(outs[0].shape[1] // 256):
        cols = pl.ds(pl.multiple_of(p * 512 + half * 256, 256), 256)
        y = (
            jnp.dot(hid[:, :k], wd[:, cols], preferred_element_type=F32)
            + jnp.dot(hid[:, k:], wd2[:, cols], preferred_element_type=F32)
        ).astype(BF16)
        for i, out in enumerate(outs):
            out[:, p * 256 : (p + 1) * 256] = y[i * rows : (i + 1) * rows]


def keep_body(par, hidden, wd, wd2, keep):
    down(hidden[...], wd, wd2, par[0], (keep,))


def add_body(keep, got_a, got_b, out):
    h = got_a.shape[0]
    out[:h] = (keep[:h].astype(F32) + got_a[...].astype(F32)).astype(BF16)
    out[h:] = (keep[h:].astype(F32) + got_b[...].astype(F32)).astype(BF16)


def combine_body(pos, rows, share, back, own, other):
    n = back.shape[0]
    tok = rows.shape[1]
    n_p = own.shape[0]
    r_iota = lax.broadcasted_iota(jnp.int32, (n, tok), 0)
    weight = jnp.zeros((n, tok), F32)
    for k in range(2):
        weight = jnp.where(r_iota == rows[k : k + 1, :], share[k : k + 1, :], weight)
    high = weight.astype(BF16)
    low = (weight - high.astype(F32)).astype(BF16)
    dims = (((0,), (0,)), ((), ()))
    first = pos[0] == 0
    for s in range(n_p):
        x = back[:, pl.ds(pl.multiple_of(((pos[1] + s) % n_p) * 256, 256), 256)]
        y = lax.dot_general(high, x, dims, preferred_element_type=F32) + lax.dot_general(
            low, x, dims, preferred_element_type=F32
        )
        a = y[:, :128]
        b = y[:, 128:]
        own[s] = jnp.where(first, a, b)
        other[s] = jnp.where(first, b, a)


def fold_body(own, got, *outs):
    for s, out in enumerate(outs):
        out[...] = (own[s] + got[s]).astype(BF16)


def shards(tokens, norm_gain, expert_ids, gate_share, gate_weight, up_weight, down_weight):
    tok, width = tokens.shape
    n_ep = lax.axis_size("z") * lax.axis_size("y")
    n_p = lax.axis_size("p")
    slot_cap = 4 * tok // n_ep
    half = slot_cap // 2
    n = n_ep * half
    h = n // 2
    feats = n_p * 2 * width
    pos = jnp.stack([lax.axis_index("c"), lax.axis_index("p")]).astype(jnp.int32)
    par = lax.axis_index("q").astype(jnp.int32).reshape(1)
    swap = [(0, 1), (1, 0)]
    n_x = 2 * n_p
    beside = [(x, (x + 1) % n_x if x % 2 else (x - 1) % n_x) for x in range(n_x)]

    def along(x, s):
        return lax.ppermute(x, "p", [(i, (i + s) % n_p) for i in range(n_p)])

    hid = gate_weight.shape[2]
    wg = gate_weight.reshape(n_p, 2, 256, hid)
    wu = up_weight.reshape(n_p, 2, 256, hid)
    wd = down_weight.reshape(hid, down_weight.shape[2])
    wg2, wu2, wd2 = (lax.ppermute(w, "c", swap) for w in (wg, wu, wd))

    mine = jnp.where(
        lax.broadcasted_iota(jnp.int32, (tok + PAD, width), 0) < tok,
        jnp.pad(tokens, ((0, PAD), (0, 0))),
        norm_gain[None, :],
    )
    gathered = jnp.stack([mine] + [along(mine, s) for s in range(1, n_p)])
    other = lax.ppermute(gathered, "c", swap)

    def shape(*dims, dtype=BF16):
        return jax.ShapeDtypeStruct(dims, dtype)

    buf, rows, gain = call(
        functools.partial(dispatch_body, n_ep),
        (shape(n, feats), shape(2, tok, dtype=jnp.int32), shape(PAD, feats)),
        3,
        True,
        300_000_000,
        "dispatch",
        8,
    )(pos, expert_ids.T, gathered, other)
    arrived = lax.all_to_all(
        buf.reshape(n_ep, half, feats), EP, split_axis=0, concat_axis=0, tiled=True
    ).reshape(n, feats)
    other_a = lax.ppermute(jnp.concatenate([arrived[:h], gain], axis=0), "q", swap)
    other_b = lax.ppermute(arrived[h:], X, beside)
    wide = shape(n, 2 * hid, dtype=F32)
    gate, up, squares = call(
        near_body, (wide, wide, shape(n, 128, dtype=F32)), 6, True, 1_100_000_000, "near", 10
    )(par, arrived, gain, wg, wu, wg2, wu2)
    send_a, send_b, hidden = call(
        far_body,
        (shape(h, feats), shape(h, feats), shape(n, 2 * hid)),
        11,
        True,
        1_600_000_000,
        "far",
        12,
    )(par, other_a, other_b, gate, up, squares, wg, wu, wg2, wu2, wd, wd2)
    got_a = lax.ppermute(send_a, "q", swap)
    got_b = lax.ppermute(send_b, X, beside)
    (keep,) = call(keep_body, (shape(n, feats),), 3, True, 550_000_000, "keep", 6)(
        par, hidden, wd, wd2
    )
    (sums,) = call(add_body, (shape(n, feats),), 3, False, 1_000_000, "pairsum", 4)(
        keep, got_a, got_b
    )
    returned = lax.all_to_all(
        sums.reshape(n_ep, half, feats), EP, split_axis=0, concat_axis=0, tiled=True
    ).reshape(n, feats)
    part = shape(n_p, tok, width, dtype=F32)
    own, away = call(combine_body, (part, part), 3, True, 600_000_000, "combine", 8)(
        pos, rows, gate_share.T, returned
    )
    pieces = call(
        fold_body, (shape(tok, width),) * n_p, 2, False, 1_000_000, "fold", 4
    )(own, lax.ppermute(away, "c", swap))
    total = pieces[0].astype(F32)
    for s in range(1, n_p):
        total = total + along(pieces[s], s).astype(F32)
    return total.astype(BF16)


def solution(mesh):
    n_ep, n_tp = mesh.devices.shape
    side = 8 if n_ep == 64 else n_ep
    fine = Mesh(
        mesh.devices.reshape(n_ep // side, side, n_tp // 4, 2, 2), ("z", "y", "p", "q", "c")
    )
    tp = ("p", "q", "c")
    in_specs = (
        P(EP, tp),
        P(tp),
        P(EP, None),
        P(EP, None),
        P(EP, None, tp),
        P(EP, None, tp),
        P(EP, tp, None),
    )
    return jax.shard_map(
        shards, mesh=fine, in_specs=in_specs, out_specs=P(EP, tp), check_vma=False
    )
```

time: 187 us -> 180 us (0.963)
  the two profiles are of different devices: /device:TPU:16 before, /device:TPU:15 now
where the time goes in v2:
time: 180 us; the launch traced here: 177 us
  starting transfers between devices  72 us (40%)
  waiting for transfers between devices  52.1 us (29%)
  blocking collectives  35.5 us (20%)
  Pallas kernels  11.9 us (7%)
  other arithmetic  2.58 us (1%)
  local copies, waits for them, and re-layouts  2.53 us (1%)
    all_to_all x1, blocking collectives, shards(): lax.all_to_all(sums.reshape(n_ep, half, feats), EP, split_axis=0, concat_...  35.5 us
    all_to_all x1, starting transfers between devices, shards(): lax.all_to_all(buf.reshape(n_ep, half, feats), EP, split_axis=0, concat_a...  24.1 us
    all_to_all x1, waiting for transfers between devices, shards(): lax.all_to_all(buf.reshape(n_ep, half, feats), EP, split_axis=0, concat_a...  20.8 us
    ppermute x6, starting transfers between devices, along(): return lax.ppermute(x, 'p', [(i, (i + s) % n_p) for i in range(n_p)])  20.1 us
    ppermute x6, waiting for transfers between devices, along(): return lax.ppermute(x, 'p', [(i, (i + s) % n_p) for i in range(n_p)])  11.2 us
    ppermute x1, waiting for transfers between devices, shards(): other_b = lax.ppermute(arrived[h:], X, beside)  8.98 us
    ppermute x1, starting transfers between devices, shards(): lax.ppermute(away, 'c', swap)  7.81 us
    ppermute x3, starting transfers between devices, shards(): wg2, wu2, wd2 = (lax.ppermute(w, 'c', swap) for w in (wg, wu, wd))  6.89 us
  transfers between devices with their start and end apart: 16, of which 10 were waited for; matrix products, arithmetic and copies ran while one was open for 1% of the time, Pallas kernels for 3%

profile of v2, /device:TPU:15, one launch (start us, length us, event | category | flops | bytes accessed | tf_op | source)
XLA Modules:
  0.0 176.9 jit_solution(12512225657766678043)
XLA Ops:
  0.0 1.0 fusion
  1.0 4.8 %collective-permute-start.1 = (bf16[272,128]{1,0:T(8,128)(2,1)S(1)}, bf16[272,128]{1,0:T(8,128)(2,1)S(1)}, u32[]{:S(2)}, u32[]{:S(2)}) collective-permute-start(bf16[272,128]{1,0:T(8,128)(2,1)S(1)} %get-tuple-element.38), channel_id=1, source_target_pairs={{0,8},{4,12},{8,0},{12,4},{1,9},{5,13},{9,1},{13,5},{2,10},{6,14},... | collective-permute-start | bytes 208904 | tf_op jit(solution)/shard_map/ppermute | solution.py:173
  5.8 4.4 %collective-permute-start = (bf16[272,128]{1,0:T(8,128)(2,1)S(1)}, bf16[272,128]{1,0:T(8,128)(2,1)S(1)}, u32[]{:S(2)}, u32[]{:S(2)}) collective-permute-start(bf16[272,128]{1,0:T(8,128)(2,1)S(1)} %get-tuple-element.38), channel_id=1, source_target_pairs={{0,4},{4,8},{8,12},{12,0},{1,5},{5,9},{9,13},{13,1},{2,6},{6,10},{... | collective-permute-start | bytes 208904 | tf_op jit(solution)/shard_map/ppermute | solution.py:173
  10.1 1.9 %collective-permute-start.2 = (bf16[272,128]{1,0:T(8,128)(2,1)S(1)}, bf16[272,128]{1,0:T(8,128)(2,1)S(1)}, u32[]{:S(2)}, u32[]{:S(2)}) collective-permute-start(bf16[272,128]{1,0:T(8,128)(2,1)S(1)} %get-tuple-element.38), channel_id=1, source_target_pairs={{0,12},{4,0},{8,4},{12,8},{1,13},{5,1},{9,5},{13,9},{2,14},{6,2},{... | collective-permute-start | bytes 208904 | tf_op jit(solution)/shard_map/ppermute | solution.py:173
  12.0 0.0 collective-permute-done.1
  12.1 2.1 %collective-permute-done = bf16[272,128]{1,0:T(8,128)(2,1)S(1)} collective-permute-done((bf16[272,128]{1,0:T(8,128)(2,1)S(1)}, bf16[272,128]{1,0:T(8,128)(2,1)S(1)}, u32[]{:S(2)}, u32[]{:S(2)}) %collective-permute-start) | collective-permute-done | bytes 69664 | tf_op jit(solution)/shard_map/ppermute | solution.py:173
  14.1 3.6 %collective-permute-done.2 = bf16[272,128]{1,0:T(8,128)(2,1)S(1)} collective-permute-done((bf16[272,128]{1,0:T(8,128)(2,1)S(1)}, bf16[272,128]{1,0:T(8,128)(2,1)S(1)}, u32[]{:S(2)}, u32[]{:S(2)}) %collective-permute-start.2) | collective-permute-done | bytes 69664 | tf_op jit(solution)/shard_map/ppermute | solution.py:173
  17.7 3.9 %collective-permute-start.3 = (bf16[4,272,128]{2,1,0:T(8,128)(2,1)S(1)}, bf16[4,272,128]{2,1,0:T(8,128)(2,1)S(1)}, u32[]{:S(2)}, u32[]{:S(2)}) collective-permute-start(bf16[4,272,128]{2,1,0:T(8,128)(2,1)S(1)} %pad_maximum_fusion.1.own), channel_id=1, source_target_pairs={{0,1},{1,0},{2,3},{3,2},{4,5},{5,4},{6,7},{7,6},{8,9},{9,8},{10,11... | collective-permute-start | bytes 835592 | tf_op jit(solution)/shard_map/ppermute | solution.py:187
  21.6 0.1 pad_add_fusion.pos
  21.7 1.1 collective-permute-done.3.other
  22.8 0.0 copy-start.4
  22.8 0.7 copy-done.4
  23.5 1.2 dispatch.1
  24.7 0.0 copy-start.3
  24.7 1.0 copy-done.3
  25.6 0.0 copy-start
  25.6 0.0 copy-start.1
  25.7 24.1 %all-to-all-start = ((bf16[64,8,1024]{2,1,0:T(8,128)(2,1)}), bf16[64,8,1024]{2,1,0:T(8,128)(2,1)S(1)}, u32[]{:S(2)}, u32[]{:S(2)}) async-start(bf16[64,8,1024]{2,1,0:T(8,128)(2,1)} %bitcast.32), calls=%async_computation | async-start | bytes 2097152 | tf_op jit(solution)/shard_map/all_to_all | solution.py:201
  49.8 0.0 copy-done
  49.8 2.6 %collective-permute-start.6 = (bf16[4,2,256,256]{3,2,1,0:T(8,128)(2,1)S(1)}, bf16[4,2,256,256]{3,2,1,0:T(8,128)(2,1)}, u32[]{:S(2)}, u32[]{:S(2)}) collective-permute-start(bf16[4,2,256,256]{3,2,1,0:T(8,128)(2,1)S(1)} %bitcast.23), channel_id=1, source_target_pairs={{0,1},{1,0},{2,3},{3,2},{4,5},{5,4},{6,7},{7,6},{8,9},{9,8},{10,11... | collective-permute-start | bytes 3145736 | tf_op jit(solution)/shard_map/ppermute | solution.py:179
  52.4 0.0 copy-done.1
  52.4 1.9 %collective-permute-start.7 = (bf16[4,2,256,256]{3,2,1,0:T(8,128)(2,1)S(1)}, bf16[4,2,256,256]{3,2,1,0:T(8,128)(2,1)}, u32[]{:S(2)}, u32[]{:S(2)}) collective-permute-start(bf16[4,2,256,256]{3,2,1,0:T(8,128)(2,1)S(1)} %bitcast.26), channel_id=1, source_target_pairs={{0,1},{1,0},{2,3},{3,2},{4,5},{5,4},{6,7},{7,6},{8,9},{9,8},{10,11... | collective-permute-start | bytes 3145736 | tf_op jit(solution)/shard_map/ppermute | solution.py:179
  54.3 2.4 %collective-permute-start.8 = (bf16[256,2048]{1,0:T(8,128)(2,1)}, bf16[256,2048]{1,0:T(8,128)(2,1)}, u32[]{:S(2)}, u32[]{:S(2)}) collective-permute-start(bf16[256,2048]{1,0:T(8,128)(2,1)} %bitcast.29), channel_id=1, source_target_pairs={{0,1},{1,0},{2,3},{3,2},{4,5},{5,4},{6,7},{7,6},{8,9},{9,8},{10,11... | collective-permute-start | bytes 3145736 | tf_op jit(solution)/shard_map/ppermute | solution.py:179
  56.7 20.8 %all-to-all-done = bf16[64,8,1024]{2,1,0:T(8,128)(2,1)S(1)} async-done(((bf16[64,8,1024]{2,1,0:T(8,128)(2,1)}), bf16[64,8,1024]{2,1,0:T(8,128)(2,1)S(1)}, u32[]{:S(2)}, u32[]{:S(2)}) %all-to-all-start) | async-done | bytes 1048608 | tf_op jit(solution)/shard_map/all_to_all | solution.py:201
  77.5 0.9 slice_bitcast_fusion
  78.4 0.8 pad_maximum_fusion
  79.3 3.2 %collective-permute-start.4 = (bf16[272,1024]{1,0:T(8,128)(2,1)}, bf16[272,1024]{1,0:T(8,128)(2,1)}, u32[]{:S(2)}, u32[]{:S(2)}) collective-permute-start(bf16[272,1024]{1,0:T(8,128)(2,1)} %pad_maximum_fusion), channel_id=1, source_target_pairs={{0,2},{2,0},{1,3},{3,1},{4,6},{6,4},{5,7},{7,5},{8,10},{10,8},{9,1... | collective-permute-start | bytes 1671176 | tf_op jit(solution)/shard_map/ppermute | solution.py:204
  82.5 1.9 %collective-permute-start.5 = (bf16[256,1024]{1,0:T(8,128)(2,1)}, bf16[256,1024]{1,0:T(8,128)(2,1)}, u32[]{:S(2)}, u32[]{:S(2)}) collective-permute-start(bf16[256,1024]{1,0:T(8,128)(2,1)} %get-tuple-element.35), channel_id=1, source_target_pairs={{0,14},{2,4},{4,2},{6,8},{8,6},{10,12},{12,10},{14,0},{1,15},{3,5}... | collective-permute-start | bytes 1572872 | tf_op jit(solution)/shard_map/ppermute | solution.py:205
  84.4 0.0 collective-permute-done.6.wg2
  84.4 0.0 collective-permute-done.7.wu2
  84.4 0.0 copy-start.2
  84.4 2.9 %near.1 = (f32[512,512]{1,0:T(8,128)S(1)}, f32[512,512]{1,0:T(8,128)S(1)}, f32[512,128]{1,0:T(8,128)S(1)}) custom-call(s32[1]{0:T(128)} %bitcast.8.par, bf16[512,1024]{1,0:T(8,128)(2,1)S(1)} %bitcast.21, bf16[16,1024]{1,0:T(8,128)(2,1)S(1)} %get-tuple-element.22.gain, bf16[4,2,256,256]{3,2,1,0:T(8,128)(2,1)S(1)} %bitcast.24, ...), custom_call_target="tpu_custom_call" | custom-call | flops 1100000000 | bytes 4194304 | tf_op jit(solution)/shard_map/near/pallas_call | solution.py:207
  87.3 0.0 collective-permute-done.8.wd2
  87.3 9.0 %collective-permute-done.5.other_b = bf16[256,1024]{1,0:T(8,128)(2,1)} collective-permute-done((bf16[256,1024]{1,0:T(8,128)(2,1)}, bf16[256,1024]{1,0:T(8,128)(2,1)}, u32[]{:S(2)}, u32[]{:S(2)}) %collective-permute-start.5) | collective-permute-done | bytes 524320 | tf_op jit(solution)/shard_map/ppermute | solution.py:205
  96.3 0.0 collective-permute-done.4.other_a
  96.3 0.0 copy-done.2
  96.3 4.1 %far.1 = (bf16[256,1024]{1,0:T(8,128)(2,1)S(1)}, bf16[256,1024]{1,0:T(8,128)(2,1)S(1)}, bf16[512,512]{1,0:T(8,128)(2,1)S(1)}) custom-call(s32[1]{0:T(128)} %bitcast.8.par, bf16[272,1024]{1,0:T(8,128)(2,1)} %collective-permute-done.4.other_a, bf16[256,1024]{1,0:T(8,128)(2,1)} %collective-permute-done.5.other_b, f32[512,512]{1,0:T(8,128)S(1)} %get-tuple-element.23.gate, ...), custom_call_target="tpu_custom_call" | custom-call | flops 1600000000 | bytes 4194304 | tf_op jit(solution)/shard_map/far/pallas_call | solution.py:210
  100.5 1.9 %collective-permute-start.9 = (bf16[256,1024]{1,0:T(8,128)(2,1)S(1)}, bf16[256,1024]{1,0:T(8,128)(2,1)S(1)}, u32[]{:S(2)}, u32[]{:S(2)}) collective-permute-start(bf16[256,1024]{1,0:T(8,128)(2,1)S(1)} %get-tuple-element.27), channel_id=1, source_target_pairs={{0,2},{2,0},{1,3},{3,1},{4,6},{6,4},{5,7},{7,5},{8,10},{10,8},{9,1... | collective-permute-start | bytes 1572872 | tf_op jit(solution)/shard_map/ppermute | solution.py:219
  102.4 2.2 %collective-permute-start.10 = (bf16[256,1024]{1,0:T(8,128)(2,1)S(1)}, bf16[256,1024]{1,0:T(8,128)(2,1)S(1)}, u32[]{:S(2)}, u32[]{:S(2)}) collective-permute-start(bf16[256,1024]{1,0:T(8,128)(2,1)S(1)} %get-tuple-element.28), channel_id=1, source_target_pairs={{0,14},{2,4},{4,2},{6,8},{8,6},{10,12},{12,10},{14,0},{1,15},{3,5}... | collective-permute-start | bytes 1572872 | tf_op jit(solution)/shard_map/ppermute | solution.py:220
  104.6 2.0 %keep.1 = bf16[512,1024]{1,0:T(8,128)(2,1)S(1)} custom-call(s32[1]{0:T(128)} %bitcast.8.par, bf16[512,512]{1,0:T(8,128)(2,1)S(1)} %get-tuple-element.26.hidden, bf16[256,2048]{1,0:T(8,128)(2,1)S(1)} %bitcast.31, bf16[256,2048]{1,0:T(8,128)(2,1)} %collective-permute-done.8.wd2), custom_call_target="tpu_custom_call" | custom-call | flops 550000000 | bytes 4194304 | tf_op jit(solution)/shard_map/keep/pallas_call | solution.py:221
  106.6 5.4 %collective-permute-done.9.got_a = bf16[256,1024]{1,0:T(8,128)(2,1)S(1)} collective-permute-done((bf16[256,1024]{1,0:T(8,128)(2,1)S(1)}, bf16[256,1024]{1,0:T(8,128)(2,1)S(1)}, u32[]{:S(2)}, u32[]{:S(2)}) %collective-permute-start.9) | collective-permute-done | bytes 524320 | tf_op jit(solution)/shard_map/ppermute | solution.py:219
  111.9 3.1 %collective-permute-done.10.got_b = bf16[256,1024]{1,0:T(8,128)(2,1)S(1)} collective-permute-done((bf16[256,1024]{1,0:T(8,128)(2,1)S(1)}, bf16[256,1024]{1,0:T(8,128)(2,1)S(1)}, u32[]{:S(2)}, u32[]{:S(2)}) %collective-permute-start.10) | collective-permute-done | bytes 524320 | tf_op jit(solution)/shard_map/ppermute | solution.py:220
  115.1 0.3 pairsum.1
  115.3 0.0 copy-start.5
  115.4 35.5 %all_to_all.10 = bf16[64,8,1024]{2,1,0:T(8,128)(2,1)S(1)} all-to-all(bf16[64,8,1024]{2,1,0:T(8,128)(2,1)S(1)} %bitcast.22), channel_id=1, replica_groups=mesh['z'=8,'y'=8,'p'=4,'q'=2,'c'=2] {'z','y'}, dimensions={0} | all-to-all | bytes 2097152 | tf_op jit(solution)/shard_map/all_to_all | solution.py:227
  150.8 0.0 copy-done.5
  150.8 1.3 combine.1
  152.2 7.8 %collective-permute-start.11 = (f32[4,256,128]{2,1,0:T(8,128)S(1)}, f32[4,256,128]{2,1,0:T(8,128)S(1)}, u32[]{:S(2)}, u32[]{:S(2)}) collective-permute-start(f32[4,256,128]{2,1,0:T(8,128)S(1)} %get-tuple-element.30), channel_id=1, source_target_pairs={{0,1},{1,0},{2,3},{3,2},{4,5},{5,4},{6,7},{7,6},{8,9},{9,8},{10,11... | collective-permute-start | bytes 1572872 | tf_op jit(solution)/shard_map/ppermute | solution.py:236
  160.0 1.5 collective-permute-done.11.got
  161.5 0.1 fold.1
  161.6 2.2 %collective-permute-start.12 = (bf16[256,128]{1,0:T(8,128)(2,1)S(1)}, bf16[256,128]{1,0:T(8,128)(2,1)S(1)}, u32[]{:S(2)}, u32[]{:S(2)}) collective-permute-start(bf16[256,128]{1,0:T(8,128)(2,1)S(1)} %get-tuple-element.32), channel_id=1, source_target_pairs={{0,4},{4,8},{8,12},{12,0},{1,5},{5,9},{9,13},{13,1},{2,6},{6,10},{... | collective-permute-start | bytes 196616 | tf_op jit(solution)/shard_map/ppermute | solution.py:173
  163.8 4.9 %collective-permute-start.13 = (bf16[256,128]{1,0:T(8,128)(2,1)S(1)}, bf16[256,128]{1,0:T(8,128)(2,1)S(1)}, u32[]{:S(2)}, u32[]{:S(2)}) collective-permute-start(bf16[256,128]{1,0:T(8,128)(2,1)S(1)} %get-tuple-element.33), channel_id=1, source_target_pairs={{0,8},{4,12},{8,0},{12,4},{1,9},{5,13},{9,1},{13,5},{2,10},{6,14},... | collective-permute-start | bytes 196616 | tf_op jit(solution)/shard_map/ppermute | solution.py:173
  168.7 1.9 %collective-permute-start.14 = (bf16[256,128]{1,0:T(8,128)(2,1)S(1)}, bf16[256,128]{1,0:T(8,128)(2,1)S(1)}, u32[]{:S(2)}, u32[]{:S(2)}) collective-permute-start(bf16[256,128]{1,0:T(8,128)(2,1)S(1)} %get-tuple-element.34), channel_id=1, source_target_pairs={{0,12},{4,0},{8,4},{12,8},{1,13},{5,1},{9,5},{13,9},{2,14},{6,2},{... | collective-permute-start | bytes 196616 | tf_op jit(solution)/shard_map/ppermute | solution.py:173
  170.6 0.0 collective-permute-done.12
  170.6 4.0 %collective-permute-done.13 = bf16[256,128]{1,0:T(8,128)(2,1)S(1)} collective-permute-done((bf16[256,128]{1,0:T(8,128)(2,1)S(1)}, bf16[256,128]{1,0:T(8,128)(2,1)S(1)}, u32[]{:S(2)}, u32[]{:S(2)}) %collective-permute-start.13) | collective-permute-done | bytes 65568 | tf_op jit(solution)/shard_map/ppermute | solution.py:173
  174.7 1.5 collective-permute-done.14
  176.2 0.7 add_convert_fusion
  (2 shorter events, 0.0 us)
Async XLA Ops:
  1.0 11.1 %collective-permute-start.1 = (bf16[272,128]{1,0:T(8,128)(2,1)S(1)}, bf16[272,128]{1,0:T(8,128)(2,1)S(1)}, u32[]{:S(2)}, u32[]{:S(2)}) collective-permute-start(bf16[272,128]{1,0:T(8,128)(2,1)S(1)} %get-tuple-element.38), channel_id=1, source_target_pairs={{0,8},{4,12},{8,0},{12,4},{1,9},{5,13},{9,1},{13,5},{2,10},{6,14},... | collective-permute-start | bytes 208904 | tf_op jit(solution)/shard_map/ppermute | solution.py:173
  5.8 8.4 %collective-permute-start = (bf16[272,128]{1,0:T(8,128)(2,1)S(1)}, bf16[272,128]{1,0:T(8,128)(2,1)S(1)}, u32[]{:S(2)}, u32[]{:S(2)}) collective-permute-start(bf16[272,128]{1,0:T(8,128)(2,1)S(1)} %get-tuple-element.38), channel_id=1, source_target_pairs={{0,4},{4,8},{8,12},{12,0},{1,5},{5,9},{9,13},{13,1},{2,6},{6,10},{... | collective-permute-start | bytes 208904 | tf_op jit(solution)/shard_map/ppermute | solution.py:173
  10.1 7.6 %collective-permute-start.2 = (bf16[272,128]{1,0:T(8,128)(2,1)S(1)}, bf16[272,128]{1,0:T(8,128)(2,1)S(1)}, u32[]{:S(2)}, u32[]{:S(2)}) collective-permute-start(bf16[272,128]{1,0:T(8,128)(2,1)S(1)} %get-tuple-element.38), channel_id=1, source_target_pairs={{0,12},{4,0},{8,4},{12,8},{1,13},{5,1},{9,5},{13,9},{2,14},{6,2},{... | collective-permute-start | bytes 208904 | tf_op jit(solution)/shard_map/ppermute | solution.py:173
  17.7 5.1 %collective-permute-start.3 = (bf16[4,272,128]{2,1,0:T(8,128)(2,1)S(1)}, bf16[4,272,128]{2,1,0:T(8,128)(2,1)S(1)}, u32[]{:S(2)}, u32[]{:S(2)}) collective-permute-start(bf16[4,272,128]{2,1,0:T(8,128)(2,1)S(1)} %pad_maximum_fusion.1.own), channel_id=1, source_target_pairs={{0,1},{1,0},{2,3},{3,2},{4,5},{5,4},{6,7},{7,6},{8,9},{9,8},{10,11... | collective-permute-start | bytes 835592 | tf_op jit(solution)/shard_map/ppermute | solution.py:187
  22.8 0.7 copy-start.4
  24.7 1.0 copy-start.3
  25.6 24.1 %copy-start = (bf16[1,2048,256]{2,1,0:T(8,128)(2,1)S(1)}, bf16[1,2048,256]{2,1,0:T(8,128)(2,1)}, u32[]{:S(2)}) copy-start(bf16[1,2048,256]{2,1,0:T(8,128)(2,1)} %param.11) | copy-start | bytes 3145732
  25.6 26.7 %copy-start.1 = (bf16[1,2048,256]{2,1,0:T(8,128)(2,1)S(1)}, bf16[1,2048,256]{2,1,0:T(8,128)(2,1)}, u32[]{:S(2)}) copy-start(bf16[1,2048,256]{2,1,0:T(8,128)(2,1)} %param.12) | copy-start | bytes 3145732
  25.7 51.9 %all-to-all-start = ((bf16[64,8,1024]{2,1,0:T(8,128)(2,1)}), bf16[64,8,1024]{2,1,0:T(8,128)(2,1)S(1)}, u32[]{:S(2)}, u32[]{:S(2)}) async-start(bf16[64,8,1024]{2,1,0:T(8,128)(2,1)} %bitcast.32), calls=%async_computation | async-start | bytes 2097152 | tf_op jit(solution)/shard_map/all_to_all | solution.py:201
  49.8 34.6 %collective-permute-start.6 = (bf16[4,2,256,256]{3,2,1,0:T(8,128)(2,1)S(1)}, bf16[4,2,256,256]{3,2,1,0:T(8,128)(2,1)}, u32[]{:S(2)}, u32[]{:S(2)}) collective-permute-start(bf16[4,2,256,256]{3,2,1,0:T(8,128)(2,1)S(1)} %bitcast.23), channel_id=1, source_target_pairs={{0,1},{1,0},{2,3},{3,2},{4,5},{5,4},{6,7},{7,6},{8,9},{9,8},{10,11... | collective-permute-start | bytes 3145736 | tf_op jit(solution)/shard_map/ppermute | solution.py:179
  52.4 32.0 %collective-permute-start.7 = (bf16[4,2,256,256]{3,2,1,0:T(8,128)(2,1)S(1)}, bf16[4,2,256,256]{3,2,1,0:T(8,128)(2,1)}, u32[]{:S(2)}, u32[]{:S(2)}) collective-permute-start(bf16[4,2,256,256]{3,2,1,0:T(8,128)(2,1)S(1)} %bitcast.26), channel_id=1, source_target_pairs={{0,1},{1,0},{2,3},{3,2},{4,5},{5,4},{6,7},{7,6},{8,9},{9,8},{10,11... | collective-permute-start | bytes 3145736 | tf_op jit(solution)/shard_map/ppermute | solution.py:179
  54.3 33.0 %collective-permute-start.8 = (bf16[256,2048]{1,0:T(8,128)(2,1)}, bf16[256,2048]{1,0:T(8,128)(2,1)}, u32[]{:S(2)}, u32[]{:S(2)}) collective-permute-start(bf16[256,2048]{1,0:T(8,128)(2,1)} %bitcast.29), channel_id=1, source_target_pairs={{0,1},{1,0},{2,3},{3,2},{4,5},{5,4},{6,7},{7,6},{8,9},{9,8},{10,11... | collective-permute-start | bytes 3145736 | tf_op jit(solution)/shard_map/ppermute | solution.py:179
  79.3 17.1 %collective-permute-start.4 = (bf16[272,1024]{1,0:T(8,128)(2,1)}, bf16[272,1024]{1,0:T(8,128)(2,1)}, u32[]{:S(2)}, u32[]{:S(2)}) collective-permute-start(bf16[272,1024]{1,0:T(8,128)(2,1)} %pad_maximum_fusion), channel_id=1, source_target_pairs={{0,2},{2,0},{1,3},{3,1},{4,6},{6,4},{5,7},{7,5},{8,10},{10,8},{9,1... | collective-permute-start | bytes 1671176 | tf_op jit(solution)/shard_map/ppermute | solution.py:204
  82.5 13.9 %collective-permute-start.5 = (bf16[256,1024]{1,0:T(8,128)(2,1)}, bf16[256,1024]{1,0:T(8,128)(2,1)}, u32[]{:S(2)}, u32[]{:S(2)}) collective-permute-start(bf16[256,1024]{1,0:T(8,128)(2,1)} %get-tuple-element.35), channel_id=1, source_target_pairs={{0,14},{2,4},{4,2},{6,8},{8,6},{10,12},{12,10},{14,0},{1,15},{3,5}... | collective-permute-start | bytes 1572872 | tf_op jit(solution)/shard_map/ppermute | solution.py:205
  84.4 11.9 %copy-start.2 = (bf16[1,256,2048]{2,1,0:T(8,128)(2,1)S(1)}, bf16[1,256,2048]{2,1,0:T(8,128)(2,1)}, u32[]{:S(2)}) copy-start(bf16[1,256,2048]{2,1,0:T(8,128)(2,1)} %param.13) | copy-start | bytes 3145732
  100.5 11.5 %collective-permute-start.9 = (bf16[256,1024]{1,0:T(8,128)(2,1)S(1)}, bf16[256,1024]{1,0:T(8,128)(2,1)S(1)}, u32[]{:S(2)}, u32[]{:S(2)}) collective-permute-start(bf16[256,1024]{1,0:T(8,128)(2,1)S(1)} %get-tuple-element.27), channel_id=1, source_target_pairs={{0,2},{2,0},{1,3},{3,1},{4,6},{6,4},{5,7},{7,5},{8,10},{10,8},{9,1... | collective-permute-start | bytes 1572872 | tf_op jit(solution)/shard_map/ppermute | solution.py:219
  102.4 12.7 %collective-permute-start.10 = (bf16[256,1024]{1,0:T(8,128)(2,1)S(1)}, bf16[256,1024]{1,0:T(8,128)(2,1)S(1)}, u32[]{:S(2)}, u32[]{:S(2)}) collective-permute-start(bf16[256,1024]{1,0:T(8,128)(2,1)S(1)} %get-tuple-element.28), channel_id=1, source_target_pairs={{0,14},{2,4},{4,2},{6,8},{8,6},{10,12},{12,10},{14,0},{1,15},{3,5}... | collective-permute-start | bytes 1572872 | tf_op jit(solution)/shard_map/ppermute | solution.py:220
  115.3 35.5 %copy-start.5 = (f32[256,2]{0,1:T(2,128)S(1)}, f32[256,2]{0,1:T(2,128)}, u32[]{:S(2)}) copy-start(f32[256,2]{0,1:T(2,128)} %param.10) | copy-start | bytes 6148
  152.2 9.3 %collective-permute-start.11 = (f32[4,256,128]{2,1,0:T(8,128)S(1)}, f32[4,256,128]{2,1,0:T(8,128)S(1)}, u32[]{:S(2)}, u32[]{:S(2)}) collective-permute-start(f32[4,256,128]{2,1,0:T(8,128)S(1)} %get-tuple-element.30), channel_id=1, source_target_pairs={{0,1},{1,0},{2,3},{3,2},{4,5},{5,4},{6,7},{7,6},{8,9},{9,8},{10,11... | collective-permute-start | bytes 1572872 | tf_op jit(solution)/shard_map/ppermute | solution.py:236
  161.6 9.0 %collective-permute-start.12 = (bf16[256,128]{1,0:T(8,128)(2,1)S(1)}, bf16[256,128]{1,0:T(8,128)(2,1)S(1)}, u32[]{:S(2)}, u32[]{:S(2)}) collective-permute-start(bf16[256,128]{1,0:T(8,128)(2,1)S(1)} %get-tuple-element.32), channel_id=1, source_target_pairs={{0,4},{4,8},{8,12},{12,0},{1,5},{5,9},{9,13},{13,1},{2,6},{6,10},{... | collective-permute-start | bytes 196616 | tf_op jit(solution)/shard_map/ppermute | solution.py:173
  163.8 10.9 %collective-permute-start.13 = (bf16[256,128]{1,0:T(8,128)(2,1)S(1)}, bf16[256,128]{1,0:T(8,128)(2,1)S(1)}, u32[]{:S(2)}, u32[]{:S(2)}) collective-permute-start(bf16[256,128]{1,0:T(8,128)(2,1)S(1)} %get-tuple-element.33), channel_id=1, source_target_pairs={{0,8},{4,12},{8,0},{12,4},{1,9},{5,13},{9,1},{13,5},{2,10},{6,14},... | collective-permute-start | bytes 196616 | tf_op jit(solution)/shard_map/ppermute | solution.py:173
  168.7 7.5 %collective-permute-start.14 = (bf16[256,128]{1,0:T(8,128)(2,1)S(1)}, bf16[256,128]{1,0:T(8,128)(2,1)S(1)}, u32[]{:S(2)}, u32[]{:S(2)}) collective-permute-start(bf16[256,128]{1,0:T(8,128)(2,1)S(1)} %get-tuple-element.34), channel_id=1, source_target_pairs={{0,12},{4,0},{8,4},{12,8},{1,13},{5,1},{9,5},{13,9},{2,14},{6,2},{... | collective-permute-start | bytes 196616 | tf_op jit(solution)/shard_map/ppermute | solution.py:173

commit v3 on v2

v3 whole, which is shorter than its diff:
```python
import functools

import jax
import jax.numpy as jnp
from jax import lax
from jax.experimental import pallas as pl
from jax.experimental.pallas import tpu as pltpu
from jax.sharding import Mesh, PartitionSpec as P

EPS = 1e-06
PAD = 16
EP = ("z", "y")
X = ("g", "r")
TP = ("g", "r", "c")
F32 = jnp.float32
BF16 = jnp.bfloat16
INTERPRET = False


def vmem(n):
    return [pl.BlockSpec(memory_space=pltpu.VMEM)] * n


SMEM = pl.BlockSpec(memory_space=pltpu.SMEM)


def call(body, outs, n_in, scalar, flops, name, mib):
    return pl.pallas_call(
        body,
        out_shape=outs,
        in_specs=([SMEM] if scalar else []) + vmem(n_in),
        out_specs=tuple(vmem(len(outs))),
        cost_estimate=pl.CostEstimate(flops=flops, bytes_accessed=4 << 20, transcendentals=0),
        compiler_params=pltpu.CompilerParams(vmem_limit_bytes=mib << 20),
        name=name,
        interpret=INTERPRET,
    )


def dispatch_body(experts, pos, ids, mine, swapped, far, far_swapped, buf, rows, gain):
    tok = ids.shape[1]
    half = buf.shape[0] // experts
    core = pos[0]
    e_iota = lax.broadcasted_iota(jnp.int32, (experts, tok), 0)
    hit = [e_iota == ids[k : k + 1, :] for k in range(2)]
    named = (hit[0] | hit[1]).astype(F32).astype(BF16)
    before = lax.broadcasted_iota(jnp.int32, (tok, tok), 0) < lax.broadcasted_iota(
        jnp.int32, (tok, tok), 1
    )
    counts = jnp.dot(named, before.astype(F32).astype(BF16), preferred_element_type=F32)
    r_iota = lax.broadcasted_iota(jnp.int32, (buf.shape[0], tok), 0)
    place = None
    for k in range(2):
        slot = jnp.sum(jnp.where(hit[k], counts, 0.0), axis=0, keepdims=True).astype(jnp.int32)
        slot = slot - core * half
        row = jnp.where((slot >= 0) & (slot < half), ids[k : k + 1, :] * half + slot, -1)
        rows[k : k + 1, :] = row
        here = r_iota == row
        place = here if place is None else place | here
    place = place.astype(F32).astype(BF16)
    low = core == 0
    for s, (own, other) in enumerate(((mine, swapped), (far, far_swapped))):
        group = pos[1] if s == 0 else 1 - pos[1]
        cols = pl.ds(pl.multiple_of(group * 256, 256), 256)
        a = own[...]
        b = other[...]
        x = jnp.concatenate([jnp.where(low, a, b), jnp.where(low, b, a)], axis=1)
        buf[:, cols] = jnp.dot(place, x[:tok], preferred_element_type=F32).astype(BF16)
        gain[:, cols] = x[tok:]


def product(x, quarter, w):
    k = x.shape[1]
    return jnp.dot(x, w[:, pl.ds(quarter, 1)].reshape(k, w.shape[3]), preferred_element_type=F32)


def near_body(pos, mine, gain, wg, wu, wg2, wu2, gate, up, squares):
    x = mine[...].astype(F32)
    squares[...] = jnp.broadcast_to(jnp.sum(x * x, axis=1, keepdims=True), squares.shape)
    y = (x * gain[0:1, :].astype(F32)).astype(BF16)
    hid = wg.shape[3]
    for i, (w_gate, w_up) in enumerate(((wg, wu), (wg2, wu2))):
        cols = slice(i * hid, (i + 1) * hid)
        gate[:, cols] = product(y, pos[2], w_gate)
        up[:, cols] = product(y, pos[2], w_up)


def middle_body(
    pos, left, right, gain_l, gain_r, gate_in, up_in, squares_in, wg, wu, wg2, wu2, gate, up, squares
):
    total = squares_in[...]
    ys = []
    for piece, gain in ((left, gain_l), (right, gain_r)):
        x = piece[...].astype(F32)
        total = total + jnp.sum(x * x, axis=1, keepdims=True)
        ys.append((x * gain[0:1, :].astype(F32)).astype(BF16))
    squares[...] = total
    ql = (pos[2] + 3) % 4
    qr = (pos[2] + 1) % 4
    hid = wg.shape[3]
    for i, (w_gate, w_up) in enumerate(((wg, wu), (wg2, wu2))):
        cols = slice(i * hid, (i + 1) * hid)
        gate[:, cols] = gate_in[:, cols] + (product(ys[0], ql, w_gate) + product(ys[1], qr, w_gate))
        up[:, cols] = up_in[:, cols] + (product(ys[0], ql, w_up) + product(ys[1], qr, w_up))


def far_body(
    pos, left2, right2, gain, gate, up, squares, wg, wu, wg2, wu2, wd, wd2, send_a, send_b, hidden
):
    x = jnp.concatenate([left2[...], right2[...]], axis=0).astype(F32)
    total = squares[:, 0:1] + jnp.sum(x * x, axis=1, keepdims=True)
    factor = lax.rsqrt(total / (4 * x.shape[1]) + EPS)
    y = (x * gain[0:1, :].astype(F32)).astype(BF16)
    hid = wg.shape[3]
    quarter = (pos[2] + 2) % 4
    for i, (w_gate, w_up) in enumerate(((wg, wu), (wg2, wu2))):
        cols = slice(i * hid, (i + 1) * hid)
        g = (gate[:, cols] + product(y, quarter, w_gate)) * factor
        u = (up[:, cols] + product(y, quarter, w_up)) * factor
        hidden[:, cols] = (g / (1.0 + jnp.exp(-g)) * u).astype(BF16)
    down(hidden[...], wd, wd2, quarter, (send_a, send_b))


def down(hid, wd, wd2, quarter, outs):
    k = wd.shape[0]
    rows = hid.shape[0] // len(outs)
    for g in range(2):
        cols = pl.ds(pl.multiple_of(g * 1024 + quarter * 256, 256), 256)
        y = (
            jnp.dot(hid[:, :k], wd[:, cols], preferred_element_type=F32)
            + jnp.dot(hid[:, k:], wd2[:, cols], preferred_element_type=F32)
        ).astype(BF16)
        for i, out in enumerate(outs):
            out[:, g * 256 : (g + 1) * 256] = y[i * rows : (i + 1) * rows]


def keep_body(pos, hidden, wd, wd2, to_left, keep, to_right):
    hid = hidden[...]
    down(hid, wd, wd2, (pos[2] + 3) % 4, (to_left,))
    down(hid, wd, wd2, pos[2], (keep,))
    down(hid, wd, wd2, (pos[2] + 1) % 4, (to_right,))


def relay_body(to_left, to_right, got_a, got_b, left, right):
    h = got_a.shape[0]
    right[:h] = (to_right[:h].astype(F32) + got_a[...].astype(F32)).astype(BF16)
    right[h:] = to_right[h:]
    left[:h] = to_left[:h]
    left[h:] = (to_left[h:].astype(F32) + got_b[...].astype(F32)).astype(BF16)


def add_body(keep, got_a, got_b, out):
    out[...] = (
        keep[...].astype(F32) + got_a[...].astype(F32) + got_b[...].astype(F32)
    ).astype(BF16)


def combine_body(pos, rows, share, back, own, swapped, far, far_swapped):
    n = back.shape[0]
    tok = rows.shape[1]
    r_iota = lax.broadcasted_iota(jnp.int32, (n, tok), 0)
    weight = jnp.zeros((n, tok), F32)
    for k in range(2):
        weight = jnp.where(r_iota == rows[k : k + 1, :], share[k : k + 1, :], weight)
    high = weight.astype(BF16)
    low = (weight - high.astype(F32)).astype(BF16)
    dims = (((0,), (0,)), ((), ()))
    first = pos[0] == 0
    for s, (mine, other) in enumerate(((own, swapped), (far, far_swapped))):
        group = pos[1] if s == 0 else 1 - pos[1]
        x = back[:, pl.ds(pl.multiple_of(group * 256, 256), 256)]
        y = lax.dot_general(high, x, dims, preferred_element_type=F32) + lax.dot_general(
            low, x, dims, preferred_element_type=F32
        )
        a = y[:, :128]
        b = y[:, 128:]
        mine[...] = jnp.where(first, a, b).astype(mine.dtype)
        other[...] = jnp.where(first, b, a).astype(other.dtype)


def shards(tokens, norm_gain, expert_ids, gate_share, gate_weight, up_weight, down_weight):
    tok, width = tokens.shape
    n_ep = lax.axis_size("z") * lax.axis_size("y")
    slot_cap = 4 * tok // n_ep
    half = slot_cap // 2
    n = n_ep * half
    h = n // 2
    feats = 4 * width
    pos = jnp.stack([lax.axis_index("c"), lax.axis_index("g"), lax.axis_index("r")])
    pos = pos.astype(jnp.int32)
    swap = [(0, 1), (1, 0)]

    def step(x, s):
        return lax.ppermute(x, X, [(i, (i + s) % 8) for i in range(8)])

    def flip(x, bits):
        return lax.ppermute(x, TP, [(i, i ^ bits) for i in range(16)])

    hid = gate_weight.shape[2]
    wg = gate_weight.reshape(2, 4, 256, hid)
    wu = up_weight.reshape(2, 4, 256, hid)
    wd = down_weight.reshape(hid, down_weight.shape[2])
    wg2, wu2, wd2 = (lax.ppermute(w, "c", swap) for w in (wg, wu, wd))

    mine = jnp.where(
        lax.broadcasted_iota(jnp.int32, (tok + PAD, width), 0) < tok,
        jnp.pad(tokens, ((0, PAD), (0, 0))),
        norm_gain[None, :],
    )
    far, far_swapped, swapped = flip(mine, 8), flip(mine, 9), flip(mine, 1)

    def shape(*dims, dtype=BF16):
        return jax.ShapeDtypeStruct(dims, dtype)

    buf, rows, gain = call(
        functools.partial(dispatch_body, n_ep),
        (shape(n, feats), shape(2, tok, dtype=jnp.int32), shape(PAD, feats)),
        5,
        True,
        150_000_000,
        "dispatch",
        8,
    )(pos, expert_ids.T, mine, swapped, far, far_swapped)
    gain_l, gain_r, gain_2 = step(gain, 1), step(gain, -1), step(gain, 2)
    here = lax.all_to_all(
        buf.reshape(n_ep, half, feats), EP, split_axis=0, concat_axis=0, tiled=True
    ).reshape(n, feats)
    here, gain_l, gain_r, gain_2 = lax.optimization_barrier((here, gain_l, gain_r, gain_2))
    wide = shape(n, 2 * hid, dtype=F32)
    thin = shape(n, 128, dtype=F32)
    left = step(here, 1)
    right = step(here, -1)
    gate, up, squares = call(near_body, (wide, wide, thin), 6, True, 600_000_000, "near", 8)(
        pos, here, gain, wg, wu, wg2, wu2
    )
    left2 = step(left[:h], 1)
    right2 = step(right[h:], -1)
    gate, up, squares = call(
        middle_body, (wide, wide, thin), 11, True, 1_100_000_000, "middle", 10
    )(pos, left, right, gain_l, gain_r, gate, up, squares, wg, wu, wg2, wu2)
    send_a, send_b, hidden = call(
        far_body,
        (shape(h, feats), shape(h, feats), shape(n, 2 * hid)),
        12,
        True,
        800_000_000,
        "far",
        10,
    )(pos, left2, right2, gain_2, gate, up, squares, wg, wu, wg2, wu2, wd, wd2)
    got_a = step(send_a, 1)
    got_b = step(send_b, -1)
    whole = shape(n, feats)
    to_left, keep, to_right = call(
        keep_body, (whole, whole, whole), 3, True, 800_000_000, "keep", 6
    )(pos, hidden, wd, wd2)
    to_left, to_right = call(relay_body, (whole, whole), 4, False, 1_000_000, "relay", 4)(
        to_left, to_right, got_a, got_b
    )
    from_left = step(to_right, 1)
    from_right = step(to_left, -1)
    (sums,) = call(add_body, (whole,), 3, False, 1_000_000, "pairsum", 4)(
        keep, from_left, from_right
    )
    returned = lax.all_to_all(
        sums.reshape(n_ep, half, feats), EP, split_axis=0, concat_axis=0, tiled=True
    ).reshape(n, feats)
    part = shape(tok, width, dtype=F32)
    sent = shape(tok, width)
    own, swapped, far, far_swapped = call(
        combine_body, (part, part, sent, sent), 3, True, 300_000_000, "combine", 8
    )(pos, rows, gate_share.T, returned)
    total = own + flip(far, 8).astype(F32) + flip(far_swapped, 9).astype(F32) + flip(swapped, 1)
    return total.astype(BF16)


def solution(mesh):
    n_ep, n_tp = mesh.devices.shape
    side = 8 if n_ep == 64 else n_ep
    fine = Mesh(
        mesh.devices.reshape(n_ep // side, side, 2, n_tp // 4, 2), ("z", "y", "g", "r", "c")
    )
    tp = TP
    in_specs = (
        P(EP, tp),
        P(tp),
        P(EP, None),
        P(EP, None),
        P(EP, None, tp),
        P(EP, None, tp),
        P(EP, tp, None),
    )
    return jax.shard_map(
        shards, mesh=fine, in_specs=in_specs, out_specs=P(EP, tp), check_vma=False
    )
```

time: 180 us -> 177 us (0.983); the launches traced: 177 us -> 176 us
  starting transfers between devices: 72 us -> 98.2 us
  waiting for transfers between devices: 52.1 us -> 34.6 us
  blocking collectives: 35.5 us -> 26.7 us
    ppermute x12 -> x17, starting transfers between devices: 41 us -> 66.8 us  [the longest x11 36.9 us: step(): return lax.ppermute(x, X, [(i, (i + s) % 8) for i in range(8)])]
    all_to_all x1, waiting for transfers between devices: 20.8 us -> 0.01 us  [shards(): lax.all_to_all(buf.reshape(n_ep, half, feats), EP, split_axis=0, concat_a...]
    all_to_all x1, blocking collectives: 35.5 us -> 26.7 us  [shards(): lax.all_to_all(sums.reshape(n_ep, half, feats), EP, split_axis=0, concat_...]
    ppermute x12 -> x17, waiting for transfers between devices: 31.3 us -> 34.5 us  [the longest x11 22.8 us: step(): return lax.ppermute(x, X, [(i, (i + s) % 8) for i in range(8)])]
    pallas_call x6 -> x7, Pallas kernels: 10.7 us -> 11.1 us  [the longest x1 2.74 us: shards(): call(far_body, (shape(h, feats), shape(h, feats), shape(n, 2 * hid)), 12,...]
  transfers between devices with their start and end apart: 16 -> 21, of which waited for: 10 -> 10; matrix products, arithmetic and copies ran while one was open for 1% -> 0% of each run, Pallas kernels for 3% -> 4%
where the time goes in v3:
time: 177 us; the launch traced here: 176 us
  starting transfers between devices  98.2 us (55%)
  waiting for transfers between devices  34.6 us (20%)
  blocking collectives  26.7 us (15%)
  Pallas kernels  12.9 us (7%)
  other arithmetic  1.77 us (1%)
    ppermute x11, starting transfers between devices, step(): return lax.ppermute(x, X, [(i, (i + s) % 8) for i in range(8)])  36.9 us
    ppermute x6, starting transfers between devices, flip(): return lax.ppermute(x, TP, [(i, i ^ bits) for i in range(16)])  29.9 us
    all_to_all x1, blocking collectives, shards(): lax.all_to_all(sums.reshape(n_ep, half, feats), EP, split_axis=0, concat_...  26.7 us
    all_to_all x1, starting transfers between devices, shards(): lax.all_to_all(buf.reshape(n_ep, half, feats), EP, split_axis=0, concat_a...  24.6 us
    ppermute x11, waiting for transfers between devices, step(): return lax.ppermute(x, X, [(i, (i + s) % 8) for i in range(8)])  22.8 us
    ppermute x6, waiting for transfers between devices, flip(): return lax.ppermute(x, TP, [(i, i ^ bits) for i in range(16)])  11.8 us
    ppermute x3, starting transfers between devices, shards(): wg2, wu2, wd2 = (lax.ppermute(w, 'c', swap) for w in (wg, wu, wd))  6.82 us
  transfers between devices with their start and end apart: 21, of which 10 were waited for; matrix products, arithmetic and copies ran while one was open for 0% of the time, Pallas kernels for 4%

profile of v3, /device:TPU:15, one launch (start us, length us, event | category | flops | bytes accessed | tf_op | source)
XLA Modules:
  0.0 175.9 jit_solution(9921666834617292123)
XLA Ops:
  0.0 0.0 copy-start
  0.0 1.0 pad_select_fusion.mine
  1.1 2.6 %collective-permute-start = (bf16[272,128]{1,0:T(8,128)(2,1)S(1)}, bf16[272,128]{1,0:T(8,128)(2,1)S(1)}, u32[]{:S(2)}, u32[]{:S(2)}) collective-permute-start(bf16[272,128]{1,0:T(8,128)(2,1)S(1)} %pad_select_fusion.mine), channel_id=1, source_target_pairs={{0,1},{1,0},{2,3},{3,2},{4,5},{5,4},{6,7},{7,6},{8,9},{9,8},{10,11... | collective-permute-start | bytes 208904 | tf_op jit(solution)/shard_map/ppermute | solution.py:197
  3.6 4.8 %collective-permute-start.1 = (bf16[272,128]{1,0:T(8,128)(2,1)S(1)}, bf16[272,128]{1,0:T(8,128)(2,1)S(1)}, u32[]{:S(2)}, u32[]{:S(2)}) collective-permute-start(bf16[272,128]{1,0:T(8,128)(2,1)S(1)} %pad_select_fusion.mine), channel_id=1, source_target_pairs={{0,8},{1,9},{2,10},{3,11},{4,12},{5,13},{6,14},{7,15},{8,0},{9,1},... | collective-permute-start | bytes 208904 | tf_op jit(solution)/shard_map/ppermute | solution.py:197
  8.4 4.6 %collective-permute-start.2 = (bf16[272,128]{1,0:T(8,128)(2,1)S(1)}, bf16[272,128]{1,0:T(8,128)(2,1)S(1)}, u32[]{:S(2)}, u32[]{:S(2)}) collective-permute-start(bf16[272,128]{1,0:T(8,128)(2,1)S(1)} %pad_select_fusion.mine), channel_id=1, source_target_pairs={{0,9},{1,8},{2,11},{3,10},{4,13},{5,12},{6,15},{7,14},{8,1},{9,0},... | collective-permute-start | bytes 208904 | tf_op jit(solution)/shard_map/ppermute | solution.py:197
  13.0 0.1 pad_add_fusion.pos
  13.1 0.0 collective-permute-done.swapped
  13.1 1.5 collective-permute-done.1.far
  14.7 3.6 %collective-permute-done.2.far_swapped = bf16[272,128]{1,0:T(8,128)(2,1)S(1)} collective-permute-done((bf16[272,128]{1,0:T(8,128)(2,1)S(1)}, bf16[272,128]{1,0:T(8,128)(2,1)S(1)}, u32[]{:S(2)}, u32[]{:S(2)}) %collective-permute-start.2) | collective-permute-done | bytes 69664 | tf_op jit(solution)/shard_map/ppermute | solution.py:197
  18.3 0.0 copy-start.3
  18.3 0.7 copy-done.3
  19.0 1.8 %dispatch.1 = (bf16[512,512]{1,0:T(8,128)(2,1)}, s32[2,256]{1,0:T(2,128)S(1)}, bf16[16,512]{1,0:T(8,128)(2,1)S(1)}) custom-call(s32[3]{0:T(128)S(1)} %pad_add_fusion.pos, s32[2,256]{1,0:T(2,128)S(1)} %bitcast.25, bf16[272,128]{1,0:T(8,128)(2,1)S(1)} %pad_select_fusion.mine, bf16[272,128]{1,0:T(8,128)(2,1)S(1)} %collective-permute-done.swapped, ...), custom_call_target="tpu_custom_call" | custom-call | flops 150000000 | bytes 4194304 | tf_op jit(solution)/shard_map/dispatch/pallas_call | solution.py:215
  20.8 0.0 copy-start.1
  20.8 24.6 %all-to-all-start = ((bf16[64,8,512]{2,1,0:T(8,128)(2,1)}), bf16[64,8,512]{2,1,0:T(8,128)(2,1)}, u32[]{:S(2)}, u32[]{:S(2)}) async-start(bf16[64,8,512]{2,1,0:T(8,128)(2,1)} %bitcast.5), calls=%async_computation | async-start | bytes 1048576 | tf_op jit(solution)/shard_map/all_to_all | solution.py:225
  45.4 0.0 copy-done
  45.4 2.5 %collective-permute-start.10 = (bf16[2,4,256,256]{3,2,1,0:T(8,128)(2,1)S(1)}, bf16[2,4,256,256]{3,2,1,0:T(8,128)(2,1)S(1)}, u32[]{:S(2)}, u32[]{:S(2)}) collective-permute-start(bf16[2,4,256,256]{3,2,1,0:T(8,128)(2,1)S(1)} %bitcast.12), channel_id=1, source_target_pairs={{0,1},{1,0},{2,3},{3,2},{4,5},{5,4},{6,7},{7,6},{8,9},{9,8},{10,11... | collective-permute-start | bytes 3145736 | tf_op jit(solution)/shard_map/ppermute | solution.py:203
  47.9 1.9 %collective-permute-start.11 = (bf16[2,4,256,256]{3,2,1,0:T(8,128)(2,1)}, bf16[2,4,256,256]{3,2,1,0:T(8,128)(2,1)}, u32[]{:S(2)}, u32[]{:S(2)}) collective-permute-start(bf16[2,4,256,256]{3,2,1,0:T(8,128)(2,1)} %bitcast.16), channel_id=1, source_target_pairs={{0,1},{1,0},{2,3},{3,2},{4,5},{5,4},{6,7},{7,6},{8,9},{9,8},{10,11... | collective-permute-start | bytes 3145736 | tf_op jit(solution)/shard_map/ppermute | solution.py:203
  49.8 2.4 %collective-permute-start.12 = (bf16[256,2048]{1,0:T(8,128)(2,1)}, bf16[256,2048]{1,0:T(8,128)(2,1)}, u32[]{:S(2)}, u32[]{:S(2)}) collective-permute-start(bf16[256,2048]{1,0:T(8,128)(2,1)} %bitcast.21), channel_id=1, source_target_pairs={{0,1},{1,0},{2,3},{3,2},{4,5},{5,4},{6,7},{7,6},{8,9},{9,8},{10,11... | collective-permute-start | bytes 3145736 | tf_op jit(solution)/shard_map/ppermute | solution.py:203
  52.3 5.1 %collective-permute-start.3 = (bf16[16,512]{1,0:T(8,128)(2,1)S(1)}, bf16[16,512]{1,0:T(8,128)(2,1)S(1)}, u32[]{:S(2)}, u32[]{:S(2)}) collective-permute-start(bf16[16,512]{1,0:T(8,128)(2,1)S(1)} %get-tuple-element.32.gain), channel_id=1, source_target_pairs={{0,2},{2,4},{4,6},{6,8},{8,10},{10,12},{12,14},{14,0},{1,3},{3,5},... | collective-permute-start | bytes 49160 | tf_op jit(solution)/shard_map/ppermute | solution.py:194
  57.4 1.9 %collective-permute-start.4 = (bf16[16,512]{1,0:T(8,128)(2,1)S(1)}, bf16[16,512]{1,0:T(8,128)(2,1)S(1)}, u32[]{:S(2)}, u32[]{:S(2)}) collective-permute-start(bf16[16,512]{1,0:T(8,128)(2,1)S(1)} %get-tuple-element.32.gain), channel_id=1, source_target_pairs={{0,14},{2,0},{4,2},{6,4},{8,6},{10,8},{12,10},{14,12},{1,15},{3,1}... | collective-permute-start | bytes 49160 | tf_op jit(solution)/shard_map/ppermute | solution.py:194
  59.3 0.0 collective-permute-done.3.gain_l
  59.3 4.9 %collective-permute-start.5 = (bf16[16,512]{1,0:T(8,128)(2,1)S(1)}, bf16[16,512]{1,0:T(8,128)(2,1)S(1)}, u32[]{:S(2)}, u32[]{:S(2)}) collective-permute-start(bf16[16,512]{1,0:T(8,128)(2,1)S(1)} %get-tuple-element.32.gain), channel_id=1, source_target_pairs={{0,4},{2,6},{4,8},{6,10},{8,12},{10,14},{12,0},{14,2},{1,5},{3,7},... | collective-permute-start | bytes 49160 | tf_op jit(solution)/shard_map/ppermute | solution.py:194
  64.2 0.0 collective-permute-done.4.gain_r
  64.2 0.8 collective-permute-done.5.gain
  65.0 0.0 all-to-all-done
  65.0 5.4 %collective-permute-start.6 = (bf16[512,512]{1,0:T(8,128)(2,1)}, bf16[512,512]{1,0:T(8,128)(2,1)S(1)}, u32[]{:S(2)}, u32[]{:S(2)}) collective-permute-start(bf16[512,512]{1,0:T(8,128)(2,1)} %bitcast.6.mine), channel_id=1, source_target_pairs={{0,2},{2,4},{4,6},{6,8},{8,10},{10,12},{12,14},{14,0},{1,3},{3,5},... | collective-permute-start | bytes 1572872 | tf_op jit(solution)/shard_map/ppermute | solution.py:194
  70.5 1.9 %collective-permute-start.8 = (bf16[512,512]{1,0:T(8,128)(2,1)}, bf16[512,512]{1,0:T(8,128)(2,1)S(1)}, u32[]{:S(2)}, u32[]{:S(2)}) collective-permute-start(bf16[512,512]{1,0:T(8,128)(2,1)} %bitcast.6.mine), channel_id=1, source_target_pairs={{0,14},{2,0},{4,2},{6,4},{8,6},{10,8},{12,10},{14,12},{1,15},{3,1}... | collective-permute-start | bytes 1572872 | tf_op jit(solution)/shard_map/ppermute | solution.py:194
  72.4 7.9 %collective-permute-done.6.left = bf16[512,512]{1,0:T(8,128)(2,1)S(1)} collective-permute-done((bf16[512,512]{1,0:T(8,128)(2,1)}, bf16[512,512]{1,0:T(8,128)(2,1)S(1)}, u32[]{:S(2)}, u32[]{:S(2)}) %collective-permute-start.6) | collective-permute-done | bytes 524320 | tf_op jit(solution)/shard_map/ppermute | solution.py:194
  80.3 5.2 %collective-permute-start.7 = (bf16[256,512]{1,0:T(8,128)(2,1)S(1)}, bf16[256,512]{1,0:T(8,128)(2,1)S(1)}, u32[]{:S(2)}, u32[]{:S(2)}) collective-permute-start(bf16[256,512]{1,0:T(8,128)(2,1)S(1)} %slice.8), channel_id=1, source_target_pairs={{0,2},{2,4},{4,6},{6,8},{8,10},{10,12},{12,14},{14,0},{1,3},{3,5},... | collective-permute-start | bytes 786440 | tf_op jit(solution)/shard_map/ppermute | solution.py:194
  85.6 0.0 collective-permute-done.8.right
  85.6 1.9 %collective-permute-start.9 = (bf16[256,512]{1,0:T(8,128)(2,1)S(1)}, bf16[256,512]{1,0:T(8,128)(2,1)S(1)}, u32[]{:S(2)}, u32[]{:S(2)}) collective-permute-start(bf16[256,512]{1,0:T(8,128)(2,1)S(1)} %slice.9), channel_id=1, source_target_pairs={{0,14},{2,0},{4,2},{6,4},{8,6},{10,8},{12,10},{14,12},{1,15},{3,1}... | collective-permute-start | bytes 786440 | tf_op jit(solution)/shard_map/ppermute | solution.py:194
  87.5 0.0 collective-permute-done.10.wg2
  87.5 0.0 collective-permute-done.11.wu2
  87.5 0.0 copy-done.1
  87.6 2.1 %near.1 = (f32[512,512]{1,0:T(8,128)S(1)}, f32[512,512]{1,0:T(8,128)S(1)}, f32[512,128]{1,0:T(8,128)S(1)}) custom-call(s32[3]{0:T(128)S(1)} %pad_add_fusion.pos, bf16[512,512]{1,0:T(8,128)(2,1)} %bitcast.6.mine, bf16[16,512]{1,0:T(8,128)(2,1)S(1)} %get-tuple-element.32.gain, bf16[2,4,256,256]{3,2,1,0:T(8,128)(2,1)S(1)} %bitcast.13, ...), custom_call_target="tpu_custom_call" | custom-call | flops 600000000 | bytes 4194304 | tf_op jit(solution)/shard_map/near/pallas_call | solution.py:233
  89.7 0.0 copy-start.2
  89.7 2.6 %middle.1 = (f32[512,512]{1,0:T(8,128)S(1)}, f32[512,512]{1,0:T(8,128)S(1)}, f32[512,128]{1,0:T(8,128)S(1)}) custom-call(s32[3]{0:T(128)S(1)} %pad_add_fusion.pos, bf16[512,512]{1,0:T(8,128)(2,1)S(1)} %collective-permute-done.6.left, bf16[512,512]{1,0:T(8,128)(2,1)S(1)} %collective-permute-done.8.right, bf16[16,512]{1,0:T(8,128)(2,1)S(1)} %collective-permute-done.3.gain_l, ...), custom_call_target="tpu_custom_call" | custom-call | flops 1100000000 | bytes 4194304 | tf_op jit(solution)/shard_map/middle/pallas_call | solution.py:238
  92.3 0.0 collective-permute-done.12.wd2
  92.3 0.0 collective-permute-done.7.left2
  92.3 1.6 collective-permute-done.9.right2
  93.9 0.0 copy-done.2
  93.9 2.7 %far.1 = (bf16[256,512]{1,0:T(8,128)(2,1)S(1)}, bf16[256,512]{1,0:T(8,128)(2,1)S(1)}, bf16[512,512]{1,0:T(8,128)(2,1)S(1)}) custom-call(s32[3]{0:T(128)S(1)} %pad_add_fusion.pos, bf16[256,512]{1,0:T(8,128)(2,1)S(1)} %collective-permute-done.7.left2, bf16[256,512]{1,0:T(8,128)(2,1)S(1)} %collective-permute-done.9.right2, ...), custom_call_target="tpu_custom_call" | custom-call | flops 800000000 | bytes 4194304 | tf_op jit(solution)/shard_map/far/pallas_call | solution.py:241
  96.7 3.0 %collective-permute-start.13 = (bf16[256,512]{1,0:T(8,128)(2,1)S(1)}, bf16[256,512]{1,0:T(8,128)(2,1)S(1)}, u32[]{:S(2)}, u32[]{:S(2)}) collective-permute-start(bf16[256,512]{1,0:T(8,128)(2,1)S(1)} %get-tuple-element.47), channel_id=1, source_target_pairs={{0,2},{2,4},{4,6},{6,8},{8,10},{10,12},{12,14},{14,0},{1,3},{3,5},... | collective-permute-start | bytes 786440 | tf_op jit(solution)/shard_map/ppermute | solution.py:194
  99.7 2.3 %collective-permute-start.14 = (bf16[256,512]{1,0:T(8,128)(2,1)S(1)}, bf16[256,512]{1,0:T(8,128)(2,1)S(1)}, u32[]{:S(2)}, u32[]{:S(2)}) collective-permute-start(bf16[256,512]{1,0:T(8,128)(2,1)S(1)} %get-tuple-element.48), channel_id=1, source_target_pairs={{0,14},{2,0},{4,2},{6,4},{8,6},{10,8},{12,10},{14,12},{1,15},{3,1}... | collective-permute-start | bytes 786440 | tf_op jit(solution)/shard_map/ppermute | solution.py:194
  102.0 2.2 %keep.1 = (bf16[512,512]{1,0:T(8,128)(2,1)S(1)}, bf16[512,512]{1,0:T(8,128)(2,1)S(1)}, bf16[512,512]{1,0:T(8,128)(2,1)S(1)}) custom-call(s32[3]{0:T(128)S(1)} %pad_add_fusion.pos, bf16[512,512]{1,0:T(8,128)(2,1)S(1)} %get-tuple-element.43.hidden, bf16[256,2048]{1,0:T(8,128)(2,1)S(1)} %bitcast.23, bf16[256,2048]{1,0:T(8,128)(2,1)} %collective-permute-done.12.wd2), custom_call_target="tpu_custom_call" | custom-call | flops 800000000 | bytes 4194304 | tf_op jit(solution)/shard_map/keep/pallas_call | solution.py:253
  104.2 0.0 collective-permute-done.13.got_a
  104.2 3.8 %collective-permute-done.14.got_b = bf16[256,512]{1,0:T(8,128)(2,1)S(1)} collective-permute-done((bf16[256,512]{1,0:T(8,128)(2,1)S(1)}, bf16[256,512]{1,0:T(8,128)(2,1)S(1)}, u32[]{:S(2)}, u32[]{:S(2)}) %collective-permute-start.14) | collective-permute-done | bytes 262176 | tf_op jit(solution)/shard_map/ppermute | solution.py:194
  108.0 0.1 relay.1
  108.1 1.9 %collective-permute-start.15 = (bf16[512,512]{1,0:T(8,128)(2,1)S(1)}, bf16[512,512]{1,0:T(8,128)(2,1)S(1)}, u32[]{:S(2)}, u32[]{:S(2)}) collective-permute-start(bf16[512,512]{1,0:T(8,128)(2,1)S(1)} %get-tuple-element.49), channel_id=1, source_target_pairs={{0,2},{2,4},{4,6},{6,8},{8,10},{10,12},{12,14},{14,0},{1,3},{3,5},... | collective-permute-start | bytes 1572872 | tf_op jit(solution)/shard_map/ppermute | solution.py:194
  110.1 3.4 %collective-permute-start.16 = (bf16[512,512]{1,0:T(8,128)(2,1)S(1)}, bf16[512,512]{1,0:T(8,128)(2,1)S(1)}, u32[]{:S(2)}, u32[]{:S(2)}) collective-permute-start(bf16[512,512]{1,0:T(8,128)(2,1)S(1)} %get-tuple-element.50), channel_id=1, source_target_pairs={{0,14},{2,0},{4,2},{6,4},{8,6},{10,8},{12,10},{14,12},{1,15},{3,1}... | collective-permute-start | bytes 1572872 | tf_op jit(solution)/shard_map/ppermute | solution.py:194
  113.4 5.5 %collective-permute-done.15.got_a = bf16[512,512]{1,0:T(8,128)(2,1)S(1)} collective-permute-done((bf16[512,512]{1,0:T(8,128)(2,1)S(1)}, bf16[512,512]{1,0:T(8,128)(2,1)S(1)}, u32[]{:S(2)}, u32[]{:S(2)}) %collective-permute-start.15) | collective-permute-done | bytes 524320 | tf_op jit(solution)/shard_map/ppermute | solution.py:194
  119.0 3.1 %collective-permute-done.16.got_b = bf16[512,512]{1,0:T(8,128)(2,1)S(1)} collective-permute-done((bf16[512,512]{1,0:T(8,128)(2,1)S(1)}, bf16[512,512]{1,0:T(8,128)(2,1)S(1)}, u32[]{:S(2)}, u32[]{:S(2)}) %collective-permute-start.16) | collective-permute-done | bytes 524320 | tf_op jit(solution)/shard_map/ppermute | solution.py:194
  122.1 0.2 pairsum.1
  122.3 26.7 %all_to_all.10 = bf16[64,8,512]{2,1,0:T(8,128)(2,1)S(1)} all-to-all(bf16[64,8,512]{2,1,0:T(8,128)(2,1)S(1)} %bitcast.20), channel_id=1, replica_groups=mesh['z'=8,'y'=8,'g'=2,'r'=4,'c'=2] {'z','y'}, dimensions={0} | all-to-all | bytes 1048576 | tf_op jit(solution)/shard_map/all_to_all | solution.py:264
  149.0 0.0 copy-start.4
  149.0 0.7 copy-done.4
  149.7 1.0 combine.1
  150.7 8.6 %collective-permute-start.19 = (f32[256,128]{1,0:T(8,128)S(1)}, f32[256,128]{1,0:T(8,128)S(1)}, u32[]{:S(2)}, u32[]{:S(2)}) collective-permute-start(f32[256,128]{1,0:T(8,128)S(1)} %get-tuple-element.54), channel_id=1, source_target_pairs={{0,1},{1,0},{2,3},{3,2},{4,5},{5,4},{6,7},{7,6},{8,9},{9,8},{10,11... | collective-permute-start | bytes 393224 | tf_op jit(solution)/shard_map/ppermute | solution.py:197
  159.3 4.7 %collective-permute-start.17 = (bf16[256,128]{1,0:T(8,128)(2,1)S(1)}, bf16[256,128]{1,0:T(8,128)(2,1)S(1)}, u32[]{:S(2)}, u32[]{:S(2)}) collective-permute-start(bf16[256,128]{1,0:T(8,128)(2,1)S(1)} %get-tuple-element.52), channel_id=1, source_target_pairs={{0,8},{1,9},{2,10},{3,11},{4,12},{5,13},{6,14},{7,15},{8,0},{9,1},... | collective-permute-start | bytes 196616 | tf_op jit(solution)/shard_map/ppermute | solution.py:197
  164.1 4.6 %collective-permute-start.18 = (bf16[256,128]{1,0:T(8,128)(2,1)S(1)}, bf16[256,128]{1,0:T(8,128)(2,1)S(1)}, u32[]{:S(2)}, u32[]{:S(2)}) collective-permute-start(bf16[256,128]{1,0:T(8,128)(2,1)S(1)} %get-tuple-element.53), channel_id=1, source_target_pairs={{0,9},{1,8},{2,11},{3,10},{4,13},{5,12},{6,15},{7,14},{8,1},{9,0},... | collective-permute-start | bytes 196616 | tf_op jit(solution)/shard_map/ppermute | solution.py:197
  168.7 1.5 collective-permute-done.17
  170.2 5.1 %collective-permute-done.18 = bf16[256,128]{1,0:T(8,128)(2,1)S(1)} collective-permute-done((bf16[256,128]{1,0:T(8,128)(2,1)S(1)}, bf16[256,128]{1,0:T(8,128)(2,1)S(1)}, u32[]{:S(2)}, u32[]{:S(2)}) %collective-permute-start.18) | collective-permute-done | bytes 65568 | tf_op jit(solution)/shard_map/ppermute | solution.py:197
  175.3 0.0 collective-permute-done.19
  175.3 0.7 add_convert_fusion
  (3 shorter events, 0.0 us)
Async XLA Ops:
  0.0 45.4 %copy-start = (bf16[1,2048,256]{2,1,0:T(8,128)(2,1)S(1)}, bf16[1,2048,256]{2,1,0:T(8,128)(2,1)}, u32[]{:S(2)}) copy-start(bf16[1,2048,256]{2,1,0:T(8,128)(2,1)} %param.11) | copy-start | bytes 3145732
  1.1 12.1 %collective-permute-start = (bf16[272,128]{1,0:T(8,128)(2,1)S(1)}, bf16[272,128]{1,0:T(8,128)(2,1)S(1)}, u32[]{:S(2)}, u32[]{:S(2)}) collective-permute-start(bf16[272,128]{1,0:T(8,128)(2,1)S(1)} %pad_select_fusion.mine), channel_id=1, source_target_pairs={{0,1},{1,0},{2,3},{3,2},{4,5},{5,4},{6,7},{7,6},{8,9},{9,8},{10,11... | collective-permute-start | bytes 208904 | tf_op jit(solution)/shard_map/ppermute | solution.py:197
  3.6 11.0 %collective-permute-start.1 = (bf16[272,128]{1,0:T(8,128)(2,1)S(1)}, bf16[272,128]{1,0:T(8,128)(2,1)S(1)}, u32[]{:S(2)}, u32[]{:S(2)}) collective-permute-start(bf16[272,128]{1,0:T(8,128)(2,1)S(1)} %pad_select_fusion.mine), channel_id=1, source_target_pairs={{0,8},{1,9},{2,10},{3,11},{4,12},{5,13},{6,14},{7,15},{8,0},{9,1},... | collective-permute-start | bytes 208904 | tf_op jit(solution)/shard_map/ppermute | solution.py:197
  8.4 9.9 %collective-permute-start.2 = (bf16[272,128]{1,0:T(8,128)(2,1)S(1)}, bf16[272,128]{1,0:T(8,128)(2,1)S(1)}, u32[]{:S(2)}, u32[]{:S(2)}) collective-permute-start(bf16[272,128]{1,0:T(8,128)(2,1)S(1)} %pad_select_fusion.mine), channel_id=1, source_target_pairs={{0,9},{1,8},{2,11},{3,10},{4,13},{5,12},{6,15},{7,14},{8,1},{9,0},... | collective-permute-start | bytes 208904 | tf_op jit(solution)/shard_map/ppermute | solution.py:197
  18.3 0.7 copy-start.3
  20.8 66.7 %copy-start.1 = (bf16[1,2048,256]{2,1,0:T(8,128)(2,1)S(1)}, bf16[1,2048,256]{2,1,0:T(8,128)(2,1)}, u32[]{:S(2)}) copy-start(bf16[1,2048,256]{2,1,0:T(8,128)(2,1)} %param.12) | copy-start | bytes 3145732
  20.8 44.2 %all-to-all-start = ((bf16[64,8,512]{2,1,0:T(8,128)(2,1)}), bf16[64,8,512]{2,1,0:T(8,128)(2,1)}, u32[]{:S(2)}, u32[]{:S(2)}) async-start(bf16[64,8,512]{2,1,0:T(8,128)(2,1)} %bitcast.5), calls=%async_computation | async-start | bytes 1048576 | tf_op jit(solution)/shard_map/all_to_all | solution.py:225
  45.4 42.1 %collective-permute-start.10 = (bf16[2,4,256,256]{3,2,1,0:T(8,128)(2,1)S(1)}, bf16[2,4,256,256]{3,2,1,0:T(8,128)(2,1)S(1)}, u32[]{:S(2)}, u32[]{:S(2)}) collective-permute-start(bf16[2,4,256,256]{3,2,1,0:T(8,128)(2,1)S(1)} %bitcast.12), channel_id=1, source_target_pairs={{0,1},{1,0},{2,3},{3,2},{4,5},{5,4},{6,7},{7,6},{8,9},{9,8},{10,11... | collective-permute-start | bytes 3145736 | tf_op jit(solution)/shard_map/ppermute | solution.py:203
  47.9 39.6 %collective-permute-start.11 = (bf16[2,4,256,256]{3,2,1,0:T(8,128)(2,1)}, bf16[2,4,256,256]{3,2,1,0:T(8,128)(2,1)}, u32[]{:S(2)}, u32[]{:S(2)}) collective-permute-start(bf16[2,4,256,256]{3,2,1,0:T(8,128)(2,1)} %bitcast.16), channel_id=1, source_target_pairs={{0,1},{1,0},{2,3},{3,2},{4,5},{5,4},{6,7},{7,6},{8,9},{9,8},{10,11... | collective-permute-start | bytes 3145736 | tf_op jit(solution)/shard_map/ppermute | solution.py:203
  49.8 42.5 %collective-permute-start.12 = (bf16[256,2048]{1,0:T(8,128)(2,1)}, bf16[256,2048]{1,0:T(8,128)(2,1)}, u32[]{:S(2)}, u32[]{:S(2)}) collective-permute-start(bf16[256,2048]{1,0:T(8,128)(2,1)} %bitcast.21), channel_id=1, source_target_pairs={{0,1},{1,0},{2,3},{3,2},{4,5},{5,4},{6,7},{7,6},{8,9},{9,8},{10,11... | collective-permute-start | bytes 3145736 | tf_op jit(solution)/shard_map/ppermute | solution.py:203
  52.3 7.0 %collective-permute-start.3 = (bf16[16,512]{1,0:T(8,128)(2,1)S(1)}, bf16[16,512]{1,0:T(8,128)(2,1)S(1)}, u32[]{:S(2)}, u32[]{:S(2)}) collective-permute-start(bf16[16,512]{1,0:T(8,128)(2,1)S(1)} %get-tuple-element.32.gain), channel_id=1, source_target_pairs={{0,2},{2,4},{4,6},{6,8},{8,10},{10,12},{12,14},{14,0},{1,3},{3,5},... | collective-permute-start | bytes 49160 | tf_op jit(solution)/shard_map/ppermute | solution.py:194
  57.4 6.8 %collective-permute-start.4 = (bf16[16,512]{1,0:T(8,128)(2,1)S(1)}, bf16[16,512]{1,0:T(8,128)(2,1)S(1)}, u32[]{:S(2)}, u32[]{:S(2)}) collective-permute-start(bf16[16,512]{1,0:T(8,128)(2,1)S(1)} %get-tuple-element.32.gain), channel_id=1, source_target_pairs={{0,14},{2,0},{4,2},{6,4},{8,6},{10,8},{12,10},{14,12},{1,15},{3,1}... | collective-permute-start | bytes 49160 | tf_op jit(solution)/shard_map/ppermute | solution.py:194
  59.3 5.8 %collective-permute-start.5 = (bf16[16,512]{1,0:T(8,128)(2,1)S(1)}, bf16[16,512]{1,0:T(8,128)(2,1)S(1)}, u32[]{:S(2)}, u32[]{:S(2)}) collective-permute-start(bf16[16,512]{1,0:T(8,128)(2,1)S(1)} %get-tuple-element.32.gain), channel_id=1, source_target_pairs={{0,4},{2,6},{4,8},{6,10},{8,12},{10,14},{12,0},{14,2},{1,5},{3,7},... | collective-permute-start | bytes 49160 | tf_op jit(solution)/shard_map/ppermute | solution.py:194
  65.0 15.3 %collective-permute-start.6 = (bf16[512,512]{1,0:T(8,128)(2,1)}, bf16[512,512]{1,0:T(8,128)(2,1)S(1)}, u32[]{:S(2)}, u32[]{:S(2)}) collective-permute-start(bf16[512,512]{1,0:T(8,128)(2,1)} %bitcast.6.mine), channel_id=1, source_target_pairs={{0,2},{2,4},{4,6},{6,8},{8,10},{10,12},{12,14},{14,0},{1,3},{3,5},... | collective-permute-start | bytes 1572872 | tf_op jit(solution)/shard_map/ppermute | solution.py:194
  70.5 15.1 %collective-permute-start.8 = (bf16[512,512]{1,0:T(8,128)(2,1)}, bf16[512,512]{1,0:T(8,128)(2,1)S(1)}, u32[]{:S(2)}, u32[]{:S(2)}) collective-permute-start(bf16[512,512]{1,0:T(8,128)(2,1)} %bitcast.6.mine), channel_id=1, source_target_pairs={{0,14},{2,0},{4,2},{6,4},{8,6},{10,8},{12,10},{14,12},{1,15},{3,1}... | collective-permute-start | bytes 1572872 | tf_op jit(solution)/shard_map/ppermute | solution.py:194
  80.3 12.0 %collective-permute-start.7 = (bf16[256,512]{1,0:T(8,128)(2,1)S(1)}, bf16[256,512]{1,0:T(8,128)(2,1)S(1)}, u32[]{:S(2)}, u32[]{:S(2)}) collective-permute-start(bf16[256,512]{1,0:T(8,128)(2,1)S(1)} %slice.8), channel_id=1, source_target_pairs={{0,2},{2,4},{4,6},{6,8},{8,10},{10,12},{12,14},{14,0},{1,3},{3,5},... | collective-permute-start | bytes 786440 | tf_op jit(solution)/shard_map/ppermute | solution.py:194
  85.6 8.3 %collective-permute-start.9 = (bf16[256,512]{1,0:T(8,128)(2,1)S(1)}, bf16[256,512]{1,0:T(8,128)(2,1)S(1)}, u32[]{:S(2)}, u32[]{:S(2)}) collective-permute-start(bf16[256,512]{1,0:T(8,128)(2,1)S(1)} %slice.9), channel_id=1, source_target_pairs={{0,14},{2,0},{4,2},{6,4},{8,6},{10,8},{12,10},{14,12},{1,15},{3,1}... | collective-permute-start | bytes 786440 | tf_op jit(solution)/shard_map/ppermute | solution.py:194
  89.7 4.2 %copy-start.2 = (bf16[1,256,2048]{2,1,0:T(8,128)(2,1)S(1)}, bf16[1,256,2048]{2,1,0:T(8,128)(2,1)}, u32[]{:S(2)}) copy-start(bf16[1,256,2048]{2,1,0:T(8,128)(2,1)} %param.13) | copy-start | bytes 3145732
  96.7 7.6 %collective-permute-start.13 = (bf16[256,512]{1,0:T(8,128)(2,1)S(1)}, bf16[256,512]{1,0:T(8,128)(2,1)S(1)}, u32[]{:S(2)}, u32[]{:S(2)}) collective-permute-start(bf16[256,512]{1,0:T(8,128)(2,1)S(1)} %get-tuple-element.47), channel_id=1, source_target_pairs={{0,2},{2,4},{4,6},{6,8},{8,10},{10,12},{12,14},{14,0},{1,3},{3,5},... | collective-permute-start | bytes 786440 | tf_op jit(solution)/shard_map/ppermute | solution.py:194
  99.7 8.3 %collective-permute-start.14 = (bf16[256,512]{1,0:T(8,128)(2,1)S(1)}, bf16[256,512]{1,0:T(8,128)(2,1)S(1)}, u32[]{:S(2)}, u32[]{:S(2)}) collective-permute-start(bf16[256,512]{1,0:T(8,128)(2,1)S(1)} %get-tuple-element.48), channel_id=1, source_target_pairs={{0,14},{2,0},{4,2},{6,4},{8,6},{10,8},{12,10},{14,12},{1,15},{3,1}... | collective-permute-start | bytes 786440 | tf_op jit(solution)/shard_map/ppermute | solution.py:194
  108.1 10.8 %collective-permute-start.15 = (bf16[512,512]{1,0:T(8,128)(2,1)S(1)}, bf16[512,512]{1,0:T(8,128)(2,1)S(1)}, u32[]{:S(2)}, u32[]{:S(2)}) collective-permute-start(bf16[512,512]{1,0:T(8,128)(2,1)S(1)} %get-tuple-element.49), channel_id=1, source_target_pairs={{0,2},{2,4},{4,6},{6,8},{8,10},{10,12},{12,14},{14,0},{1,3},{3,5},... | collective-permute-start | bytes 1572872 | tf_op jit(solution)/shard_map/ppermute | solution.py:194
  110.1 12.0 %collective-permute-start.16 = (bf16[512,512]{1,0:T(8,128)(2,1)S(1)}, bf16[512,512]{1,0:T(8,128)(2,1)S(1)}, u32[]{:S(2)}, u32[]{:S(2)}) collective-permute-start(bf16[512,512]{1,0:T(8,128)(2,1)S(1)} %get-tuple-element.50), channel_id=1, source_target_pairs={{0,14},{2,0},{4,2},{6,4},{8,6},{10,8},{12,10},{14,12},{1,15},{3,1}... | collective-permute-start | bytes 1572872 | tf_op jit(solution)/shard_map/ppermute | solution.py:194
  149.0 0.7 copy-start.4
  150.7 24.5 %collective-permute-start.19 = (f32[256,128]{1,0:T(8,128)S(1)}, f32[256,128]{1,0:T(8,128)S(1)}, u32[]{:S(2)}, u32[]{:S(2)}) collective-permute-start(f32[256,128]{1,0:T(8,128)S(1)} %get-tuple-element.54), channel_id=1, source_target_pairs={{0,1},{1,0},{2,3},{3,2},{4,5},{5,4},{6,7},{7,6},{8,9},{9,8},{10,11... | collective-permute-start | bytes 393224 | tf_op jit(solution)/shard_map/ppermute | solution.py:197
  159.3 10.9 %collective-permute-start.17 = (bf16[256,128]{1,0:T(8,128)(2,1)S(1)}, bf16[256,128]{1,0:T(8,128)(2,1)S(1)}, u32[]{:S(2)}, u32[]{:S(2)}) collective-permute-start(bf16[256,128]{1,0:T(8,128)(2,1)S(1)} %get-tuple-element.52), channel_id=1, source_target_pairs={{0,8},{1,9},{2,10},{3,11},{4,12},{5,13},{6,14},{7,15},{8,0},{9,1},... | collective-permute-start | bytes 196616 | tf_op jit(solution)/shard_map/ppermute | solution.py:197
  164.1 11.2 %collective-permute-start.18 = (bf16[256,128]{1,0:T(8,128)(2,1)S(1)}, bf16[256,128]{1,0:T(8,128)(2,1)S(1)}, u32[]{:S(2)}, u32[]{:S(2)}) collective-permute-start(bf16[256,128]{1,0:T(8,128)(2,1)S(1)} %get-tuple-element.53), channel_id=1, source_target_pairs={{0,9},{1,8},{2,11},{3,10},{4,13},{5,12},{6,15},{7,14},{8,1},{9,0},... | collective-permute-start | bytes 196616 | tf_op jit(solution)/shard_map/ppermute | solution.py:197

commit v4 on v3

v4 whole, which is shorter than its diff:
```python
import functools

import jax
import jax.numpy as jnp
from jax import lax
from jax.experimental import pallas as pl
from jax.experimental.pallas import tpu as pltpu
from jax.sharding import Mesh, PartitionSpec as P

EPS = 1e-06
PAD = 16
EP = ("z", "y")
X = ("g", "r")
TP = ("g", "r", "c")
F32 = jnp.float32
BF16 = jnp.bfloat16
INTERPRET = False


def vmem(n):
    return [pl.BlockSpec(memory_space=pltpu.VMEM)] * n


SMEM = pl.BlockSpec(memory_space=pltpu.SMEM)


def call(body, outs, n_in, scalar, flops, mib):
    return pl.pallas_call(
        body,
        out_shape=outs,
        in_specs=([SMEM] if scalar else []) + vmem(n_in),
        out_specs=tuple(vmem(len(outs))),
        cost_estimate=pl.CostEstimate(flops=flops, bytes_accessed=4 << 20, transcendentals=0),
        compiler_params=pltpu.CompilerParams(vmem_limit_bytes=mib << 20),
        interpret=INTERPRET,
    )


def slots_body(experts, pos, ids, rows, place):
    tok = ids.shape[1]
    half = place.shape[0] // experts
    e_iota = lax.broadcasted_iota(jnp.int32, (experts, tok), 0)
    hit = [e_iota == ids[k : k + 1, :] for k in range(2)]
    named = (hit[0] | hit[1]).astype(F32).astype(BF16)
    before = lax.broadcasted_iota(jnp.int32, (tok, tok), 0) < lax.broadcasted_iota(
        jnp.int32, (tok, tok), 1
    )
    counts = jnp.dot(named, before.astype(F32).astype(BF16), preferred_element_type=F32)
    r_iota = lax.broadcasted_iota(jnp.int32, place.shape, 0)
    here = None
    for k in range(2):
        slot = jnp.sum(jnp.where(hit[k], counts, 0.0), axis=0, keepdims=True).astype(jnp.int32)
        slot = slot - pos[0] * half
        row = jnp.where((slot >= 0) & (slot < half), ids[k : k + 1, :] * half + slot, -1)
        rows[k : k + 1, :] = row
        match = r_iota == row
        here = match if here is None else here | match
    place[...] = here.astype(F32).astype(BF16)


def dispatch_body(pos, place, own, other, buf, gain):
    tok = place.shape[1]
    low = pos[0] == 0
    for s in range(2):
        group = pos[1] if s == 0 else 1 - pos[1]
        cols = pl.ds(pl.multiple_of(group * 256, 256), 256)
        a = own[s]
        b = other[s]
        x = jnp.concatenate([jnp.where(low, a, b), jnp.where(low, b, a)], axis=1)
        buf[:, cols] = jnp.dot(place[...], x[:tok], preferred_element_type=F32).astype(BF16)
        gain[:, cols] = x[tok:]


def product(x, quarter, w):
    k = x.shape[1]
    return jnp.dot(x, w[:, pl.ds(quarter, 1)].reshape(k, w.shape[3]), preferred_element_type=F32)


def near_body(pos, mine, gain, wg, wu, gate, up, squares):
    x = mine[...].astype(F32)
    squares[...] = jnp.broadcast_to(jnp.sum(x * x, axis=1, keepdims=True), squares.shape)
    y = (x * gain[0:1, :].astype(F32)).astype(BF16)
    gate[...] = product(y, pos[2], wg)
    up[...] = product(y, pos[2], wu)


def middle_body(
    pos, mine, gain_m, left, right, gate_in, up_in, squares_in, wg, wu, wg2, wu2, gate, up, squares
):
    n = mine.shape[0]
    total = squares_in[...]
    ys = []
    for piece in (left, right):
        x = piece[:n].astype(F32)
        total = total + jnp.sum(x * x, axis=1, keepdims=True)
        ys.append((x * piece[n : n + 1, :].astype(F32)).astype(BF16))
    squares[...] = total
    y = (mine[...].astype(F32) * gain_m[0:1, :].astype(F32)).astype(BF16)
    ql = (pos[2] + 3) % 4
    qr = (pos[2] + 1) % 4
    hid = wg.shape[3]
    for w, start, out in ((wg, gate_in, gate), (wu, up_in, up)):
        out[:, :hid] = start[...] + (product(ys[0], ql, w) + product(ys[1], qr, w))
    for w, out in ((wg2, gate), (wu2, up)):
        out[:, hid:] = product(y, pos[2], w) + (product(ys[0], ql, w) + product(ys[1], qr, w))


def far_body(
    pos, left2, right2, gate, up, squares, wg, wu, wg2, wu2, wd, wd2, send_a, send_b, hidden
):
    h = left2.shape[0]
    x = jnp.concatenate([left2[...], right2[:h]], axis=0).astype(F32)
    total = squares[:, 0:1] + jnp.sum(x * x, axis=1, keepdims=True)
    factor = lax.rsqrt(total / (4 * x.shape[1]) + EPS)
    y = (x * right2[h : h + 1, :].astype(F32)).astype(BF16)
    hid = wg.shape[3]
    quarter = (pos[2] + 2) % 4
    for i, (w_gate, w_up) in enumerate(((wg, wu), (wg2, wu2))):
        cols = slice(i * hid, (i + 1) * hid)
        g = (gate[:, cols] + product(y, quarter, w_gate)) * factor
        u = (up[:, cols] + product(y, quarter, w_up)) * factor
        hidden[:, cols] = (g / (1.0 + jnp.exp(-g)) * u).astype(BF16)
    down(hidden[...], wd, wd2, quarter, (send_a, send_b))


def down(hid, wd, wd2, quarter, outs):
    k = wd.shape[0]
    rows = hid.shape[0] // len(outs)
    for g in range(2):
        cols = pl.ds(pl.multiple_of(g * 1024 + quarter * 256, 256), 256)
        y = (
            jnp.dot(hid[:, :k], wd[:, cols], preferred_element_type=F32)
            + jnp.dot(hid[:, k:], wd2[:, cols], preferred_element_type=F32)
        ).astype(BF16)
        for i, out in enumerate(outs):
            out[:, g * 256 : (g + 1) * 256] = y[i * rows : (i + 1) * rows]


def keep_body(pos, hidden, wd, wd2, to_left, keep, to_right):
    hid = hidden[...]
    down(hid, wd, wd2, (pos[2] + 3) % 4, (to_left,))
    down(hid, wd, wd2, pos[2], (keep,))
    down(hid, wd, wd2, (pos[2] + 1) % 4, (to_right,))


def relay_body(to_left, to_right, got_a, got_b, left, right):
    h = got_a.shape[0]
    right[:h] = (to_right[:h].astype(F32) + got_a[...].astype(F32)).astype(BF16)
    right[h:] = to_right[h:]
    left[:h] = to_left[:h]
    left[h:] = (to_left[h:].astype(F32) + got_b[...].astype(F32)).astype(BF16)


def add_body(keep, got_a, got_b, out):
    out[...] = (
        keep[...].astype(F32) + got_a[...].astype(F32) + got_b[...].astype(F32)
    ).astype(BF16)


def mix_body(rows, share, high, low):
    r_iota = lax.broadcasted_iota(jnp.int32, high.shape, 0)
    weight = jnp.zeros(high.shape, F32)
    for k in range(2):
        weight = jnp.where(r_iota == rows[k : k + 1, :], share[k : k + 1, :], weight)
    top = weight.astype(BF16)
    high[...] = top
    low[...] = (weight - top.astype(F32)).astype(BF16)


def combine_body(pos, high, low, back, near, near_away, far, far_away):
    dims = (((0,), (0,)), ((), ()))
    first = pos[0] == 0
    for s, (mine, other) in enumerate(((near, near_away), (far, far_away))):
        group = pos[1] if s == 0 else 1 - pos[1]
        x = back[:, pl.ds(pl.multiple_of(group * 256, 256), 256)]
        y = lax.dot_general(high[...], x, dims, preferred_element_type=F32) + lax.dot_general(
            low[...], x, dims, preferred_element_type=F32
        )
        a = y[:, :128]
        b = y[:, 128:]
        mine[...] = jnp.where(first, a, b)
        other[...] = jnp.where(first, b, a)


def fold_body(own, got, out):
    out[...] = (own[...] + got[...]).astype(BF16)


def shards(tokens, norm_gain, expert_ids, gate_share, gate_weight, up_weight, down_weight):
    tok, width = tokens.shape
    n_ep = lax.axis_size("z") * lax.axis_size("y")
    slot_cap = 4 * tok // n_ep
    half = slot_cap // 2
    n = n_ep * half
    h = n // 2
    feats = 4 * width
    pos = jnp.stack([lax.axis_index("c"), lax.axis_index("g"), lax.axis_index("r")])
    pos = pos.astype(jnp.int32)

    def step(x, s):
        return lax.ppermute(x, X, [(i, (i + s) % 8) for i in range(8)])

    def flip(x, bits):
        return lax.ppermute(x, TP, [(i, i ^ bits) for i in range(16)])

    hid = gate_weight.shape[2]
    wg = gate_weight.reshape(2, 4, 256, hid)
    wu = up_weight.reshape(2, 4, 256, hid)
    wd = down_weight.reshape(hid, down_weight.shape[2])

    def shape(*dims, dtype=BF16):
        return jax.ShapeDtypeStruct(dims, dtype)

    rows, place = call(
        functools.partial(slots_body, n_ep),
        (shape(2, tok, dtype=jnp.int32), shape(n, tok)),
        1,
        True,
        20_000_000,
        4,
    )(pos, expert_ids.T)
    mine = jnp.where(
        lax.broadcasted_iota(jnp.int32, (tok + PAD, width), 0) < tok,
        jnp.pad(tokens, ((0, PAD), (0, 0))),
        norm_gain[None, :],
    )
    own = jnp.stack([mine, flip(mine, 8)])
    other = flip(own, 1)
    buf, gain = call(
        dispatch_body, (shape(n, feats), shape(PAD, feats)), 3, True, 150_000_000, 4
    )(pos, place, own, other)
    here = lax.all_to_all(
        buf.reshape(n_ep, half, feats), EP, split_axis=0, concat_axis=0, tiled=True
    ).reshape(n, feats)
    sent = jnp.concatenate([here, gain], axis=0)
    left = step(sent, 1)
    right = step(sent, -1)
    wg2, wu2, wd2 = flip(wg, 1), flip(wu, 1), flip(wd, 1)
    wide = shape(n, 2 * hid, dtype=F32)
    slim = shape(n, hid, dtype=F32)
    thin = shape(n, 128, dtype=F32)
    gate, up, squares = call(near_body, (slim, slim, thin), 4, True, 300_000_000, 6)(
        pos, here, gain, wg, wu
    )
    left, right, gate = lax.optimization_barrier((left, right, gate))
    left2 = step(left[:h], 1)
    right2 = step(right[h:], -1)
    gate, up, squares = call(
        middle_body, (wide, wide, thin), 11, True, 1_300_000_000, 10
    )(pos, here, gain, left, right, gate, up, squares, wg, wu, wg2, wu2)
    send_a, send_b, hidden = call(
        far_body, (shape(h, feats), shape(h, feats), shape(n, 2 * hid)), 11, True, 800_000_000, 10
    )(pos, left2, right2, gate, up, squares, wg, wu, wg2, wu2, wd, wd2)
    got_a = step(send_a, 1)
    got_b = step(send_b, -1)
    whole = shape(n, feats)
    to_left, keep, to_right = call(
        keep_body, (whole, whole, whole), 3, True, 800_000_000, 6
    )(pos, hidden, wd, wd2)
    to_left, to_right = call(relay_body, (whole, whole), 4, False, 1_000_000, 4)(
        to_left, to_right, got_a, got_b
    )
    from_left = step(to_right, 1)
    from_right = step(to_left, -1)
    (sums,) = call(add_body, (whole,), 3, False, 1_000_000, 4)(keep, from_left, from_right)
    returned = lax.all_to_all(
        sums.reshape(n_ep, half, feats), EP, split_axis=0, concat_axis=0, tiled=True
    ).reshape(n, feats)
    high, low = call(mix_body, (shape(n, tok), shape(n, tok)), 2, False, 1_000_000, 4)(
        rows, gate_share.T
    )
    part = shape(tok, width, dtype=F32)
    near, near_away, far, far_away = call(
        combine_body, (part, part, part, part), 3, True, 300_000_000, 6
    )(pos, high, low, returned)
    (folded,) = call(fold_body, (shape(tok, width),), 2, False, 1_000_000, 2)(
        far, flip(far_away, 1)
    )
    return (near + flip(near_away, 1) + flip(folded, 8).astype(F32)).astype(BF16)


def solution(mesh):
    n_ep, n_tp = mesh.devices.shape
    side = 8 if n_ep == 64 else n_ep
    fine = Mesh(
        mesh.devices.reshape(n_ep // side, side, 2, n_tp // 4, 2), ("z", "y", "g", "r", "c")
    )
    tp = TP
    in_specs = (
        P(EP, tp),
        P(tp),
        P(EP, None),
        P(EP, None),
        P(EP, None, tp),
        P(EP, None, tp),
        P(EP, tp, None),
    )
    return jax.shard_map(shards, mesh=fine, in_specs=in_specs, out_specs=P(EP, tp), check_vma=False)
```

time: 177 us -> 166 us (0.938)
  blocking collectives: 26.7 us -> 0 us
  waiting for transfers between devices: 34.6 us -> 56.5 us
  starting transfers between devices: 98.2 us -> 90.3 us
    all_to_all x1 -> x0, blocking collectives: 26.7 us -> none  [shards(): lax.all_to_all(sums.reshape(n_ep, half, feats), EP, split_axis=0, concat_...]
    all_to_all x0 -> x1, waiting for transfers between devices: none -> 14.5 us  [shards(): lax.all_to_all(sums.reshape(n_ep, half, feats), EP, split_axis=0, concat_...]
    ppermute x11 -> x8, starting transfers between devices: 36.9 us -> 24.9 us  [step(): return lax.ppermute(x, X, [(i, (i + s) % 8) for i in range(8)])]
    all_to_all x1, waiting for transfers between devices: 0.01 us -> 11.4 us  [shards(): lax.all_to_all(buf.reshape(n_ep, half, feats), EP, split_axis=0, concat_a...]
    all_to_all x0 -> x1, starting transfers between devices: none -> 9.1 us  [shards(): lax.all_to_all(sums.reshape(n_ep, half, feats), EP, split_axis=0, concat_...]
    ppermute x3 -> x0, starting transfers between devices: 6.82 us -> none  [shards(): wg2, wu2, wd2 = (lax.ppermute(w, 'c', swap) for w in (wg, wu, wd))]
    ppermute x6 -> x8, waiting for transfers between devices: 11.8 us -> 8.39 us  [flip(): return lax.ppermute(x, TP, [(i, i ^ bits) for i in range(16)])]
    ppermute x6 -> x8, starting transfers between devices: 29.9 us -> 32.3 us  [flip(): return lax.ppermute(x, TP, [(i, i ^ bits) for i in range(16)])]
  transfers between devices with their start and end apart: 21 -> 18, of which waited for: 10 -> 10; matrix products, arithmetic and copies ran while one was open for 0% -> 0% of each run, Pallas kernels for 4% -> 5%
where the time goes in v4:
time: 166 us; the launch traced here: 164 us
  starting transfers between devices  90.3 us (54%)
  waiting for transfers between devices  56.5 us (34%)
  Pallas kernels  14.3 us (9%)
  other arithmetic  1.83 us (1%)
    ppermute x8, starting transfers between devices, flip(): return lax.ppermute(x, TP, [(i, i ^ bits) for i in range(16)])  32.3 us
    ppermute x8, starting transfers between devices, step(): return lax.ppermute(x, X, [(i, (i + s) % 8) for i in range(8)])  24.9 us
    all_to_all x1, starting transfers between devices, shards(): lax.all_to_all(buf.reshape(n_ep, half, feats), EP, split_axis=0, concat_a...  24 us
    ppermute x8, waiting for transfers between devices, step(): return lax.ppermute(x, X, [(i, (i + s) % 8) for i in range(8)])  22.2 us
    all_to_all x1, waiting for transfers between devices, shards(): lax.all_to_all(sums.reshape(n_ep, half, feats), EP, split_axis=0, concat_...  14.5 us
    all_to_all x1, waiting for transfers between devices, shards(): lax.all_to_all(buf.reshape(n_ep, half, feats), EP, split_axis=0, concat_a...  11.4 us
    all_to_all x1, starting transfers between devices, shards(): lax.all_to_all(sums.reshape(n_ep, half, feats), EP, split_axis=0, concat_...  9.1 us
    ppermute x8, waiting for transfers between devices, flip(): return lax.ppermute(x, TP, [(i, i ^ bits) for i in range(16)])  8.39 us
  transfers between devices with their start and end apart: 18, of which 10 were waited for; matrix products, arithmetic and copies ran while one was open for 0% of the time, Pallas kernels for 5%

profile of v4, /device:TPU:15, one launch (start us, length us, event | category | flops | bytes accessed | tf_op | source)
XLA Modules:
  0.0 164.1 jit_solution(1217322967189199668)
XLA Ops:
  0.0 0.0 copy-start.1
  0.0 1.0 fusion
  1.1 0.0 copy-start
  1.1 4.9 %collective-permute-start = (bf16[272,128]{1,0:T(8,128)(2,1)S(1)}, bf16[272,128]{1,0:T(8,128)(2,1)S(1)}, u32[]{:S(2)}, u32[]{:S(2)}) collective-permute-start(bf16[272,128]{1,0:T(8,128)(2,1)S(1)} %get-tuple-element.60), channel_id=1, source_target_pairs={{0,8},{1,9},{2,10},{3,11},{4,12},{5,13},{6,14},{7,15},{8,0},{9,1},... | collective-permute-start | bytes 208904 | tf_op jit(solution)/shard_map/ppermute | solution.py:204
  6.0 4.4 %collective-permute-done = bf16[272,128]{1,0:T(8,128)(2,1)S(1)} collective-permute-done((bf16[272,128]{1,0:T(8,128)(2,1)S(1)}, bf16[272,128]{1,0:T(8,128)(2,1)S(1)}, u32[]{:S(2)}, u32[]{:S(2)}) %collective-permute-start) | collective-permute-done | bytes 69664 | tf_op jit(solution)/shard_map/ppermute | solution.py:204
  10.4 4.7 %collective-permute-start.1 = (bf16[2,272,128]{2,1,0:T(8,128)(2,1)S(1)}, bf16[2,272,128]{2,1,0:T(8,128)(2,1)S(1)}, u32[]{:S(2)}, u32[]{:S(2)}) collective-permute-start(bf16[2,272,128]{2,1,0:T(8,128)(2,1)S(1)} %pad_maximum_fusion.1.own), channel_id=1, source_target_pairs={{0,1},{1,0},{2,3},{3,2},{4,5},{5,4},{6,7},{7,6},{8,9},{9,8},{10,11... | collective-permute-start | bytes 417800 | tf_op jit(solution)/shard_map/ppermute | solution.py:204
  15.1 0.1 pad_add_fusion.pos
  15.2 0.0 copy-start.4
  15.2 0.7 copy-done.4
  15.8 0.8 shard_map.73
  16.7 0.0 collective-permute-done.1.other
  16.7 1.7 %shard_map.75 = (bf16[512,512]{1,0:T(8,128)(2,1)}, bf16[16,512]{1,0:T(8,128)(2,1)S(1)}) custom-call(s32[3]{0:T(128)S(1)} %pad_add_fusion.pos, bf16[512,256]{1,0:T(8,128)(2,1)S(1)} %get-tuple-element.35.place, bf16[2,272,128]{2,1,0:T(8,128)(2,1)S(1)} %pad_maximum_fusion.1.own, bf16[2,272,128]{2,1,0:T(8,128)(2,1)S(1)} %collective-permute-done.1.other), custom_call_target="tpu_custom_call" | custom-call | flops 150000000 | bytes 4194304 | tf_op jit(solution)/shard_map/pallas_call | solution.py:229
  18.3 24.0 %all-to-all-start = ((bf16[64,8,512]{2,1,0:T(8,128)(2,1)}), bf16[64,8,512]{2,1,0:T(8,128)(2,1)S(1)}, u32[]{:S(2)}, u32[]{:S(2)}) async-start(bf16[64,8,512]{2,1,0:T(8,128)(2,1)} %bitcast.7), calls=%async_computation | async-start | bytes 1048576 | tf_op jit(solution)/shard_map/all_to_all | solution.py:232
  42.4 0.0 copy-done
  42.4 2.2 %collective-permute-start.6 = (bf16[2,4,256,256]{3,2,1,0:T(8,128)(2,1)S(1)}, bf16[2,4,256,256]{3,2,1,0:T(8,128)(2,1)}, u32[]{:S(2)}, u32[]{:S(2)}) collective-permute-start(bf16[2,4,256,256]{3,2,1,0:T(8,128)(2,1)S(1)} %bitcast.15), channel_id=1, source_target_pairs={{0,1},{1,0},{2,3},{3,2},{4,5},{5,4},{6,7},{7,6},{8,9},{9,8},{10,11... | collective-permute-start | bytes 3145736 | tf_op jit(solution)/shard_map/ppermute | solution.py:204
  44.6 0.0 copy-done.1
  44.6 2.1 %collective-permute-start.7 = (bf16[2,4,256,256]{3,2,1,0:T(8,128)(2,1)S(1)}, bf16[2,4,256,256]{3,2,1,0:T(8,128)(2,1)}, u32[]{:S(2)}, u32[]{:S(2)}) collective-permute-start(bf16[2,4,256,256]{3,2,1,0:T(8,128)(2,1)S(1)} %bitcast.19), channel_id=1, source_target_pairs={{0,1},{1,0},{2,3},{3,2},{4,5},{5,4},{6,7},{7,6},{8,9},{9,8},{10,11... | collective-permute-start | bytes 3145736 | tf_op jit(solution)/shard_map/ppermute | solution.py:204
  46.7 2.2 %collective-permute-start.8 = (bf16[256,2048]{1,0:T(8,128)(2,1)}, bf16[256,2048]{1,0:T(8,128)(2,1)}, u32[]{:S(2)}, u32[]{:S(2)}) collective-permute-start(bf16[256,2048]{1,0:T(8,128)(2,1)} %bitcast.26), channel_id=1, source_target_pairs={{0,1},{1,0},{2,3},{3,2},{4,5},{5,4},{6,7},{7,6},{8,9},{9,8},{10,11... | collective-permute-start | bytes 3145736 | tf_op jit(solution)/shard_map/ppermute | solution.py:204
  48.9 11.4 %all-to-all-done = bf16[64,8,512]{2,1,0:T(8,128)(2,1)S(1)} async-done(((bf16[64,8,512]{2,1,0:T(8,128)(2,1)}), bf16[64,8,512]{2,1,0:T(8,128)(2,1)S(1)}, u32[]{:S(2)}, u32[]{:S(2)}) %all-to-all-start) | async-done | bytes 524320 | tf_op jit(solution)/shard_map/all_to_all | solution.py:232
  60.4 1.9 %collective-permute-start.2 = (bf16[528,512]{1,0:T(8,128)(2,1)S(1)}, bf16[528,512]{1,0:T(8,128)(2,1)S(1)}, u32[]{:S(2)}, u32[]{:S(2)}) collective-permute-start(bf16[528,512]{1,0:T(8,128)(2,1)S(1)} %pad_maximum_fusion), channel_id=1, source_target_pairs={{0,2},{2,4},{4,6},{6,8},{8,10},{10,12},{12,14},{14,0},{1,3},{3,5},... | collective-permute-start | bytes 1622024 | tf_op jit(solution)/shard_map/ppermute | solution.py:201
  62.3 3.4 %collective-permute-start.3 = (bf16[528,512]{1,0:T(8,128)(2,1)S(1)}, bf16[528,512]{1,0:T(8,128)(2,1)S(1)}, u32[]{:S(2)}, u32[]{:S(2)}) collective-permute-start(bf16[528,512]{1,0:T(8,128)(2,1)S(1)} %pad_maximum_fusion), channel_id=1, source_target_pairs={{0,14},{2,0},{4,2},{6,4},{8,6},{10,8},{12,10},{14,12},{1,15},{3,1}... | collective-permute-start | bytes 1622024 | tf_op jit(solution)/shard_map/ppermute | solution.py:201
  65.7 1.0 shard_map.76
  66.7 8.0 %collective-permute-done.2.left = bf16[528,512]{1,0:T(8,128)(2,1)S(1)} collective-permute-done((bf16[528,512]{1,0:T(8,128)(2,1)S(1)}, bf16[528,512]{1,0:T(8,128)(2,1)S(1)}, u32[]{:S(2)}, u32[]{:S(2)}) %collective-permute-start.2) | collective-permute-done | bytes 540704 | tf_op jit(solution)/shard_map/ppermute | solution.py:201
  74.7 3.1 %collective-permute-done.3.right = bf16[528,512]{1,0:T(8,128)(2,1)S(1)} collective-permute-done((bf16[528,512]{1,0:T(8,128)(2,1)S(1)}, bf16[528,512]{1,0:T(8,128)(2,1)S(1)}, u32[]{:S(2)}, u32[]{:S(2)}) %collective-permute-start.3) | collective-permute-done | bytes 540704 | tf_op jit(solution)/shard_map/ppermute | solution.py:201
  77.9 1.9 %collective-permute-start.5 = (bf16[272,512]{1,0:T(8,128)(2,1)S(1)}, bf16[272,512]{1,0:T(8,128)(2,1)S(1)}, u32[]{:S(2)}, u32[]{:S(2)}) collective-permute-start(bf16[272,512]{1,0:T(8,128)(2,1)S(1)} %slice.7), channel_id=1, source_target_pairs={{0,14},{2,0},{4,2},{6,4},{8,6},{10,8},{12,10},{14,12},{1,15},{3,1}... | collective-permute-start | bytes 835592 | tf_op jit(solution)/shard_map/ppermute | solution.py:201
  79.8 4.6 %collective-permute-start.4 = (bf16[256,512]{1,0:T(8,128)(2,1)S(1)}, bf16[256,512]{1,0:T(8,128)(2,1)S(1)}, u32[]{:S(2)}, u32[]{:S(2)}) collective-permute-start(bf16[256,512]{1,0:T(8,128)(2,1)S(1)} %slice.6), channel_id=1, source_target_pairs={{0,2},{2,4},{4,6},{6,8},{8,10},{10,12},{12,14},{14,0},{1,3},{3,5},... | collective-permute-start | bytes 786440 | tf_op jit(solution)/shard_map/ppermute | solution.py:201
  84.4 0.0 collective-permute-done.6.wg2
  84.4 0.0 collective-permute-done.7.wu2
  84.4 0.0 copy-start.2
  84.4 3.2 %shard_map.77 = (f32[512,512]{1,0:T(8,128)S(1)}, f32[512,512]{1,0:T(8,128)S(1)}, f32[512,128]{1,0:T(8,128)S(1)}) custom-call(s32[3]{0:T(128)S(1)} %pad_add_fusion.pos, bf16[512,512]{1,0:T(8,128)(2,1)S(1)} %bitcast.25, bf16[16,512]{1,0:T(8,128)(2,1)S(1)} %get-tuple-element.37.gain.gain_m, bf16[528,512]{1,0:T(8,128)(2,1)S(1)} %collective-permute-done.2.left, ...), custom_call_target="tpu_custom_call" | custom-call | flops 1300000000 | bytes 4194304 | tf_op jit(solution)/shard_map/pallas_call | solution.py:248
  87.6 0.0 collective-permute-done.8.wd2
  87.6 0.1 collective-permute-done.4.left2
  87.7 0.0 collective-permute-done.5.right2
  87.7 0.0 copy-done.2
  87.7 3.1 %shard_map.78 = (bf16[256,512]{1,0:T(8,128)(2,1)S(1)}, bf16[256,512]{1,0:T(8,128)(2,1)S(1)}, bf16[512,512]{1,0:T(8,128)(2,1)S(1)}) custom-call(s32[3]{0:T(128)S(1)} %pad_add_fusion.pos, bf16[256,512]{1,0:T(8,128)(2,1)S(1)} %collective-permute-done.4.left2, bf16[272,512]{1,0:T(8,128)(2,1)S(1)} %collective-permute-done.5.right2, ...), custom_call_target="tpu_custom_call" | custom-call | flops 800000000 | bytes 4194304 | tf_op jit(solution)/shard_map/pallas_call | solution.py:251
  90.8 2.3 %collective-permute-start.10 = (bf16[256,512]{1,0:T(8,128)(2,1)S(1)}, bf16[256,512]{1,0:T(8,128)(2,1)S(1)}, u32[]{:S(2)}, u32[]{:S(2)}) collective-permute-start(bf16[256,512]{1,0:T(8,128)(2,1)S(1)} %get-tuple-element.52), channel_id=1, source_target_pairs={{0,14},{2,0},{4,2},{6,4},{8,6},{10,8},{12,10},{14,12},{1,15},{3,1}... | collective-permute-start | bytes 786440 | tf_op jit(solution)/shard_map/ppermute | solution.py:201
  93.1 4.6 %collective-permute-start.9 = (bf16[256,512]{1,0:T(8,128)(2,1)S(1)}, bf16[256,512]{1,0:T(8,128)(2,1)S(1)}, u32[]{:S(2)}, u32[]{:S(2)}) collective-permute-start(bf16[256,512]{1,0:T(8,128)(2,1)S(1)} %get-tuple-element.51), channel_id=1, source_target_pairs={{0,2},{2,4},{4,6},{6,8},{8,10},{10,12},{12,14},{14,0},{1,3},{3,5},... | collective-permute-start | bytes 786440 | tf_op jit(solution)/shard_map/ppermute | solution.py:201
  97.7 2.2 %shard_map.79 = (bf16[512,512]{1,0:T(8,128)(2,1)S(1)}, bf16[512,512]{1,0:T(8,128)(2,1)S(1)}, bf16[512,512]{1,0:T(8,128)(2,1)S(1)}) custom-call(s32[3]{0:T(128)S(1)} %pad_add_fusion.pos, bf16[512,512]{1,0:T(8,128)(2,1)S(1)} %get-tuple-element.47.hidden, bf16[256,2048]{1,0:T(8,128)(2,1)S(1)} %bitcast.28, bf16[256,2048]{1,0:T(8,128)(2,1)} %collective-permute-done.8.wd2), custom_call_target="tpu_custom_call" | custom-call | flops 800000000 | bytes 4194304 | tf_op jit(solution)/shard_map/pallas_call | solution.py:257
  100.0 0.0 collective-permute-done.10.got_b
  100.0 1.8 %collective-permute-done.9.got_a = bf16[256,512]{1,0:T(8,128)(2,1)S(1)} collective-permute-done((bf16[256,512]{1,0:T(8,128)(2,1)S(1)}, bf16[256,512]{1,0:T(8,128)(2,1)S(1)}, u32[]{:S(2)}, u32[]{:S(2)}) %collective-permute-start.9) | collective-permute-done | bytes 262176 | tf_op jit(solution)/shard_map/ppermute | solution.py:201
  101.8 0.2 shard_map.80
  101.9 4.3 %collective-permute-start.11 = (bf16[512,512]{1,0:T(8,128)(2,1)S(1)}, bf16[512,512]{1,0:T(8,128)(2,1)S(1)}, u32[]{:S(2)}, u32[]{:S(2)}) collective-permute-start(bf16[512,512]{1,0:T(8,128)(2,1)S(1)} %get-tuple-element.53), channel_id=1, source_target_pairs={{0,2},{2,4},{4,6},{6,8},{8,10},{10,12},{12,14},{14,0},{1,3},{3,5},... | collective-permute-start | bytes 1572872 | tf_op jit(solution)/shard_map/ppermute | solution.py:201
  106.2 1.9 %collective-permute-start.12 = (bf16[512,512]{1,0:T(8,128)(2,1)S(1)}, bf16[512,512]{1,0:T(8,128)(2,1)S(1)}, u32[]{:S(2)}, u32[]{:S(2)}) collective-permute-start(bf16[512,512]{1,0:T(8,128)(2,1)S(1)} %get-tuple-element.54), channel_id=1, source_target_pairs={{0,14},{2,0},{4,2},{6,4},{8,6},{10,8},{12,10},{14,12},{1,15},{3,1}... | collective-permute-start | bytes 1572872 | tf_op jit(solution)/shard_map/ppermute | solution.py:201
  108.2 5.2 %collective-permute-done.11.got_a = bf16[512,512]{1,0:T(8,128)(2,1)S(1)} collective-permute-done((bf16[512,512]{1,0:T(8,128)(2,1)S(1)}, bf16[512,512]{1,0:T(8,128)(2,1)S(1)}, u32[]{:S(2)}, u32[]{:S(2)}) %collective-permute-start.11) | collective-permute-done | bytes 524320 | tf_op jit(solution)/shard_map/ppermute | solution.py:201
  113.4 4.0 %collective-permute-done.12.got_b = bf16[512,512]{1,0:T(8,128)(2,1)S(1)} collective-permute-done((bf16[512,512]{1,0:T(8,128)(2,1)S(1)}, bf16[512,512]{1,0:T(8,128)(2,1)S(1)}, u32[]{:S(2)}, u32[]{:S(2)}) %collective-permute-start.12) | collective-permute-done | bytes 524320 | tf_op jit(solution)/shard_map/ppermute | solution.py:201
  117.4 1.0 shard_map.81
  118.3 0.0 copy-start.3
  118.3 9.1 %all-to-all-start.1 = ((bf16[64,8,512]{2,1,0:T(8,128)(2,1)}), bf16[64,8,512]{2,1,0:T(8,128)(2,1)S(1)}, u32[]{:S(2)}, u32[]{:S(2)}) async-start(bf16[64,8,512]{2,1,0:T(8,128)(2,1)} %bitcast.12), calls=%async_computation.1 | async-start | bytes 1048576 | tf_op jit(solution)/shard_map/all_to_all | solution.py:266
  127.4 0.0 copy-done.3
  127.5 0.1 shard_map.74
  127.6 14.5 %all-to-all-done.1 = bf16[64,8,512]{2,1,0:T(8,128)(2,1)S(1)} async-done(((bf16[64,8,512]{2,1,0:T(8,128)(2,1)}), bf16[64,8,512]{2,1,0:T(8,128)(2,1)S(1)}, u32[]{:S(2)}, u32[]{:S(2)}) %all-to-all-start.1) | async-done | bytes 524320 | tf_op jit(solution)/shard_map/all_to_all | solution.py:266
  142.1 1.0 shard_map.82
  143.2 8.2 %collective-permute-start.14 = (f32[256,128]{1,0:T(8,128)S(1)}, f32[256,128]{1,0:T(8,128)S(1)}, u32[]{:S(2)}, u32[]{:S(2)}) collective-permute-start(f32[256,128]{1,0:T(8,128)S(1)} %get-tuple-element.58), channel_id=1, source_target_pairs={{0,1},{1,0},{2,3},{3,2},{4,5},{5,4},{6,7},{7,6},{8,9},{9,8},{10,11... | collective-permute-start | bytes 393224 | tf_op jit(solution)/shard_map/ppermute | solution.py:204
  151.4 1.9 %collective-permute-start.13 = (f32[256,128]{1,0:T(8,128)S(1)}, f32[256,128]{1,0:T(8,128)S(1)}, u32[]{:S(2)}, u32[]{:S(2)}) collective-permute-start(f32[256,128]{1,0:T(8,128)S(1)} %get-tuple-element.56), channel_id=1, source_target_pairs={{0,1},{1,0},{2,3},{3,2},{4,5},{5,4},{6,7},{7,6},{8,9},{9,8},{10,11... | collective-permute-start | bytes 393224 | tf_op jit(solution)/shard_map/ppermute | solution.py:204
  153.3 0.0 collective-permute-done.14.got
  153.3 6.1 %collective-permute-start.15 = (bf16[256,128]{1,0:T(8,128)(2,1)S(1)}, bf16[256,128]{1,0:T(8,128)(2,1)S(1)}, u32[]{:S(2)}, u32[]{:S(2)}) collective-permute-start(bf16[256,128]{1,0:T(8,128)(2,1)S(1)} %shard_map.83), channel_id=1, source_target_pairs={{0,8},{1,9},{2,10},{3,11},{4,12},{5,13},{6,14},{7,15},{8,0},{9,1},... | collective-permute-start | bytes 196616 | tf_op jit(solution)/shard_map/ppermute | solution.py:204
  159.4 0.0 collective-permute-done.13
  159.4 4.0 %collective-permute-done.15 = bf16[256,128]{1,0:T(8,128)(2,1)S(1)} collective-permute-done((bf16[256,128]{1,0:T(8,128)(2,1)S(1)}, bf16[256,128]{1,0:T(8,128)(2,1)S(1)}, u32[]{:S(2)}, u32[]{:S(2)}) %collective-permute-start.15) | collective-permute-done | bytes 65568 | tf_op jit(solution)/shard_map/ppermute | solution.py:204
  163.4 0.7 add_convert_fusion
  (6 shorter events, 0.1 us)
Async XLA Ops:
  0.0 44.6 %copy-start.1 = (bf16[1,2048,256]{2,1,0:T(8,128)(2,1)S(1)}, bf16[1,2048,256]{2,1,0:T(8,128)(2,1)}, u32[]{:S(2)}) copy-start(bf16[1,2048,256]{2,1,0:T(8,128)(2,1)} %param.12) | copy-start | bytes 3145732
  1.1 41.3 %copy-start = (bf16[1,2048,256]{2,1,0:T(8,128)(2,1)S(1)}, bf16[1,2048,256]{2,1,0:T(8,128)(2,1)}, u32[]{:S(2)}) copy-start(bf16[1,2048,256]{2,1,0:T(8,128)(2,1)} %param.11) | copy-start | bytes 3145732
  1.1 9.3 %collective-permute-start = (bf16[272,128]{1,0:T(8,128)(2,1)S(1)}, bf16[272,128]{1,0:T(8,128)(2,1)S(1)}, u32[]{:S(2)}, u32[]{:S(2)}) collective-permute-start(bf16[272,128]{1,0:T(8,128)(2,1)S(1)} %get-tuple-element.60), channel_id=1, source_target_pairs={{0,8},{1,9},{2,10},{3,11},{4,12},{5,13},{6,14},{7,15},{8,0},{9,1},... | collective-permute-start | bytes 208904 | tf_op jit(solution)/shard_map/ppermute | solution.py:204
  10.4 6.3 %collective-permute-start.1 = (bf16[2,272,128]{2,1,0:T(8,128)(2,1)S(1)}, bf16[2,272,128]{2,1,0:T(8,128)(2,1)S(1)}, u32[]{:S(2)}, u32[]{:S(2)}) collective-permute-start(bf16[2,272,128]{2,1,0:T(8,128)(2,1)S(1)} %pad_maximum_fusion.1.own), channel_id=1, source_target_pairs={{0,1},{1,0},{2,3},{3,2},{4,5},{5,4},{6,7},{7,6},{8,9},{9,8},{10,11... | collective-permute-start | bytes 417800 | tf_op jit(solution)/shard_map/ppermute | solution.py:204
  15.2 0.7 copy-start.4
  18.3 42.0 %all-to-all-start = ((bf16[64,8,512]{2,1,0:T(8,128)(2,1)}), bf16[64,8,512]{2,1,0:T(8,128)(2,1)S(1)}, u32[]{:S(2)}, u32[]{:S(2)}) async-start(bf16[64,8,512]{2,1,0:T(8,128)(2,1)} %bitcast.7), calls=%async_computation | async-start | bytes 1048576 | tf_op jit(solution)/shard_map/all_to_all | solution.py:232
  42.4 42.0 %collective-permute-start.6 = (bf16[2,4,256,256]{3,2,1,0:T(8,128)(2,1)S(1)}, bf16[2,4,256,256]{3,2,1,0:T(8,128)(2,1)}, u32[]{:S(2)}, u32[]{:S(2)}) collective-permute-start(bf16[2,4,256,256]{3,2,1,0:T(8,128)(2,1)S(1)} %bitcast.15), channel_id=1, source_target_pairs={{0,1},{1,0},{2,3},{3,2},{4,5},{5,4},{6,7},{7,6},{8,9},{9,8},{10,11... | collective-permute-start | bytes 3145736 | tf_op jit(solution)/shard_map/ppermute | solution.py:204
  44.6 39.8 %collective-permute-start.7 = (bf16[2,4,256,256]{3,2,1,0:T(8,128)(2,1)S(1)}, bf16[2,4,256,256]{3,2,1,0:T(8,128)(2,1)}, u32[]{:S(2)}, u32[]{:S(2)}) collective-permute-start(bf16[2,4,256,256]{3,2,1,0:T(8,128)(2,1)S(1)} %bitcast.19), channel_id=1, source_target_pairs={{0,1},{1,0},{2,3},{3,2},{4,5},{5,4},{6,7},{7,6},{8,9},{9,8},{10,11... | collective-permute-start | bytes 3145736 | tf_op jit(solution)/shard_map/ppermute | solution.py:204
  46.7 40.9 %collective-permute-start.8 = (bf16[256,2048]{1,0:T(8,128)(2,1)}, bf16[256,2048]{1,0:T(8,128)(2,1)}, u32[]{:S(2)}, u32[]{:S(2)}) collective-permute-start(bf16[256,2048]{1,0:T(8,128)(2,1)} %bitcast.26), channel_id=1, source_target_pairs={{0,1},{1,0},{2,3},{3,2},{4,5},{5,4},{6,7},{7,6},{8,9},{9,8},{10,11... | collective-permute-start | bytes 3145736 | tf_op jit(solution)/shard_map/ppermute | solution.py:204
  60.4 14.3 %collective-permute-start.2 = (bf16[528,512]{1,0:T(8,128)(2,1)S(1)}, bf16[528,512]{1,0:T(8,128)(2,1)S(1)}, u32[]{:S(2)}, u32[]{:S(2)}) collective-permute-start(bf16[528,512]{1,0:T(8,128)(2,1)S(1)} %pad_maximum_fusion), channel_id=1, source_target_pairs={{0,2},{2,4},{4,6},{6,8},{8,10},{10,12},{12,14},{14,0},{1,3},{3,5},... | collective-permute-start | bytes 1622024 | tf_op jit(solution)/shard_map/ppermute | solution.py:201
  62.3 15.5 %collective-permute-start.3 = (bf16[528,512]{1,0:T(8,128)(2,1)S(1)}, bf16[528,512]{1,0:T(8,128)(2,1)S(1)}, u32[]{:S(2)}, u32[]{:S(2)}) collective-permute-start(bf16[528,512]{1,0:T(8,128)(2,1)S(1)} %pad_maximum_fusion), channel_id=1, source_target_pairs={{0,14},{2,0},{4,2},{6,4},{8,6},{10,8},{12,10},{14,12},{1,15},{3,1}... | collective-permute-start | bytes 1622024 | tf_op jit(solution)/shard_map/ppermute | solution.py:201
  77.9 9.8 %collective-permute-start.5 = (bf16[272,512]{1,0:T(8,128)(2,1)S(1)}, bf16[272,512]{1,0:T(8,128)(2,1)S(1)}, u32[]{:S(2)}, u32[]{:S(2)}) collective-permute-start(bf16[272,512]{1,0:T(8,128)(2,1)S(1)} %slice.7), channel_id=1, source_target_pairs={{0,14},{2,0},{4,2},{6,4},{8,6},{10,8},{12,10},{14,12},{1,15},{3,1}... | collective-permute-start | bytes 835592 | tf_op jit(solution)/shard_map/ppermute | solution.py:201
  79.8 7.9 %collective-permute-start.4 = (bf16[256,512]{1,0:T(8,128)(2,1)S(1)}, bf16[256,512]{1,0:T(8,128)(2,1)S(1)}, u32[]{:S(2)}, u32[]{:S(2)}) collective-permute-start(bf16[256,512]{1,0:T(8,128)(2,1)S(1)} %slice.6), channel_id=1, source_target_pairs={{0,2},{2,4},{4,6},{6,8},{8,10},{10,12},{12,14},{14,0},{1,3},{3,5},... | collective-permute-start | bytes 786440 | tf_op jit(solution)/shard_map/ppermute | solution.py:201
  84.4 3.3 %copy-start.2 = (bf16[1,256,2048]{2,1,0:T(8,128)(2,1)S(1)}, bf16[1,256,2048]{2,1,0:T(8,128)(2,1)}, u32[]{:S(2)}) copy-start(bf16[1,256,2048]{2,1,0:T(8,128)(2,1)} %param.13) | copy-start | bytes 3145732
  90.8 9.2 %collective-permute-start.10 = (bf16[256,512]{1,0:T(8,128)(2,1)S(1)}, bf16[256,512]{1,0:T(8,128)(2,1)S(1)}, u32[]{:S(2)}, u32[]{:S(2)}) collective-permute-start(bf16[256,512]{1,0:T(8,128)(2,1)S(1)} %get-tuple-element.52), channel_id=1, source_target_pairs={{0,14},{2,0},{4,2},{6,4},{8,6},{10,8},{12,10},{14,12},{1,15},{3,1}... | collective-permute-start | bytes 786440 | tf_op jit(solution)/shard_map/ppermute | solution.py:201
  93.1 8.7 %collective-permute-start.9 = (bf16[256,512]{1,0:T(8,128)(2,1)S(1)}, bf16[256,512]{1,0:T(8,128)(2,1)S(1)}, u32[]{:S(2)}, u32[]{:S(2)}) collective-permute-start(bf16[256,512]{1,0:T(8,128)(2,1)S(1)} %get-tuple-element.51), channel_id=1, source_target_pairs={{0,2},{2,4},{4,6},{6,8},{8,10},{10,12},{12,14},{14,0},{1,3},{3,5},... | collective-permute-start | bytes 786440 | tf_op jit(solution)/shard_map/ppermute | solution.py:201
  101.9 11.4 %collective-permute-start.11 = (bf16[512,512]{1,0:T(8,128)(2,1)S(1)}, bf16[512,512]{1,0:T(8,128)(2,1)S(1)}, u32[]{:S(2)}, u32[]{:S(2)}) collective-permute-start(bf16[512,512]{1,0:T(8,128)(2,1)S(1)} %get-tuple-element.53), channel_id=1, source_target_pairs={{0,2},{2,4},{4,6},{6,8},{8,10},{10,12},{12,14},{14,0},{1,3},{3,5},... | collective-permute-start | bytes 1572872 | tf_op jit(solution)/shard_map/ppermute | solution.py:201
  106.2 11.1 %collective-permute-start.12 = (bf16[512,512]{1,0:T(8,128)(2,1)S(1)}, bf16[512,512]{1,0:T(8,128)(2,1)S(1)}, u32[]{:S(2)}, u32[]{:S(2)}) collective-permute-start(bf16[512,512]{1,0:T(8,128)(2,1)S(1)} %get-tuple-element.54), channel_id=1, source_target_pairs={{0,14},{2,0},{4,2},{6,4},{8,6},{10,8},{12,10},{14,12},{1,15},{3,1}... | collective-permute-start | bytes 1572872 | tf_op jit(solution)/shard_map/ppermute | solution.py:201
  118.3 9.1 %copy-start.3 = (f32[256,2]{0,1:T(2,128)S(1)}, f32[256,2]{0,1:T(2,128)}, u32[]{:S(2)}) copy-start(f32[256,2]{0,1:T(2,128)} %param.10) | copy-start | bytes 6148
  118.3 23.8 %all-to-all-start.1 = ((bf16[64,8,512]{2,1,0:T(8,128)(2,1)}), bf16[64,8,512]{2,1,0:T(8,128)(2,1)S(1)}, u32[]{:S(2)}, u32[]{:S(2)}) async-start(bf16[64,8,512]{2,1,0:T(8,128)(2,1)} %bitcast.12), calls=%async_computation.1 | async-start | bytes 1048576 | tf_op jit(solution)/shard_map/all_to_all | solution.py:266
  143.2 10.1 %collective-permute-start.14 = (f32[256,128]{1,0:T(8,128)S(1)}, f32[256,128]{1,0:T(8,128)S(1)}, u32[]{:S(2)}, u32[]{:S(2)}) collective-permute-start(f32[256,128]{1,0:T(8,128)S(1)} %get-tuple-element.58), channel_id=1, source_target_pairs={{0,1},{1,0},{2,3},{3,2},{4,5},{5,4},{6,7},{7,6},{8,9},{9,8},{10,11... | collective-permute-start | bytes 393224 | tf_op jit(solution)/shard_map/ppermute | solution.py:204
  151.4 8.1 %collective-permute-start.13 = (f32[256,128]{1,0:T(8,128)S(1)}, f32[256,128]{1,0:T(8,128)S(1)}, u32[]{:S(2)}, u32[]{:S(2)}) collective-permute-start(f32[256,128]{1,0:T(8,128)S(1)} %get-tuple-element.56), channel_id=1, source_target_pairs={{0,1},{1,0},{2,3},{3,2},{4,5},{5,4},{6,7},{7,6},{8,9},{9,8},{10,11... | collective-permute-start | bytes 393224 | tf_op jit(solution)/shard_map/ppermute | solution.py:204
  153.3 10.1 %collective-permute-start.15 = (bf16[256,128]{1,0:T(8,128)(2,1)S(1)}, bf16[256,128]{1,0:T(8,128)(2,1)S(1)}, u32[]{:S(2)}, u32[]{:S(2)}) collective-permute-start(bf16[256,128]{1,0:T(8,128)(2,1)S(1)} %shard_map.83), channel_id=1, source_target_pairs={{0,8},{1,9},{2,10},{3,11},{4,12},{5,13},{6,14},{7,15},{8,0},{9,1},... | collective-permute-start | bytes 196616 | tf_op jit(solution)/shard_map/ppermute | solution.py:204

commit v5 on v4

--- a/solution.py
+++ b/solution.py
@@ -157,20 +157,19 @@
     ).astype(BF16)
 
 
-def mix_body(rows, share, high, low):
-    r_iota = lax.broadcasted_iota(jnp.int32, high.shape, 0)
-    weight = jnp.zeros(high.shape, F32)
+def mix_body(part, rows, share, out):
+    r_iota = lax.broadcasted_iota(jnp.int32, out.shape, 0)
+    weight = jnp.zeros(out.shape, F32)
     for k in range(2):
         weight = jnp.where(r_iota == rows[k : k + 1, :], share[k : k + 1, :], weight)
     top = weight.astype(BF16)
-    high[...] = top
-    low[...] = (weight - top.astype(F32)).astype(BF16)
-
-
-def combine_body(pos, high, low, back, near, near_away, far, far_away):
+    out[...] = top if part == 0 else (weight - top.astype(F32)).astype(BF16)
+
+
+def combine_body(pos, high, low, back, own, away):
     dims = (((0,), (0,)), ((), ()))
     first = pos[0] == 0
-    for s, (mine, other) in enumerate(((near, near_away), (far, far_away))):
+    for s in range(2):
         group = pos[1] if s == 0 else 1 - pos[1]
         x = back[:, pl.ds(pl.multiple_of(group * 256, 256), 256)]
         y = lax.dot_general(high[...], x, dims, preferred_element_type=F32) + lax.dot_general(
@@ -178,12 +177,13 @@
         )
         a = y[:, :128]
         b = y[:, 128:]
-        mine[...] = jnp.where(first, a, b)
-        other[...] = jnp.where(first, b, a)
-
-
-def fold_body(own, got, out):
-    out[...] = (own[...] + got[...]).astype(BF16)
+        own[s] = jnp.where(first, a, b)
+        away[s] = jnp.where(first, b, a)
+
+
+def fold_body(own, got, near, far):
+    far[...] = (own[1] + got[1]).astype(BF16)
+    near[...] = own[0] + got[0]
 
 
 def shards(tokens, norm_gain, expert_ids, gate_share, gate_weight, up_weight, down_weight):
@@ -224,18 +224,27 @@
         jnp.pad(tokens, ((0, PAD), (0, 0))),
         norm_gain[None, :],
     )
-    own = jnp.stack([mine, flip(mine, 8)])
+    far = flip(mine, 8)
+    wg2, wu2 = flip(wg, 1), flip(wu, 1)
+    own = jnp.stack([mine, far])
     other = flip(own, 1)
     buf, gain = call(
         dispatch_body, (shape(n, feats), shape(PAD, feats)), 3, True, 150_000_000, 4
     )(pos, place, own, other)
+
+    def mix(which):
+        return call(
+            functools.partial(mix_body, which), (shape(n, tok),), 2, False, 1_000_000, 4
+        )(rows, gate_share.T)
+
+    (high,) = mix(0)
     here = lax.all_to_all(
         buf.reshape(n_ep, half, feats), EP, split_axis=0, concat_axis=0, tiled=True
     ).reshape(n, feats)
     sent = jnp.concatenate([here, gain], axis=0)
     left = step(sent, 1)
     right = step(sent, -1)
-    wg2, wu2, wd2 = flip(wg, 1), flip(wu, 1), flip(wd, 1)
+    wd2 = flip(wd, 1)
     wide = shape(n, 2 * hid, dtype=F32)
     slim = shape(n, hid, dtype=F32)
     thin = shape(n, 128, dtype=F32)
@@ -266,17 +275,13 @@
     returned = lax.all_to_all(
         sums.reshape(n_ep, half, feats), EP, split_axis=0, concat_axis=0, tiled=True
     ).reshape(n, feats)
-    high, low = call(mix_body, (shape(n, tok), shape(n, tok)), 2, False, 1_000_000, 4)(
-        rows, gate_share.T
-    )
-    part = shape(tok, width, dtype=F32)
-    near, near_away, far, far_away = call(
-        combine_body, (part, part, part, part), 3, True, 300_000_000, 6
-    )(pos, high, low, returned)
-    (folded,) = call(fold_body, (shape(tok, width),), 2, False, 1_000_000, 2)(
-        far, flip(far_away, 1)
-    )
-    return (near + flip(near_away, 1) + flip(folded, 8).astype(F32)).astype(BF16)
+    (low,) = mix(1)
+    part = shape(2, tok, width, dtype=F32)
+    own, away = call(combine_body, (part, part), 3, True, 300_000_000, 6)(pos, high, low, returned)
+    near, far = call(
+        fold_body, (shape(tok, width, dtype=F32), shape(tok, width)), 2, False, 1_000_000, 2
+    )(own, flip(away, 1))
+    return (near + flip(far, 8).astype(F32)).astype(BF16)
 
 
 def solution(mesh):

time: 166 us -> 165 us (level)
  starting transfers between devices: 90.3 us -> 88.4 us
    ppermute x8 -> x7, starting transfers between devices: 32.3 us -> 30.4 us  [flip(): return lax.ppermute(x, TP, [(i, i ^ bits) for i in range(16)])]
    ppermute x8 -> x7, waiting for transfers between devices: 8.39 us -> 9.41 us  [flip(): return lax.ppermute(x, TP, [(i, i ^ bits) for i in range(16)])]
  transfers between devices with their start and end apart: 18 -> 17, of which waited for: 10 -> 11; matrix products, arithmetic and copies ran while one was open for 0% -> 0% of each run, Pallas kernels for 5% -> 5%
where the time goes in v5:
time: 165 us; the launch traced here: 163 us
  starting transfers between devices  88.4 us (54%)
  waiting for transfers between devices  57.5 us (35%)
  Pallas kernels  14.4 us (9%)
  other arithmetic  1.83 us (1%)
    ppermute x7, starting transfers between devices, flip(): return lax.ppermute(x, TP, [(i, i ^ bits) for i in range(16)])  30.4 us
    ppermute x8, starting transfers between devices, step(): return lax.ppermute(x, X, [(i, (i + s) % 8) for i in range(8)])  24.9 us
    all_to_all x1, starting transfers between devices, shards(): lax.all_to_all(buf.reshape(n_ep, half, feats), EP, split_axis=0, concat_a...  24 us
    ppermute x8, waiting for transfers between devices, step(): return lax.ppermute(x, X, [(i, (i + s) % 8) for i in range(8)])  22.2 us
    all_to_all x1, waiting for transfers between devices, shards(): lax.all_to_all(sums.reshape(n_ep, half, feats), EP, split_axis=0, concat_...  14.4 us
    all_to_all x1, waiting for transfers between devices, shards(): lax.all_to_all(buf.reshape(n_ep, half, feats), EP, split_axis=0, concat_a...  11.4 us
    ppermute x7, waiting for transfers between devices, flip(): return lax.ppermute(x, TP, [(i, i ^ bits) for i in range(16)])  9.41 us
    all_to_all x1, starting transfers between devices, shards(): lax.all_to_all(sums.reshape(n_ep, half, feats), EP, split_axis=0, concat_...  9.09 us
  transfers between devices with their start and end apart: 17, of which 11 were waited for; matrix products, arithmetic and copies ran while one was open for 0% of the time, Pallas kernels for 5%

profile of v5, /device:TPU:15, one launch (start us, length us, event | category | flops | bytes accessed | tf_op | source)
XLA Modules:
  0.0 163.1 jit_solution(4666672044994230349)
XLA Ops:
  0.0 0.0 copy-start.1
  0.0 1.0 fusion
  1.1 0.0 copy-start
  1.1 4.9 %collective-permute-start = (bf16[272,128]{1,0:T(8,128)(2,1)S(1)}, bf16[272,128]{1,0:T(8,128)(2,1)S(1)}, u32[]{:S(2)}, u32[]{:S(2)}) collective-permute-start(bf16[272,128]{1,0:T(8,128)(2,1)S(1)} %get-tuple-element.56), channel_id=1, source_target_pairs={{0,8},{1,9},{2,10},{3,11},{4,12},{5,13},{6,14},{7,15},{8,0},{9,1},... | collective-permute-start | bytes 208904 | tf_op jit(solution)/shard_map/ppermute | solution.py:204
  6.0 4.4 %collective-permute-done = bf16[272,128]{1,0:T(8,128)(2,1)S(1)} collective-permute-done((bf16[272,128]{1,0:T(8,128)(2,1)S(1)}, bf16[272,128]{1,0:T(8,128)(2,1)S(1)}, u32[]{:S(2)}, u32[]{:S(2)}) %collective-permute-start) | collective-permute-done | bytes 69664 | tf_op jit(solution)/shard_map/ppermute | solution.py:204
  10.4 4.7 %collective-permute-start.1 = (bf16[2,272,128]{2,1,0:T(8,128)(2,1)S(1)}, bf16[2,272,128]{2,1,0:T(8,128)(2,1)S(1)}, u32[]{:S(2)}, u32[]{:S(2)}) collective-permute-start(bf16[2,272,128]{2,1,0:T(8,128)(2,1)S(1)} %pad_maximum_fusion.1.own), channel_id=1, source_target_pairs={{0,1},{1,0},{2,3},{3,2},{4,5},{5,4},{6,7},{7,6},{8,9},{9,8},{10,11... | collective-permute-start | bytes 417800 | tf_op jit(solution)/shard_map/ppermute | solution.py:204
  15.1 0.1 pad_add_fusion.pos
  15.2 0.0 copy-start.4
  15.2 0.7 copy-done.4
  15.8 0.8 shard_map.73
  16.7 0.0 collective-permute-done.1.other
  16.7 1.7 %shard_map.76 = (bf16[512,512]{1,0:T(8,128)(2,1)}, bf16[16,512]{1,0:T(8,128)(2,1)S(1)}) custom-call(s32[3]{0:T(128)S(1)} %pad_add_fusion.pos, bf16[512,256]{1,0:T(8,128)(2,1)S(1)} %get-tuple-element.31.place, bf16[2,272,128]{2,1,0:T(8,128)(2,1)S(1)} %pad_maximum_fusion.1.own, bf16[2,272,128]{2,1,0:T(8,128)(2,1)S(1)} %collective-permute-done.1.other), custom_call_target="tpu_custom_call" | custom-call | flops 150000000 | bytes 4194304 | tf_op jit(solution)/shard_map/pallas_call | solution.py:231
  18.3 24.0 %all-to-all-start = ((bf16[64,8,512]{2,1,0:T(8,128)(2,1)}), bf16[64,8,512]{2,1,0:T(8,128)(2,1)S(1)}, u32[]{:S(2)}, u32[]{:S(2)}) async-start(bf16[64,8,512]{2,1,0:T(8,128)(2,1)} %bitcast.7), calls=%async_computation | async-start | bytes 1048576 | tf_op jit(solution)/shard_map/all_to_all | solution.py:241
  42.4 0.0 copy-done
  42.4 2.2 %collective-permute-start.6 = (bf16[2,4,256,256]{3,2,1,0:T(8,128)(2,1)S(1)}, bf16[2,4,256,256]{3,2,1,0:T(8,128)(2,1)}, u32[]{:S(2)}, u32[]{:S(2)}) collective-permute-start(bf16[2,4,256,256]{3,2,1,0:T(8,128)(2,1)S(1)} %bitcast.15), channel_id=1, source_target_pairs={{0,1},{1,0},{2,3},{3,2},{4,5},{5,4},{6,7},{7,6},{8,9},{9,8},{10,11... | collective-permute-start | bytes 3145736 | tf_op jit(solution)/shard_map/ppermute | solution.py:204
  44.6 0.0 copy-done.1
  44.6 2.1 %collective-permute-start.7 = (bf16[2,4,256,256]{3,2,1,0:T(8,128)(2,1)S(1)}, bf16[2,4,256,256]{3,2,1,0:T(8,128)(2,1)}, u32[]{:S(2)}, u32[]{:S(2)}) collective-permute-start(bf16[2,4,256,256]{3,2,1,0:T(8,128)(2,1)S(1)} %bitcast.19), channel_id=1, source_target_pairs={{0,1},{1,0},{2,3},{3,2},{4,5},{5,4},{6,7},{7,6},{8,9},{9,8},{10,11... | collective-permute-start | bytes 3145736 | tf_op jit(solution)/shard_map/ppermute | solution.py:204
  46.7 2.2 %collective-permute-start.8 = (bf16[256,2048]{1,0:T(8,128)(2,1)}, bf16[256,2048]{1,0:T(8,128)(2,1)}, u32[]{:S(2)}, u32[]{:S(2)}) collective-permute-start(bf16[256,2048]{1,0:T(8,128)(2,1)} %bitcast.26), channel_id=1, source_target_pairs={{0,1},{1,0},{2,3},{3,2},{4,5},{5,4},{6,7},{7,6},{8,9},{9,8},{10,11... | collective-permute-start | bytes 3145736 | tf_op jit(solution)/shard_map/ppermute | solution.py:204
  48.9 11.4 %all-to-all-done = bf16[64,8,512]{2,1,0:T(8,128)(2,1)S(1)} async-done(((bf16[64,8,512]{2,1,0:T(8,128)(2,1)}), bf16[64,8,512]{2,1,0:T(8,128)(2,1)S(1)}, u32[]{:S(2)}, u32[]{:S(2)}) %all-to-all-start) | async-done | bytes 524320 | tf_op jit(solution)/shard_map/all_to_all | solution.py:241
  60.4 1.9 %collective-permute-start.2 = (bf16[528,512]{1,0:T(8,128)(2,1)S(1)}, bf16[528,512]{1,0:T(8,128)(2,1)S(1)}, u32[]{:S(2)}, u32[]{:S(2)}) collective-permute-start(bf16[528,512]{1,0:T(8,128)(2,1)S(1)} %pad_maximum_fusion), channel_id=1, source_target_pairs={{0,2},{2,4},{4,6},{6,8},{8,10},{10,12},{12,14},{14,0},{1,3},{3,5},... | collective-permute-start | bytes 1622024 | tf_op jit(solution)/shard_map/ppermute | solution.py:201
  62.3 3.4 %collective-permute-start.3 = (bf16[528,512]{1,0:T(8,128)(2,1)S(1)}, bf16[528,512]{1,0:T(8,128)(2,1)S(1)}, u32[]{:S(2)}, u32[]{:S(2)}) collective-permute-start(bf16[528,512]{1,0:T(8,128)(2,1)S(1)} %pad_maximum_fusion), channel_id=1, source_target_pairs={{0,14},{2,0},{4,2},{6,4},{8,6},{10,8},{12,10},{14,12},{1,15},{3,1}... | collective-permute-start | bytes 1622024 | tf_op jit(solution)/shard_map/ppermute | solution.py:201
  65.7 1.0 shard_map.77
  66.7 8.0 %collective-permute-done.2.left = bf16[528,512]{1,0:T(8,128)(2,1)S(1)} collective-permute-done((bf16[528,512]{1,0:T(8,128)(2,1)S(1)}, bf16[528,512]{1,0:T(8,128)(2,1)S(1)}, u32[]{:S(2)}, u32[]{:S(2)}) %collective-permute-start.2) | collective-permute-done | bytes 540704 | tf_op jit(solution)/shard_map/ppermute | solution.py:201
  74.7 3.1 %collective-permute-done.3.right = bf16[528,512]{1,0:T(8,128)(2,1)S(1)} collective-permute-done((bf16[528,512]{1,0:T(8,128)(2,1)S(1)}, bf16[528,512]{1,0:T(8,128)(2,1)S(1)}, u32[]{:S(2)}, u32[]{:S(2)}) %collective-permute-start.3) | collective-permute-done | bytes 540704 | tf_op jit(solution)/shard_map/ppermute | solution.py:201
  77.9 1.9 %collective-permute-start.5 = (bf16[272,512]{1,0:T(8,128)(2,1)S(1)}, bf16[272,512]{1,0:T(8,128)(2,1)S(1)}, u32[]{:S(2)}, u32[]{:S(2)}) collective-permute-start(bf16[272,512]{1,0:T(8,128)(2,1)S(1)} %slice.7), channel_id=1, source_target_pairs={{0,14},{2,0},{4,2},{6,4},{8,6},{10,8},{12,10},{14,12},{1,15},{3,1}... | collective-permute-start | bytes 835592 | tf_op jit(solution)/shard_map/ppermute | solution.py:201
  79.8 4.6 %collective-permute-start.4 = (bf16[256,512]{1,0:T(8,128)(2,1)S(1)}, bf16[256,512]{1,0:T(8,128)(2,1)S(1)}, u32[]{:S(2)}, u32[]{:S(2)}) collective-permute-start(bf16[256,512]{1,0:T(8,128)(2,1)S(1)} %slice.6), channel_id=1, source_target_pairs={{0,2},{2,4},{4,6},{6,8},{8,10},{10,12},{12,14},{14,0},{1,3},{3,5},... | collective-permute-start | bytes 786440 | tf_op jit(solution)/shard_map/ppermute | solution.py:201
  84.4 0.0 collective-permute-done.6.wg2
  84.4 0.0 collective-permute-done.7.wu2
  84.4 0.0 copy-start.2
  84.4 3.2 %shard_map.78 = (f32[512,512]{1,0:T(8,128)S(1)}, f32[512,512]{1,0:T(8,128)S(1)}, f32[512,128]{1,0:T(8,128)S(1)}) custom-call(s32[3]{0:T(128)S(1)} %pad_add_fusion.pos, bf16[512,512]{1,0:T(8,128)(2,1)S(1)} %bitcast.25, bf16[16,512]{1,0:T(8,128)(2,1)S(1)} %get-tuple-element.33.gain.gain_m, bf16[528,512]{1,0:T(8,128)(2,1)S(1)} %collective-permute-done.2.left, ...), custom_call_target="tpu_custom_call" | custom-call | flops 1300000000 | bytes 4194304 | tf_op jit(solution)/shard_map/pallas_call | solution.py:257
  87.6 0.0 collective-permute-done.8.wd2
  87.6 0.1 collective-permute-done.4.left2
  87.7 0.0 collective-permute-done.5.right2
  87.7 0.0 copy-done.2
  87.7 3.1 %shard_map.79 = (bf16[256,512]{1,0:T(8,128)(2,1)S(1)}, bf16[256,512]{1,0:T(8,128)(2,1)S(1)}, bf16[512,512]{1,0:T(8,128)(2,1)S(1)}) custom-call(s32[3]{0:T(128)S(1)} %pad_add_fusion.pos, bf16[256,512]{1,0:T(8,128)(2,1)S(1)} %collective-permute-done.4.left2, bf16[272,512]{1,0:T(8,128)(2,1)S(1)} %collective-permute-done.5.right2, ...), custom_call_target="tpu_custom_call" | custom-call | flops 800000000 | bytes 4194304 | tf_op jit(solution)/shard_map/pallas_call | solution.py:260
  90.8 2.3 %collective-permute-start.10 = (bf16[256,512]{1,0:T(8,128)(2,1)S(1)}, bf16[256,512]{1,0:T(8,128)(2,1)S(1)}, u32[]{:S(2)}, u32[]{:S(2)}) collective-permute-start(bf16[256,512]{1,0:T(8,128)(2,1)S(1)} %get-tuple-element.48), channel_id=1, source_target_pairs={{0,14},{2,0},{4,2},{6,4},{8,6},{10,8},{12,10},{14,12},{1,15},{3,1}... | collective-permute-start | bytes 786440 | tf_op jit(solution)/shard_map/ppermute | solution.py:201
  93.1 4.6 %collective-permute-start.9 = (bf16[256,512]{1,0:T(8,128)(2,1)S(1)}, bf16[256,512]{1,0:T(8,128)(2,1)S(1)}, u32[]{:S(2)}, u32[]{:S(2)}) collective-permute-start(bf16[256,512]{1,0:T(8,128)(2,1)S(1)} %get-tuple-element.47), channel_id=1, source_target_pairs={{0,2},{2,4},{4,6},{6,8},{8,10},{10,12},{12,14},{14,0},{1,3},{3,5},... | collective-permute-start | bytes 786440 | tf_op jit(solution)/shard_map/ppermute | solution.py:201
  97.7 2.2 %shard_map.80 = (bf16[512,512]{1,0:T(8,128)(2,1)S(1)}, bf16[512,512]{1,0:T(8,128)(2,1)S(1)}, bf16[512,512]{1,0:T(8,128)(2,1)S(1)}) custom-call(s32[3]{0:T(128)S(1)} %pad_add_fusion.pos, bf16[512,512]{1,0:T(8,128)(2,1)S(1)} %get-tuple-element.43.hidden, bf16[256,2048]{1,0:T(8,128)(2,1)S(1)} %bitcast.28, bf16[256,2048]{1,0:T(8,128)(2,1)} %collective-permute-done.8.wd2), custom_call_target="tpu_custom_call" | custom-call | flops 800000000 | bytes 4194304 | tf_op jit(solution)/shard_map/pallas_call | solution.py:266
  100.0 0.0 collective-permute-done.10.got_b
  100.0 1.8 %collective-permute-done.9.got_a = bf16[256,512]{1,0:T(8,128)(2,1)S(1)} collective-permute-done((bf16[256,512]{1,0:T(8,128)(2,1)S(1)}, bf16[256,512]{1,0:T(8,128)(2,1)S(1)}, u32[]{:S(2)}, u32[]{:S(2)}) %collective-permute-start.9) | collective-permute-done | bytes 262176 | tf_op jit(solution)/shard_map/ppermute | solution.py:201
  101.8 0.2 shard_map.81
  101.9 4.3 %collective-permute-start.11 = (bf16[512,512]{1,0:T(8,128)(2,1)S(1)}, bf16[512,512]{1,0:T(8,128)(2,1)S(1)}, u32[]{:S(2)}, u32[]{:S(2)}) collective-permute-start(bf16[512,512]{1,0:T(8,128)(2,1)S(1)} %get-tuple-element.49), channel_id=1, source_target_pairs={{0,2},{2,4},{4,6},{6,8},{8,10},{10,12},{12,14},{14,0},{1,3},{3,5},... | collective-permute-start | bytes 1572872 | tf_op jit(solution)/shard_map/ppermute | solution.py:201
  106.2 1.9 %collective-permute-start.12 = (bf16[512,512]{1,0:T(8,128)(2,1)S(1)}, bf16[512,512]{1,0:T(8,128)(2,1)S(1)}, u32[]{:S(2)}, u32[]{:S(2)}) collective-permute-start(bf16[512,512]{1,0:T(8,128)(2,1)S(1)} %get-tuple-element.50), channel_id=1, source_target_pairs={{0,14},{2,0},{4,2},{6,4},{8,6},{10,8},{12,10},{14,12},{1,15},{3,1}... | collective-permute-start | bytes 1572872 | tf_op jit(solution)/shard_map/ppermute | solution.py:201
  108.2 5.2 %collective-permute-done.11.got_a = bf16[512,512]{1,0:T(8,128)(2,1)S(1)} collective-permute-done((bf16[512,512]{1,0:T(8,128)(2,1)S(1)}, bf16[512,512]{1,0:T(8,128)(2,1)S(1)}, u32[]{:S(2)}, u32[]{:S(2)}) %collective-permute-start.11) | collective-permute-done | bytes 524320 | tf_op jit(solution)/shard_map/ppermute | solution.py:201
  113.4 4.0 %collective-permute-done.12.got_b = bf16[512,512]{1,0:T(8,128)(2,1)S(1)} collective-permute-done((bf16[512,512]{1,0:T(8,128)(2,1)S(1)}, bf16[512,512]{1,0:T(8,128)(2,1)S(1)}, u32[]{:S(2)}, u32[]{:S(2)}) %collective-permute-start.12) | collective-permute-done | bytes 524320 | tf_op jit(solution)/shard_map/ppermute | solution.py:201
  117.4 1.0 shard_map.82
  118.3 0.0 copy-start.3
  118.3 9.1 %all-to-all-start.1 = ((bf16[64,8,512]{2,1,0:T(8,128)(2,1)}), bf16[64,8,512]{2,1,0:T(8,128)(2,1)S(1)}, u32[]{:S(2)}, u32[]{:S(2)}) async-start(bf16[64,8,512]{2,1,0:T(8,128)(2,1)} %bitcast.12), calls=%async_computation.1 | async-start | bytes 1048576 | tf_op jit(solution)/shard_map/all_to_all | solution.py:275
  127.4 0.0 copy-done.3
  127.5 0.1 shard_map.74.high
  127.6 0.1 shard_map.75.low
  127.7 14.4 %all-to-all-done.1 = bf16[64,8,512]{2,1,0:T(8,128)(2,1)S(1)} async-done(((bf16[64,8,512]{2,1,0:T(8,128)(2,1)}), bf16[64,8,512]{2,1,0:T(8,128)(2,1)S(1)}, u32[]{:S(2)}, u32[]{:S(2)}) %all-to-all-start.1) | async-done | bytes 524320 | tf_op jit(solution)/shard_map/all_to_all | solution.py:275
  142.1 1.0 shard_map.83
  143.2 8.2 %collective-permute-start.13 = (f32[2,256,128]{2,1,0:T(8,128)S(1)}, f32[2,256,128]{2,1,0:T(8,128)S(1)}, u32[]{:S(2)}, u32[]{:S(2)}) collective-permute-start(f32[2,256,128]{2,1,0:T(8,128)S(1)} %get-tuple-element.52), channel_id=1, source_target_pairs={{0,1},{1,0},{2,3},{3,2},{4,5},{5,4},{6,7},{7,6},{8,9},{9,8},{10,11... | collective-permute-start | bytes 786440 | tf_op jit(solution)/shard_map/ppermute | solution.py:204
  151.4 1.1 collective-permute-done.13.got
  152.5 6.1 %collective-permute-start.14 = (bf16[256,128]{1,0:T(8,128)(2,1)S(1)}, bf16[256,128]{1,0:T(8,128)(2,1)S(1)}, u32[]{:S(2)}, u32[]{:S(2)}) collective-permute-start(bf16[256,128]{1,0:T(8,128)(2,1)S(1)} %get-tuple-element.54), channel_id=1, source_target_pairs={{0,8},{1,9},{2,10},{3,11},{4,12},{5,13},{6,14},{7,15},{8,0},{9,1},... | collective-permute-start | bytes 196616 | tf_op jit(solution)/shard_map/ppermute | solution.py:204
  158.6 3.9 %collective-permute-done.14 = bf16[256,128]{1,0:T(8,128)(2,1)S(1)} collective-permute-done((bf16[256,128]{1,0:T(8,128)(2,1)S(1)}, bf16[256,128]{1,0:T(8,128)(2,1)S(1)}, u32[]{:S(2)}, u32[]{:S(2)}) %collective-permute-start.14) | collective-permute-done | bytes 65568 | tf_op jit(solution)/shard_map/ppermute | solution.py:204
  162.5 0.6 add_convert_fusion
  (6 shorter events, 0.1 us)
Async XLA Ops:
  0.0 44.6 %copy-start.1 = (bf16[1,2048,256]{2,1,0:T(8,128)(2,1)S(1)}, bf16[1,2048,256]{2,1,0:T(8,128)(2,1)}, u32[]{:S(2)}) copy-start(bf16[1,2048,256]{2,1,0:T(8,128)(2,1)} %param.12) | copy-start | bytes 3145732
  1.1 41.3 %copy-start = (bf16[1,2048,256]{2,1,0:T(8,128)(2,1)S(1)}, bf16[1,2048,256]{2,1,0:T(8,128)(2,1)}, u32[]{:S(2)}) copy-start(bf16[1,2048,256]{2,1,0:T(8,128)(2,1)} %param.11) | copy-start | bytes 3145732
  1.1 9.3 %collective-permute-start = (bf16[272,128]{1,0:T(8,128)(2,1)S(1)}, bf16[272,128]{1,0:T(8,128)(2,1)S(1)}, u32[]{:S(2)}, u32[]{:S(2)}) collective-permute-start(bf16[272,128]{1,0:T(8,128)(2,1)S(1)} %get-tuple-element.56), channel_id=1, source_target_pairs={{0,8},{1,9},{2,10},{3,11},{4,12},{5,13},{6,14},{7,15},{8,0},{9,1},... | collective-permute-start | bytes 208904 | tf_op jit(solution)/shard_map/ppermute | solution.py:204
  10.4 6.3 %collective-permute-start.1 = (bf16[2,272,128]{2,1,0:T(8,128)(2,1)S(1)}, bf16[2,272,128]{2,1,0:T(8,128)(2,1)S(1)}, u32[]{:S(2)}, u32[]{:S(2)}) collective-permute-start(bf16[2,272,128]{2,1,0:T(8,128)(2,1)S(1)} %pad_maximum_fusion.1.own), channel_id=1, source_target_pairs={{0,1},{1,0},{2,3},{3,2},{4,5},{5,4},{6,7},{7,6},{8,9},{9,8},{10,11... | collective-permute-start | bytes 417800 | tf_op jit(solution)/shard_map/ppermute | solution.py:204
  15.2 0.7 copy-start.4
  18.3 42.0 %all-to-all-start = ((bf16[64,8,512]{2,1,0:T(8,128)(2,1)}), bf16[64,8,512]{2,1,0:T(8,128)(2,1)S(1)}, u32[]{:S(2)}, u32[]{:S(2)}) async-start(bf16[64,8,512]{2,1,0:T(8,128)(2,1)} %bitcast.7), calls=%async_computation | async-start | bytes 1048576 | tf_op jit(solution)/shard_map/all_to_all | solution.py:241
  42.4 42.0 %collective-permute-start.6 = (bf16[2,4,256,256]{3,2,1,0:T(8,128)(2,1)S(1)}, bf16[2,4,256,256]{3,2,1,0:T(8,128)(2,1)}, u32[]{:S(2)}, u32[]{:S(2)}) collective-permute-start(bf16[2,4,256,256]{3,2,1,0:T(8,128)(2,1)S(1)} %bitcast.15), channel_id=1, source_target_pairs={{0,1},{1,0},{2,3},{3,2},{4,5},{5,4},{6,7},{7,6},{8,9},{9,8},{10,11... | collective-permute-start | bytes 3145736 | tf_op jit(solution)/shard_map/ppermute | solution.py:204
  44.6 39.8 %collective-permute-start.7 = (bf16[2,4,256,256]{3,2,1,0:T(8,128)(2,1)S(1)}, bf16[2,4,256,256]{3,2,1,0:T(8,128)(2,1)}, u32[]{:S(2)}, u32[]{:S(2)}) collective-permute-start(bf16[2,4,256,256]{3,2,1,0:T(8,128)(2,1)S(1)} %bitcast.19), channel_id=1, source_target_pairs={{0,1},{1,0},{2,3},{3,2},{4,5},{5,4},{6,7},{7,6},{8,9},{9,8},{10,11... | collective-permute-start | bytes 3145736 | tf_op jit(solution)/shard_map/ppermute | solution.py:204
  46.7 40.9 %collective-permute-start.8 = (bf16[256,2048]{1,0:T(8,128)(2,1)}, bf16[256,2048]{1,0:T(8,128)(2,1)}, u32[]{:S(2)}, u32[]{:S(2)}) collective-permute-start(bf16[256,2048]{1,0:T(8,128)(2,1)} %bitcast.26), channel_id=1, source_target_pairs={{0,1},{1,0},{2,3},{3,2},{4,5},{5,4},{6,7},{7,6},{8,9},{9,8},{10,11... | collective-permute-start | bytes 3145736 | tf_op jit(solution)/shard_map/ppermute | solution.py:204
  60.4 14.3 %collective-permute-start.2 = (bf16[528,512]{1,0:T(8,128)(2,1)S(1)}, bf16[528,512]{1,0:T(8,128)(2,1)S(1)}, u32[]{:S(2)}, u32[]{:S(2)}) collective-permute-start(bf16[528,512]{1,0:T(8,128)(2,1)S(1)} %pad_maximum_fusion), channel_id=1, source_target_pairs={{0,2},{2,4},{4,6},{6,8},{8,10},{10,12},{12,14},{14,0},{1,3},{3,5},... | collective-permute-start | bytes 1622024 | tf_op jit(solution)/shard_map/ppermute | solution.py:201
  62.3 15.5 %collective-permute-start.3 = (bf16[528,512]{1,0:T(8,128)(2,1)S(1)}, bf16[528,512]{1,0:T(8,128)(2,1)S(1)}, u32[]{:S(2)}, u32[]{:S(2)}) collective-permute-start(bf16[528,512]{1,0:T(8,128)(2,1)S(1)} %pad_maximum_fusion), channel_id=1, source_target_pairs={{0,14},{2,0},{4,2},{6,4},{8,6},{10,8},{12,10},{14,12},{1,15},{3,1}... | collective-permute-start | bytes 1622024 | tf_op jit(solution)/shard_map/ppermute | solution.py:201
  77.9 9.8 %collective-permute-start.5 = (bf16[272,512]{1,0:T(8,128)(2,1)S(1)}, bf16[272,512]{1,0:T(8,128)(2,1)S(1)}, u32[]{:S(2)}, u32[]{:S(2)}) collective-permute-start(bf16[272,512]{1,0:T(8,128)(2,1)S(1)} %slice.7), channel_id=1, source_target_pairs={{0,14},{2,0},{4,2},{6,4},{8,6},{10,8},{12,10},{14,12},{1,15},{3,1}... | collective-permute-start | bytes 835592 | tf_op jit(solution)/shard_map/ppermute | solution.py:201
  79.8 7.9 %collective-permute-start.4 = (bf16[256,512]{1,0:T(8,128)(2,1)S(1)}, bf16[256,512]{1,0:T(8,128)(2,1)S(1)}, u32[]{:S(2)}, u32[]{:S(2)}) collective-permute-start(bf16[256,512]{1,0:T(8,128)(2,1)S(1)} %slice.6), channel_id=1, source_target_pairs={{0,2},{2,4},{4,6},{6,8},{8,10},{10,12},{12,14},{14,0},{1,3},{3,5},... | collective-permute-start | bytes 786440 | tf_op jit(solution)/shard_map/ppermute | solution.py:201
  84.4 3.3 %copy-start.2 = (bf16[1,256,2048]{2,1,0:T(8,128)(2,1)S(1)}, bf16[1,256,2048]{2,1,0:T(8,128)(2,1)}, u32[]{:S(2)}) copy-start(bf16[1,256,2048]{2,1,0:T(8,128)(2,1)} %param.13) | copy-start | bytes 3145732
  90.8 9.2 %collective-permute-start.10 = (bf16[256,512]{1,0:T(8,128)(2,1)S(1)}, bf16[256,512]{1,0:T(8,128)(2,1)S(1)}, u32[]{:S(2)}, u32[]{:S(2)}) collective-permute-start(bf16[256,512]{1,0:T(8,128)(2,1)S(1)} %get-tuple-element.48), channel_id=1, source_target_pairs={{0,14},{2,0},{4,2},{6,4},{8,6},{10,8},{12,10},{14,12},{1,15},{3,1}... | collective-permute-start | bytes 786440 | tf_op jit(solution)/shard_map/ppermute | solution.py:201
  93.1 8.7 %collective-permute-start.9 = (bf16[256,512]{1,0:T(8,128)(2,1)S(1)}, bf16[256,512]{1,0:T(8,128)(2,1)S(1)}, u32[]{:S(2)}, u32[]{:S(2)}) collective-permute-start(bf16[256,512]{1,0:T(8,128)(2,1)S(1)} %get-tuple-element.47), channel_id=1, source_target_pairs={{0,2},{2,4},{4,6},{6,8},{8,10},{10,12},{12,14},{14,0},{1,3},{3,5},... | collective-permute-start | bytes 786440 | tf_op jit(solution)/shard_map/ppermute | solution.py:201
  101.9 11.4 %collective-permute-start.11 = (bf16[512,512]{1,0:T(8,128)(2,1)S(1)}, bf16[512,512]{1,0:T(8,128)(2,1)S(1)}, u32[]{:S(2)}, u32[]{:S(2)}) collective-permute-start(bf16[512,512]{1,0:T(8,128)(2,1)S(1)} %get-tuple-element.49), channel_id=1, source_target_pairs={{0,2},{2,4},{4,6},{6,8},{8,10},{10,12},{12,14},{14,0},{1,3},{3,5},... | collective-permute-start | bytes 1572872 | tf_op jit(solution)/shard_map/ppermute | solution.py:201
  106.2 11.1 %collective-permute-start.12 = (bf16[512,512]{1,0:T(8,128)(2,1)S(1)}, bf16[512,512]{1,0:T(8,128)(2,1)S(1)}, u32[]{:S(2)}, u32[]{:S(2)}) collective-permute-start(bf16[512,512]{1,0:T(8,128)(2,1)S(1)} %get-tuple-element.50), channel_id=1, source_target_pairs={{0,14},{2,0},{4,2},{6,4},{8,6},{10,8},{12,10},{14,12},{1,15},{3,1}... | collective-permute-start | bytes 1572872 | tf_op jit(solution)/shard_map/ppermute | solution.py:201
  118.3 9.1 %copy-start.3 = (f32[256,2]{0,1:T(2,128)S(1)}, f32[256,2]{0,1:T(2,128)}, u32[]{:S(2)}) copy-start(f32[256,2]{0,1:T(2,128)} %param.10) | copy-start | bytes 6148
  118.3 23.8 %all-to-all-start.1 = ((bf16[64,8,512]{2,1,0:T(8,128)(2,1)}), bf16[64,8,512]{2,1,0:T(8,128)(2,1)S(1)}, u32[]{:S(2)}, u32[]{:S(2)}) async-start(bf16[64,8,512]{2,1,0:T(8,128)(2,1)} %bitcast.12), calls=%async_computation.1 | async-start | bytes 1048576 | tf_op jit(solution)/shard_map/all_to_all | solution.py:275
  143.2 9.3 %collective-permute-start.13 = (f32[2,256,128]{2,1,0:T(8,128)S(1)}, f32[2,256,128]{2,1,0:T(8,128)S(1)}, u32[]{:S(2)}, u32[]{:S(2)}) collective-permute-start(f32[2,256,128]{2,1,0:T(8,128)S(1)} %get-tuple-element.52), channel_id=1, source_target_pairs={{0,1},{1,0},{2,3},{3,2},{4,5},{5,4},{6,7},{7,6},{8,9},{9,8},{10,11... | collective-permute-start | bytes 786440 | tf_op jit(solution)/shard_map/ppermute | solution.py:204
  152.5 10.0 %collective-permute-start.14 = (bf16[256,128]{1,0:T(8,128)(2,1)S(1)}, bf16[256,128]{1,0:T(8,128)(2,1)S(1)}, u32[]{:S(2)}, u32[]{:S(2)}) collective-permute-start(bf16[256,128]{1,0:T(8,128)(2,1)S(1)} %get-tuple-element.54), channel_id=1, source_target_pairs={{0,8},{1,9},{2,10},{3,11},{4,12},{5,13},{6,14},{7,15},{8,0},{9,1},... | collective-permute-start | bytes 196616 | tf_op jit(solution)/shard_map/ppermute | solution.py:204

commit v6 on v5

--- a/solution.py
+++ b/solution.py
@@ -157,13 +157,14 @@
     ).astype(BF16)
 
 
-def mix_body(part, rows, share, out):
-    r_iota = lax.broadcasted_iota(jnp.int32, out.shape, 0)
-    weight = jnp.zeros(out.shape, F32)
+def mix_body(rows, share, high, low):
+    r_iota = lax.broadcasted_iota(jnp.int32, high.shape, 0)
+    weight = jnp.zeros(high.shape, F32)
     for k in range(2):
         weight = jnp.where(r_iota == rows[k : k + 1, :], share[k : k + 1, :], weight)
     top = weight.astype(BF16)
-    out[...] = top if part == 0 else (weight - top.astype(F32)).astype(BF16)
+    high[...] = top
+    low[...] = (weight - top.astype(F32)).astype(BF16)
 
 
 def combine_body(pos, high, low, back, own, away):
@@ -224,36 +225,26 @@
         jnp.pad(tokens, ((0, PAD), (0, 0))),
         norm_gain[None, :],
     )
-    far = flip(mine, 8)
-    wg2, wu2 = flip(wg, 1), flip(wu, 1)
-    own = jnp.stack([mine, far])
+    own = jnp.stack([mine, flip(mine, 8)])
     other = flip(own, 1)
     buf, gain = call(
         dispatch_body, (shape(n, feats), shape(PAD, feats)), 3, True, 150_000_000, 4
     )(pos, place, own, other)
-
-    def mix(which):
-        return call(
-            functools.partial(mix_body, which), (shape(n, tok),), 2, False, 1_000_000, 4
-        )(rows, gate_share.T)
-
-    (high,) = mix(0)
     here = lax.all_to_all(
         buf.reshape(n_ep, half, feats), EP, split_axis=0, concat_axis=0, tiled=True
     ).reshape(n, feats)
     sent = jnp.concatenate([here, gain], axis=0)
     left = step(sent, 1)
     right = step(sent, -1)
-    wd2 = flip(wd, 1)
+    left2 = step(sent[:h], 2)
+    right2 = step(sent[h:], -2)
+    wg2, wu2, wd2 = flip(wg, 1), flip(wu, 1), flip(wd, 1)
     wide = shape(n, 2 * hid, dtype=F32)
     slim = shape(n, hid, dtype=F32)
     thin = shape(n, 128, dtype=F32)
     gate, up, squares = call(near_body, (slim, slim, thin), 4, True, 300_000_000, 6)(
         pos, here, gain, wg, wu
     )
-    left, right, gate = lax.optimization_barrier((left, right, gate))
-    left2 = step(left[:h], 1)
-    right2 = step(right[h:], -1)
     gate, up, squares = call(
         middle_body, (wide, wide, thin), 11, True, 1_300_000_000, 10
     )(pos, here, gain, left, right, gate, up, squares, wg, wu, wg2, wu2)
@@ -275,7 +266,9 @@
     returned = lax.all_to_all(
         sums.reshape(n_ep, half, feats), EP, split_axis=0, concat_axis=0, tiled=True
     ).reshape(n, feats)
-    (low,) = mix(1)
+    high, low = call(mix_body, (shape(n, tok), shape(n, tok)), 2, False, 1_000_000, 4)(
+        rows, gate_share.T
+    )
     part = shape(2, tok, width, dtype=F32)
     own, away = call(combine_body, (part, part), 3, True, 300_000_000, 6)(pos, high, low, returned)
     near, far = call(

time: 165 us -> 167 us (1.012)
  waiting for transfers between devices: 57.5 us -> 61.5 us
    ppermute x7, waiting for transfers between devices: 9.41 us -> 12.2 us  [flip(): return lax.ppermute(x, TP, [(i, i ^ bits) for i in range(16)])]
    ppermute x7, starting transfers between devices: 30.4 us -> 28.3 us  [flip(): return lax.ppermute(x, TP, [(i, i ^ bits) for i in range(16)])]
  transfers between devices with their start and end apart: 17 -> 17, of which waited for: 11 -> 11; matrix products, arithmetic and copies ran while one was open for 0% -> 0% of each run, Pallas kernels for 5% -> 4%
where the time goes in v6:
time: 167 us; the launch traced here: 166 us
  starting transfers between devices  87.1 us (52%)
  waiting for transfers between devices  61.5 us (37%)
  Pallas kernels  14.3 us (9%)
  other arithmetic  1.85 us (1%)
    ppermute x7, starting transfers between devices, flip(): return lax.ppermute(x, TP, [(i, i ^ bits) for i in range(16)])  28.3 us
    ppermute x8, starting transfers between devices, step(): return lax.ppermute(x, X, [(i, (i + s) % 8) for i in range(8)])  26.3 us
    all_to_all x1, starting transfers between devices, shards(): lax.all_to_all(buf.reshape(n_ep, half, feats), EP, split_axis=0, concat_a...  24 us
    ppermute x8, waiting for transfers between devices, step(): return lax.ppermute(x, X, [(i, (i + s) % 8) for i in range(8)])  23.4 us
    all_to_all x1, waiting for transfers between devices, shards(): lax.all_to_all(sums.reshape(n_ep, half, feats), EP, split_axis=0, concat_...  14.6 us
    ppermute x7, waiting for transfers between devices, flip(): return lax.ppermute(x, TP, [(i, i ^ bits) for i in range(16)])  12.2 us
    all_to_all x1, waiting for transfers between devices, shards(): lax.all_to_all(buf.reshape(n_ep, half, feats), EP, split_axis=0, concat_a...  11.4 us
    all_to_all x1, starting transfers between devices, shards(): lax.all_to_all(sums.reshape(n_ep, half, feats), EP, split_axis=0, concat_...  8.45 us
  transfers between devices with their start and end apart: 17, of which 11 were waited for; matrix products, arithmetic and copies ran while one was open for 0% of the time, Pallas kernels for 4%

profile of v6, /device:TPU:15, one launch (start us, length us, event | category | flops | bytes accessed | tf_op | source)
XLA Modules:
  0.0 165.8 jit_solution(12091085612391541326)
XLA Ops:
  0.0 0.0 copy-start.1
  0.0 1.0 fusion.1
  1.1 0.0 copy-start
  1.1 4.9 %collective-permute-start = (bf16[272,128]{1,0:T(8,128)(2,1)S(1)}, bf16[272,128]{1,0:T(8,128)(2,1)S(1)}, u32[]{:S(2)}, u32[]{:S(2)}) collective-permute-start(bf16[272,128]{1,0:T(8,128)(2,1)S(1)} %get-tuple-element.54), channel_id=1, source_target_pairs={{0,8},{1,9},{2,10},{3,11},{4,12},{5,13},{6,14},{7,15},{8,0},{9,1},... | collective-permute-start | bytes 208904 | tf_op jit(solution)/shard_map/ppermute | solution.py:205
  6.0 4.4 %collective-permute-done = bf16[272,128]{1,0:T(8,128)(2,1)S(1)} collective-permute-done((bf16[272,128]{1,0:T(8,128)(2,1)S(1)}, bf16[272,128]{1,0:T(8,128)(2,1)S(1)}, u32[]{:S(2)}, u32[]{:S(2)}) %collective-permute-start) | collective-permute-done | bytes 69664 | tf_op jit(solution)/shard_map/ppermute | solution.py:205
  10.4 4.7 %collective-permute-start.1 = (bf16[2,272,128]{2,1,0:T(8,128)(2,1)S(1)}, bf16[2,272,128]{2,1,0:T(8,128)(2,1)S(1)}, u32[]{:S(2)}, u32[]{:S(2)}) collective-permute-start(bf16[2,272,128]{2,1,0:T(8,128)(2,1)S(1)} %pad_maximum_fusion.1.own), channel_id=1, source_target_pairs={{0,1},{1,0},{2,3},{3,2},{4,5},{5,4},{6,7},{7,6},{8,9},{9,8},{10,11... | collective-permute-start | bytes 417800 | tf_op jit(solution)/shard_map/ppermute | solution.py:205
  15.1 0.1 pad_add_fusion.pos
  15.2 0.0 copy-start.4
  15.2 0.7 copy-done.4
  15.8 0.8 shard_map.73
  16.7 0.0 collective-permute-done.1.other
  16.7 1.7 %shard_map.75 = (bf16[512,512]{1,0:T(8,128)(2,1)}, bf16[16,512]{1,0:T(8,128)(2,1)S(1)}) custom-call(s32[3]{0:T(128)S(1)} %pad_add_fusion.pos, bf16[512,256]{1,0:T(8,128)(2,1)S(1)} %get-tuple-element.32.place, bf16[2,272,128]{2,1,0:T(8,128)(2,1)S(1)} %pad_maximum_fusion.1.own, bf16[2,272,128]{2,1,0:T(8,128)(2,1)S(1)} %collective-permute-done.1.other), custom_call_target="tpu_custom_call" | custom-call | flops 150000000 | bytes 4194304 | tf_op jit(solution)/shard_map/pallas_call | solution.py:230
  18.3 24.0 %all-to-all-start = ((bf16[64,8,512]{2,1,0:T(8,128)(2,1)}), bf16[64,8,512]{2,1,0:T(8,128)(2,1)S(1)}, u32[]{:S(2)}, u32[]{:S(2)}) async-start(bf16[64,8,512]{2,1,0:T(8,128)(2,1)} %bitcast.7), calls=%async_computation | async-start | bytes 1048576 | tf_op jit(solution)/shard_map/all_to_all | solution.py:233
  42.4 0.0 copy-done
  42.4 2.2 %collective-permute-start.6 = (bf16[2,4,256,256]{3,2,1,0:T(8,128)(2,1)S(1)}, bf16[2,4,256,256]{3,2,1,0:T(8,128)(2,1)}, u32[]{:S(2)}, u32[]{:S(2)}) collective-permute-start(bf16[2,4,256,256]{3,2,1,0:T(8,128)(2,1)S(1)} %bitcast.21), channel_id=1, source_target_pairs={{0,1},{1,0},{2,3},{3,2},{4,5},{5,4},{6,7},{7,6},{8,9},{9,8},{10,11... | collective-permute-start | bytes 3145736 | tf_op jit(solution)/shard_map/ppermute | solution.py:205
  44.6 0.0 copy-done.1
  44.6 2.1 %collective-permute-start.7 = (bf16[2,4,256,256]{3,2,1,0:T(8,128)(2,1)S(1)}, bf16[2,4,256,256]{3,2,1,0:T(8,128)(2,1)}, u32[]{:S(2)}, u32[]{:S(2)}) collective-permute-start(bf16[2,4,256,256]{3,2,1,0:T(8,128)(2,1)S(1)} %bitcast.25), channel_id=1, source_target_pairs={{0,1},{1,0},{2,3},{3,2},{4,5},{5,4},{6,7},{7,6},{8,9},{9,8},{10,11... | collective-permute-start | bytes 3145736 | tf_op jit(solution)/shard_map/ppermute | solution.py:205
  46.7 2.2 %collective-permute-start.8 = (bf16[256,2048]{1,0:T(8,128)(2,1)}, bf16[256,2048]{1,0:T(8,128)(2,1)}, u32[]{:S(2)}, u32[]{:S(2)}) collective-permute-start(bf16[256,2048]{1,0:T(8,128)(2,1)} %bitcast.29), channel_id=1, source_target_pairs={{0,1},{1,0},{2,3},{3,2},{4,5},{5,4},{6,7},{7,6},{8,9},{9,8},{10,11... | collective-permute-start | bytes 3145736 | tf_op jit(solution)/shard_map/ppermute | solution.py:205
  48.9 11.4 %all-to-all-done = bf16[64,8,512]{2,1,0:T(8,128)(2,1)S(1)} async-done(((bf16[64,8,512]{2,1,0:T(8,128)(2,1)}), bf16[64,8,512]{2,1,0:T(8,128)(2,1)S(1)}, u32[]{:S(2)}, u32[]{:S(2)}) %all-to-all-start) | async-done | bytes 524320 | tf_op jit(solution)/shard_map/all_to_all | solution.py:233
  60.4 1.9 %collective-permute-start.4 = (bf16[528,512]{1,0:T(8,128)(2,1)S(1)}, bf16[528,512]{1,0:T(8,128)(2,1)S(1)}, u32[]{:S(2)}, u32[]{:S(2)}) collective-permute-start(bf16[528,512]{1,0:T(8,128)(2,1)S(1)} %pad_maximum_fusion), channel_id=1, source_target_pairs={{0,2},{2,4},{4,6},{6,8},{8,10},{10,12},{12,14},{14,0},{1,3},{3,5},... | collective-permute-start | bytes 1622024 | tf_op jit(solution)/shard_map/ppermute | solution.py:202
  62.3 3.4 %collective-permute-start.5 = (bf16[528,512]{1,0:T(8,128)(2,1)S(1)}, bf16[528,512]{1,0:T(8,128)(2,1)S(1)}, u32[]{:S(2)}, u32[]{:S(2)}) collective-permute-start(bf16[528,512]{1,0:T(8,128)(2,1)S(1)} %pad_maximum_fusion), channel_id=1, source_target_pairs={{0,14},{2,0},{4,2},{6,4},{8,6},{10,8},{12,10},{14,12},{1,15},{3,1}... | collective-permute-start | bytes 1622024 | tf_op jit(solution)/shard_map/ppermute | solution.py:202
  65.7 0.0 collective-permute-done.6.wg2
  65.7 3.1 %collective-permute-start.3 = (bf16[272,512]{1,0:T(8,128)(2,1)S(1)}, bf16[272,512]{1,0:T(8,128)(2,1)S(1)}, u32[]{:S(2)}, u32[]{:S(2)}) collective-permute-start(bf16[272,512]{1,0:T(8,128)(2,1)S(1)} %fusion), channel_id=1, source_target_pairs={{0,12},{2,14},{4,0},{6,2},{8,4},{10,6},{12,8},{14,10},{1,13},{3,15... | collective-permute-start | bytes 835592 | tf_op jit(solution)/shard_map/ppermute | solution.py:202
  68.9 0.0 collective-permute-done.7.wu2
  68.9 4.3 %collective-permute-start.2 = (bf16[256,512]{1,0:T(8,128)(2,1)S(1)}, bf16[256,512]{1,0:T(8,128)(2,1)S(1)}, u32[]{:S(2)}, u32[]{:S(2)}) collective-permute-start(bf16[256,512]{1,0:T(8,128)(2,1)S(1)} %slice_bitcast_fusion), channel_id=1, source_target_pairs={{0,4},{2,6},{4,8},{6,10},{8,12},{10,14},{12,0},{14,2},{1,5},{3,7},... | collective-permute-start | bytes 786440 | tf_op jit(solution)/shard_map/ppermute | solution.py:202
  73.2 1.0 shard_map.76
  74.2 0.5 collective-permute-done.4.left
  74.7 3.9 %collective-permute-done.5.right = bf16[528,512]{1,0:T(8,128)(2,1)S(1)} collective-permute-done((bf16[528,512]{1,0:T(8,128)(2,1)S(1)}, bf16[528,512]{1,0:T(8,128)(2,1)S(1)}, u32[]{:S(2)}, u32[]{:S(2)}) %collective-permute-start.5) | collective-permute-done | bytes 540704 | tf_op jit(solution)/shard_map/ppermute | solution.py:202
  78.6 0.0 copy-start.2
  78.6 3.2 %shard_map.77 = (f32[512,512]{1,0:T(8,128)S(1)}, f32[512,512]{1,0:T(8,128)S(1)}, f32[512,128]{1,0:T(8,128)S(1)}) custom-call(s32[3]{0:T(128)S(1)} %pad_add_fusion.pos, bf16[512,512]{1,0:T(8,128)(2,1)S(1)} %bitcast.20, bf16[16,512]{1,0:T(8,128)(2,1)S(1)} %get-tuple-element.34.gain.gain_m, bf16[528,512]{1,0:T(8,128)(2,1)S(1)} %collective-permute-done.4.left, ...), custom_call_target="tpu_custom_call" | custom-call | flops 1300000000 | bytes 4194304 | tf_op jit(solution)/shard_map/pallas_call | solution.py:248
  81.8 0.0 collective-permute-done.8.wd2
  81.8 4.8 %collective-permute-done.2.left2 = bf16[256,512]{1,0:T(8,128)(2,1)S(1)} collective-permute-done((bf16[256,512]{1,0:T(8,128)(2,1)S(1)}, bf16[256,512]{1,0:T(8,128)(2,1)S(1)}, u32[]{:S(2)}, u32[]{:S(2)}) %collective-permute-start.2) | collective-permute-done | bytes 262176 | tf_op jit(solution)/shard_map/ppermute | solution.py:202
  86.6 0.0 collective-permute-done.3.right2
  86.6 0.0 copy-done.2
  86.6 3.0 %shard_map.78 = (bf16[256,512]{1,0:T(8,128)(2,1)S(1)}, bf16[256,512]{1,0:T(8,128)(2,1)S(1)}, bf16[512,512]{1,0:T(8,128)(2,1)S(1)}) custom-call(s32[3]{0:T(128)S(1)} %pad_add_fusion.pos, bf16[256,512]{1,0:T(8,128)(2,1)S(1)} %collective-permute-done.2.left2, bf16[272,512]{1,0:T(8,128)(2,1)S(1)} %collective-permute-done.3.right2, ...), custom_call_target="tpu_custom_call" | custom-call | flops 800000000 | bytes 4194304 | tf_op jit(solution)/shard_map/pallas_call | solution.py:251
  89.6 6.3 %collective-permute-start.10 = (bf16[256,512]{1,0:T(8,128)(2,1)S(1)}, bf16[256,512]{1,0:T(8,128)(2,1)S(1)}, u32[]{:S(2)}, u32[]{:S(2)}) collective-permute-start(bf16[256,512]{1,0:T(8,128)(2,1)S(1)} %get-tuple-element.46), channel_id=1, source_target_pairs={{0,14},{2,0},{4,2},{6,4},{8,6},{10,8},{12,10},{14,12},{1,15},{3,1}... | collective-permute-start | bytes 786440 | tf_op jit(solution)/shard_map/ppermute | solution.py:202
  95.9 1.9 %collective-permute-start.9 = (bf16[256,512]{1,0:T(8,128)(2,1)S(1)}, bf16[256,512]{1,0:T(8,128)(2,1)S(1)}, u32[]{:S(2)}, u32[]{:S(2)}) collective-permute-start(bf16[256,512]{1,0:T(8,128)(2,1)S(1)} %get-tuple-element.45), channel_id=1, source_target_pairs={{0,2},{2,4},{4,6},{6,8},{8,10},{10,12},{12,14},{14,0},{1,3},{3,5},... | collective-permute-start | bytes 786440 | tf_op jit(solution)/shard_map/ppermute | solution.py:202
  97.8 2.2 %shard_map.79 = (bf16[512,512]{1,0:T(8,128)(2,1)S(1)}, bf16[512,512]{1,0:T(8,128)(2,1)S(1)}, bf16[512,512]{1,0:T(8,128)(2,1)S(1)}) custom-call(s32[3]{0:T(128)S(1)} %pad_add_fusion.pos, bf16[512,512]{1,0:T(8,128)(2,1)S(1)} %get-tuple-element.41.hidden, bf16[256,2048]{1,0:T(8,128)(2,1)S(1)} %bitcast.31, bf16[256,2048]{1,0:T(8,128)(2,1)} %collective-permute-done.8.wd2), custom_call_target="tpu_custom_call" | custom-call | flops 800000000 | bytes 4194304 | tf_op jit(solution)/shard_map/pallas_call | solution.py:257
  100.1 0.0 collective-permute-done.10.got_b
  100.1 2.9 %collective-permute-done.9.got_a = bf16[256,512]{1,0:T(8,128)(2,1)S(1)} collective-permute-done((bf16[256,512]{1,0:T(8,128)(2,1)S(1)}, bf16[256,512]{1,0:T(8,128)(2,1)S(1)}, u32[]{:S(2)}, u32[]{:S(2)}) %collective-permute-start.9) | collective-permute-done | bytes 262176 | tf_op jit(solution)/shard_map/ppermute | solution.py:202
  103.0 0.2 shard_map.80
  103.2 3.5 %collective-permute-start.11 = (bf16[512,512]{1,0:T(8,128)(2,1)S(1)}, bf16[512,512]{1,0:T(8,128)(2,1)S(1)}, u32[]{:S(2)}, u32[]{:S(2)}) collective-permute-start(bf16[512,512]{1,0:T(8,128)(2,1)S(1)} %get-tuple-element.47), channel_id=1, source_target_pairs={{0,2},{2,4},{4,6},{6,8},{8,10},{10,12},{12,14},{14,0},{1,3},{3,5},... | collective-permute-start | bytes 1572872 | tf_op jit(solution)/shard_map/ppermute | solution.py:202
  106.7 1.9 %collective-permute-start.12 = (bf16[512,512]{1,0:T(8,128)(2,1)S(1)}, bf16[512,512]{1,0:T(8,128)(2,1)S(1)}, u32[]{:S(2)}, u32[]{:S(2)}) collective-permute-start(bf16[512,512]{1,0:T(8,128)(2,1)S(1)} %get-tuple-element.48), channel_id=1, source_target_pairs={{0,14},{2,0},{4,2},{6,4},{8,6},{10,8},{12,10},{14,12},{1,15},{3,1}... | collective-permute-start | bytes 1572872 | tf_op jit(solution)/shard_map/ppermute | solution.py:202
  108.6 6.2 %collective-permute-done.11.got_a = bf16[512,512]{1,0:T(8,128)(2,1)S(1)} collective-permute-done((bf16[512,512]{1,0:T(8,128)(2,1)S(1)}, bf16[512,512]{1,0:T(8,128)(2,1)S(1)}, u32[]{:S(2)}, u32[]{:S(2)}) %collective-permute-start.11) | collective-permute-done | bytes 524320 | tf_op jit(solution)/shard_map/ppermute | solution.py:202
  114.8 5.0 %collective-permute-done.12.got_b = bf16[512,512]{1,0:T(8,128)(2,1)S(1)} collective-permute-done((bf16[512,512]{1,0:T(8,128)(2,1)S(1)}, bf16[512,512]{1,0:T(8,128)(2,1)S(1)}, u32[]{:S(2)}, u32[]{:S(2)}) %collective-permute-start.12) | collective-permute-done | bytes 524320 | tf_op jit(solution)/shard_map/ppermute | solution.py:202
  119.8 1.0 shard_map.81
  120.8 0.0 copy-start.3
  120.8 8.5 %all-to-all-start.1 = ((bf16[64,8,512]{2,1,0:T(8,128)(2,1)}), bf16[64,8,512]{2,1,0:T(8,128)(2,1)S(1)}, u32[]{:S(2)}, u32[]{:S(2)}) async-start(bf16[64,8,512]{2,1,0:T(8,128)(2,1)} %bitcast.13), calls=%async_computation.1 | async-start | bytes 1048576 | tf_op jit(solution)/shard_map/all_to_all | solution.py:266
  129.3 0.0 copy-done.3
  129.3 0.1 shard_map.74
  129.4 14.6 %all-to-all-done.1 = bf16[64,8,512]{2,1,0:T(8,128)(2,1)S(1)} async-done(((bf16[64,8,512]{2,1,0:T(8,128)(2,1)}), bf16[64,8,512]{2,1,0:T(8,128)(2,1)S(1)}, u32[]{:S(2)}, u32[]{:S(2)}) %all-to-all-start.1) | async-done | bytes 524320 | tf_op jit(solution)/shard_map/all_to_all | solution.py:266
  144.0 1.0 shard_map.82
  145.1 7.9 %collective-permute-start.13 = (f32[2,256,128]{2,1,0:T(8,128)S(1)}, f32[2,256,128]{2,1,0:T(8,128)S(1)}, u32[]{:S(2)}, u32[]{:S(2)}) collective-permute-start(f32[2,256,128]{2,1,0:T(8,128)S(1)} %get-tuple-element.50), channel_id=1, source_target_pairs={{0,1},{1,0},{2,3},{3,2},{4,5},{5,4},{6,7},{7,6},{8,9},{9,8},{10,11... | collective-permute-start | bytes 786440 | tf_op jit(solution)/shard_map/ppermute | solution.py:205
  152.9 1.1 collective-permute-done.13.got
  154.1 4.3 %collective-permute-start.14 = (bf16[256,128]{1,0:T(8,128)(2,1)S(1)}, bf16[256,128]{1,0:T(8,128)(2,1)S(1)}, u32[]{:S(2)}, u32[]{:S(2)}) collective-permute-start(bf16[256,128]{1,0:T(8,128)(2,1)S(1)} %get-tuple-element.52), channel_id=1, source_target_pairs={{0,8},{1,9},{2,10},{3,11},{4,12},{5,13},{6,14},{7,15},{8,0},{9,1},... | collective-permute-start | bytes 196616 | tf_op jit(solution)/shard_map/ppermute | solution.py:205
  158.5 6.6 %collective-permute-done.14 = bf16[256,128]{1,0:T(8,128)(2,1)S(1)} collective-permute-done((bf16[256,128]{1,0:T(8,128)(2,1)S(1)}, bf16[256,128]{1,0:T(8,128)(2,1)S(1)}, u32[]{:S(2)}, u32[]{:S(2)}) %collective-permute-start.14) | collective-permute-done | bytes 65568 | tf_op jit(solution)/shard_map/ppermute | solution.py:205
  165.1 0.6 add_convert_fusion
  (6 shorter events, 0.1 us)
Async XLA Ops:
  0.0 44.6 %copy-start.1 = (bf16[1,2048,256]{2,1,0:T(8,128)(2,1)S(1)}, bf16[1,2048,256]{2,1,0:T(8,128)(2,1)}, u32[]{:S(2)}) copy-start(bf16[1,2048,256]{2,1,0:T(8,128)(2,1)} %param.12) | copy-start | bytes 3145732
  1.1 41.3 %copy-start = (bf16[1,2048,256]{2,1,0:T(8,128)(2,1)S(1)}, bf16[1,2048,256]{2,1,0:T(8,128)(2,1)}, u32[]{:S(2)}) copy-start(bf16[1,2048,256]{2,1,0:T(8,128)(2,1)} %param.11) | copy-start | bytes 3145732
  1.1 9.3 %collective-permute-start = (bf16[272,128]{1,0:T(8,128)(2,1)S(1)}, bf16[272,128]{1,0:T(8,128)(2,1)S(1)}, u32[]{:S(2)}, u32[]{:S(2)}) collective-permute-start(bf16[272,128]{1,0:T(8,128)(2,1)S(1)} %get-tuple-element.54), channel_id=1, source_target_pairs={{0,8},{1,9},{2,10},{3,11},{4,12},{5,13},{6,14},{7,15},{8,0},{9,1},... | collective-permute-start | bytes 208904 | tf_op jit(solution)/shard_map/ppermute | solution.py:205
  10.4 6.3 %collective-permute-start.1 = (bf16[2,272,128]{2,1,0:T(8,128)(2,1)S(1)}, bf16[2,272,128]{2,1,0:T(8,128)(2,1)S(1)}, u32[]{:S(2)}, u32[]{:S(2)}) collective-permute-start(bf16[2,272,128]{2,1,0:T(8,128)(2,1)S(1)} %pad_maximum_fusion.1.own), channel_id=1, source_target_pairs={{0,1},{1,0},{2,3},{3,2},{4,5},{5,4},{6,7},{7,6},{8,9},{9,8},{10,11... | collective-permute-start | bytes 417800 | tf_op jit(solution)/shard_map/ppermute | solution.py:205
  15.2 0.7 copy-start.4
  18.3 42.0 %all-to-all-start = ((bf16[64,8,512]{2,1,0:T(8,128)(2,1)}), bf16[64,8,512]{2,1,0:T(8,128)(2,1)S(1)}, u32[]{:S(2)}, u32[]{:S(2)}) async-start(bf16[64,8,512]{2,1,0:T(8,128)(2,1)} %bitcast.7), calls=%async_computation | async-start | bytes 1048576 | tf_op jit(solution)/shard_map/all_to_all | solution.py:233
  42.4 23.4 %collective-permute-start.6 = (bf16[2,4,256,256]{3,2,1,0:T(8,128)(2,1)S(1)}, bf16[2,4,256,256]{3,2,1,0:T(8,128)(2,1)}, u32[]{:S(2)}, u32[]{:S(2)}) collective-permute-start(bf16[2,4,256,256]{3,2,1,0:T(8,128)(2,1)S(1)} %bitcast.21), channel_id=1, source_target_pairs={{0,1},{1,0},{2,3},{3,2},{4,5},{5,4},{6,7},{7,6},{8,9},{9,8},{10,11... | collective-permute-start | bytes 3145736 | tf_op jit(solution)/shard_map/ppermute | solution.py:205
  44.6 24.3 %collective-permute-start.7 = (bf16[2,4,256,256]{3,2,1,0:T(8,128)(2,1)S(1)}, bf16[2,4,256,256]{3,2,1,0:T(8,128)(2,1)}, u32[]{:S(2)}, u32[]{:S(2)}) collective-permute-start(bf16[2,4,256,256]{3,2,1,0:T(8,128)(2,1)S(1)} %bitcast.25), channel_id=1, source_target_pairs={{0,1},{1,0},{2,3},{3,2},{4,5},{5,4},{6,7},{7,6},{8,9},{9,8},{10,11... | collective-permute-start | bytes 3145736 | tf_op jit(solution)/shard_map/ppermute | solution.py:205
  46.7 35.0 %collective-permute-start.8 = (bf16[256,2048]{1,0:T(8,128)(2,1)}, bf16[256,2048]{1,0:T(8,128)(2,1)}, u32[]{:S(2)}, u32[]{:S(2)}) collective-permute-start(bf16[256,2048]{1,0:T(8,128)(2,1)} %bitcast.29), channel_id=1, source_target_pairs={{0,1},{1,0},{2,3},{3,2},{4,5},{5,4},{6,7},{7,6},{8,9},{9,8},{10,11... | collective-permute-start | bytes 3145736 | tf_op jit(solution)/shard_map/ppermute | solution.py:205
  60.4 14.3 %collective-permute-start.4 = (bf16[528,512]{1,0:T(8,128)(2,1)S(1)}, bf16[528,512]{1,0:T(8,128)(2,1)S(1)}, u32[]{:S(2)}, u32[]{:S(2)}) collective-permute-start(bf16[528,512]{1,0:T(8,128)(2,1)S(1)} %pad_maximum_fusion), channel_id=1, source_target_pairs={{0,2},{2,4},{4,6},{6,8},{8,10},{10,12},{12,14},{14,0},{1,3},{3,5},... | collective-permute-start | bytes 1622024 | tf_op jit(solution)/shard_map/ppermute | solution.py:202
  62.3 16.2 %collective-permute-start.5 = (bf16[528,512]{1,0:T(8,128)(2,1)S(1)}, bf16[528,512]{1,0:T(8,128)(2,1)S(1)}, u32[]{:S(2)}, u32[]{:S(2)}) collective-permute-start(bf16[528,512]{1,0:T(8,128)(2,1)S(1)} %pad_maximum_fusion), channel_id=1, source_target_pairs={{0,14},{2,0},{4,2},{6,4},{8,6},{10,8},{12,10},{14,12},{1,15},{3,1}... | collective-permute-start | bytes 1622024 | tf_op jit(solution)/shard_map/ppermute | solution.py:202
  65.7 20.8 %collective-permute-start.3 = (bf16[272,512]{1,0:T(8,128)(2,1)S(1)}, bf16[272,512]{1,0:T(8,128)(2,1)S(1)}, u32[]{:S(2)}, u32[]{:S(2)}) collective-permute-start(bf16[272,512]{1,0:T(8,128)(2,1)S(1)} %fusion), channel_id=1, source_target_pairs={{0,12},{2,14},{4,0},{6,2},{8,4},{10,6},{12,8},{14,10},{1,13},{3,15... | collective-permute-start | bytes 835592 | tf_op jit(solution)/shard_map/ppermute | solution.py:202
  68.9 17.7 %collective-permute-start.2 = (bf16[256,512]{1,0:T(8,128)(2,1)S(1)}, bf16[256,512]{1,0:T(8,128)(2,1)S(1)}, u32[]{:S(2)}, u32[]{:S(2)}) collective-permute-start(bf16[256,512]{1,0:T(8,128)(2,1)S(1)} %slice_bitcast_fusion), channel_id=1, source_target_pairs={{0,4},{2,6},{4,8},{6,10},{8,12},{10,14},{12,0},{14,2},{1,5},{3,7},... | collective-permute-start | bytes 786440 | tf_op jit(solution)/shard_map/ppermute | solution.py:202
  78.6 8.0 %copy-start.2 = (bf16[1,256,2048]{2,1,0:T(8,128)(2,1)S(1)}, bf16[1,256,2048]{2,1,0:T(8,128)(2,1)}, u32[]{:S(2)}) copy-start(bf16[1,256,2048]{2,1,0:T(8,128)(2,1)} %param.13) | copy-start | bytes 3145732
  89.6 10.5 %collective-permute-start.10 = (bf16[256,512]{1,0:T(8,128)(2,1)S(1)}, bf16[256,512]{1,0:T(8,128)(2,1)S(1)}, u32[]{:S(2)}, u32[]{:S(2)}) collective-permute-start(bf16[256,512]{1,0:T(8,128)(2,1)S(1)} %get-tuple-element.46), channel_id=1, source_target_pairs={{0,14},{2,0},{4,2},{6,4},{8,6},{10,8},{12,10},{14,12},{1,15},{3,1}... | collective-permute-start | bytes 786440 | tf_op jit(solution)/shard_map/ppermute | solution.py:202
  95.9 7.1 %collective-permute-start.9 = (bf16[256,512]{1,0:T(8,128)(2,1)S(1)}, bf16[256,512]{1,0:T(8,128)(2,1)S(1)}, u32[]{:S(2)}, u32[]{:S(2)}) collective-permute-start(bf16[256,512]{1,0:T(8,128)(2,1)S(1)} %get-tuple-element.45), channel_id=1, source_target_pairs={{0,2},{2,4},{4,6},{6,8},{8,10},{10,12},{12,14},{14,0},{1,3},{3,5},... | collective-permute-start | bytes 786440 | tf_op jit(solution)/shard_map/ppermute | solution.py:202
  103.2 11.6 %collective-permute-start.11 = (bf16[512,512]{1,0:T(8,128)(2,1)S(1)}, bf16[512,512]{1,0:T(8,128)(2,1)S(1)}, u32[]{:S(2)}, u32[]{:S(2)}) collective-permute-start(bf16[512,512]{1,0:T(8,128)(2,1)S(1)} %get-tuple-element.47), channel_id=1, source_target_pairs={{0,2},{2,4},{4,6},{6,8},{8,10},{10,12},{12,14},{14,0},{1,3},{3,5},... | collective-permute-start | bytes 1572872 | tf_op jit(solution)/shard_map/ppermute | solution.py:202
  106.7 13.2 %collective-permute-start.12 = (bf16[512,512]{1,0:T(8,128)(2,1)S(1)}, bf16[512,512]{1,0:T(8,128)(2,1)S(1)}, u32[]{:S(2)}, u32[]{:S(2)}) collective-permute-start(bf16[512,512]{1,0:T(8,128)(2,1)S(1)} %get-tuple-element.48), channel_id=1, source_target_pairs={{0,14},{2,0},{4,2},{6,4},{8,6},{10,8},{12,10},{14,12},{1,15},{3,1}... | collective-permute-start | bytes 1572872 | tf_op jit(solution)/shard_map/ppermute | solution.py:202
  120.8 8.5 %copy-start.3 = (f32[256,2]{0,1:T(2,128)S(1)}, f32[256,2]{0,1:T(2,128)}, u32[]{:S(2)}) copy-start(f32[256,2]{0,1:T(2,128)} %param.10) | copy-start | bytes 6148
  120.8 23.2 %all-to-all-start.1 = ((bf16[64,8,512]{2,1,0:T(8,128)(2,1)}), bf16[64,8,512]{2,1,0:T(8,128)(2,1)S(1)}, u32[]{:S(2)}, u32[]{:S(2)}) async-start(bf16[64,8,512]{2,1,0:T(8,128)(2,1)} %bitcast.13), calls=%async_computation.1 | async-start | bytes 1048576 | tf_op jit(solution)/shard_map/all_to_all | solution.py:266
  145.1 9.0 %collective-permute-start.13 = (f32[2,256,128]{2,1,0:T(8,128)S(1)}, f32[2,256,128]{2,1,0:T(8,128)S(1)}, u32[]{:S(2)}, u32[]{:S(2)}) collective-permute-start(f32[2,256,128]{2,1,0:T(8,128)S(1)} %get-tuple-element.50), channel_id=1, source_target_pairs={{0,1},{1,0},{2,3},{3,2},{4,5},{5,4},{6,7},{7,6},{8,9},{9,8},{10,11... | collective-permute-start | bytes 786440 | tf_op jit(solution)/shard_map/ppermute | solution.py:205
  154.1 11.0 %collective-permute-start.14 = (bf16[256,128]{1,0:T(8,128)(2,1)S(1)}, bf16[256,128]{1,0:T(8,128)(2,1)S(1)}, u32[]{:S(2)}, u32[]{:S(2)}) collective-permute-start(bf16[256,128]{1,0:T(8,128)(2,1)S(1)} %get-tuple-element.52), channel_id=1, source_target_pairs={{0,8},{1,9},{2,10},{3,11},{4,12},{5,13},{6,14},{7,15},{8,0},{9,1},... | collective-permute-start | bytes 196616 | tf_op jit(solution)/shard_map/ppermute | solution.py:205

commit v7 on v6

--- a/solution.py
+++ b/solution.py
@@ -236,8 +236,6 @@
     sent = jnp.concatenate([here, gain], axis=0)
     left = step(sent, 1)
     right = step(sent, -1)
-    left2 = step(sent[:h], 2)
-    right2 = step(sent[h:], -2)
     wg2, wu2, wd2 = flip(wg, 1), flip(wu, 1), flip(wd, 1)
     wide = shape(n, 2 * hid, dtype=F32)
     slim = shape(n, hid, dtype=F32)
@@ -245,6 +243,9 @@
     gate, up, squares = call(near_body, (slim, slim, thin), 4, True, 300_000_000, 6)(
         pos, here, gain, wg, wu
     )
+    left, right, gate = lax.optimization_barrier((left, right, gate))
+    left2 = step(left[:h], 1)
+    right2 = step(right[h:], -1)
     gate, up, squares = call(
         middle_body, (wide, wide, thin), 11, True, 1_300_000_000, 10
     )(pos, here, gain, left, right, gate, up, squares, wg, wu, wg2, wu2)

time: 167 us -> 165 us (0.988)
  waiting for transfers between devices: 61.5 us -> 57.6 us
    ppermute x7, waiting for transfers between devices: 12.2 us -> 9.41 us  [flip(): return lax.ppermute(x, TP, [(i, i ^ bits) for i in range(16)])]
    ppermute x7, starting transfers between devices: 28.3 us -> 30.4 us  [flip(): return lax.ppermute(x, TP, [(i, i ^ bits) for i in range(16)])]
  transfers between devices with their start and end apart: 17 -> 17, of which waited for: 11 -> 11; matrix products, arithmetic and copies ran while one was open for 0% -> 0% of each run, Pallas kernels for 4% -> 5%
where the time goes in v7:
time: 165 us; the launch traced here: 163 us
  starting transfers between devices  88.4 us (54%)
  waiting for transfers between devices  57.6 us (35%)
  Pallas kernels  14.3 us (9%)
  other arithmetic  1.83 us (1%)
    ppermute x7, starting transfers between devices, flip(): return lax.ppermute(x, TP, [(i, i ^ bits) for i in range(16)])  30.4 us
    ppermute x8, starting transfers between devices, step(): return lax.ppermute(x, X, [(i, (i + s) % 8) for i in range(8)])  24.9 us
    all_to_all x1, starting transfers between devices, shards(): lax.all_to_all(buf.reshape(n_ep, half, feats), EP, split_axis=0, concat_a...  24 us
    ppermute x8, waiting for transfers between devices, step(): return lax.ppermute(x, X, [(i, (i + s) % 8) for i in range(8)])  22.2 us
    all_to_all x1, waiting for transfers between devices, shards(): lax.all_to_all(sums.reshape(n_ep, half, feats), EP, split_axis=0, concat_...  14.5 us
    all_to_all x1, waiting for transfers between devices, shards(): lax.all_to_all(buf.reshape(n_ep, half, feats), EP, split_axis=0, concat_a...  11.4 us
    ppermute x7, waiting for transfers between devices, flip(): return lax.ppermute(x, TP, [(i, i ^ bits) for i in range(16)])  9.41 us
    all_to_all x1, starting transfers between devices, shards(): lax.all_to_all(sums.reshape(n_ep, half, feats), EP, split_axis=0, concat_...  9.1 us
  transfers between devices with their start and end apart: 17, of which 11 were waited for; matrix products, arithmetic and copies ran while one was open for 0% of the time, Pallas kernels for 5%

profile of v7, /device:TPU:15, one launch (start us, length us, event | category | flops | bytes accessed | tf_op | source)
XLA Modules:
  0.0 163.2 jit_solution(257645802028605370)
XLA Ops:
  0.0 0.0 copy-start.1
  0.0 1.0 fusion
  1.1 0.0 copy-start
  1.1 4.9 %collective-permute-start = (bf16[272,128]{1,0:T(8,128)(2,1)S(1)}, bf16[272,128]{1,0:T(8,128)(2,1)S(1)}, u32[]{:S(2)}, u32[]{:S(2)}) collective-permute-start(bf16[272,128]{1,0:T(8,128)(2,1)S(1)} %get-tuple-element.60), channel_id=1, source_target_pairs={{0,8},{1,9},{2,10},{3,11},{4,12},{5,13},{6,14},{7,15},{8,0},{9,1},... | collective-permute-start | bytes 208904 | tf_op jit(solution)/shard_map/ppermute | solution.py:205
  6.0 4.4 %collective-permute-done = bf16[272,128]{1,0:T(8,128)(2,1)S(1)} collective-permute-done((bf16[272,128]{1,0:T(8,128)(2,1)S(1)}, bf16[272,128]{1,0:T(8,128)(2,1)S(1)}, u32[]{:S(2)}, u32[]{:S(2)}) %collective-permute-start) | collective-permute-done | bytes 69664 | tf_op jit(solution)/shard_map/ppermute | solution.py:205
  10.4 4.7 %collective-permute-start.1 = (bf16[2,272,128]{2,1,0:T(8,128)(2,1)S(1)}, bf16[2,272,128]{2,1,0:T(8,128)(2,1)S(1)}, u32[]{:S(2)}, u32[]{:S(2)}) collective-permute-start(bf16[2,272,128]{2,1,0:T(8,128)(2,1)S(1)} %pad_maximum_fusion.1.own), channel_id=1, source_target_pairs={{0,1},{1,0},{2,3},{3,2},{4,5},{5,4},{6,7},{7,6},{8,9},{9,8},{10,11... | collective-permute-start | bytes 417800 | tf_op jit(solution)/shard_map/ppermute | solution.py:205
  15.1 0.1 pad_add_fusion.pos
  15.2 0.0 copy-start.4
  15.2 0.7 copy-done.4
  15.8 0.8 shard_map.73
  16.7 0.0 collective-permute-done.1.other
  16.7 1.7 %shard_map.75 = (bf16[512,512]{1,0:T(8,128)(2,1)}, bf16[16,512]{1,0:T(8,128)(2,1)S(1)}) custom-call(s32[3]{0:T(128)S(1)} %pad_add_fusion.pos, bf16[512,256]{1,0:T(8,128)(2,1)S(1)} %get-tuple-element.35.place, bf16[2,272,128]{2,1,0:T(8,128)(2,1)S(1)} %pad_maximum_fusion.1.own, bf16[2,272,128]{2,1,0:T(8,128)(2,1)S(1)} %collective-permute-done.1.other), custom_call_target="tpu_custom_call" | custom-call | flops 150000000 | bytes 4194304 | tf_op jit(solution)/shard_map/pallas_call | solution.py:230
  18.3 24.0 %all-to-all-start = ((bf16[64,8,512]{2,1,0:T(8,128)(2,1)}), bf16[64,8,512]{2,1,0:T(8,128)(2,1)S(1)}, u32[]{:S(2)}, u32[]{:S(2)}) async-start(bf16[64,8,512]{2,1,0:T(8,128)(2,1)} %bitcast.7), calls=%async_computation | async-start | bytes 1048576 | tf_op jit(solution)/shard_map/all_to_all | solution.py:233
  42.4 0.0 copy-done
  42.4 2.2 %collective-permute-start.6 = (bf16[2,4,256,256]{3,2,1,0:T(8,128)(2,1)S(1)}, bf16[2,4,256,256]{3,2,1,0:T(8,128)(2,1)}, u32[]{:S(2)}, u32[]{:S(2)}) collective-permute-start(bf16[2,4,256,256]{3,2,1,0:T(8,128)(2,1)S(1)} %bitcast.15), channel_id=1, source_target_pairs={{0,1},{1,0},{2,3},{3,2},{4,5},{5,4},{6,7},{7,6},{8,9},{9,8},{10,11... | collective-permute-start | bytes 3145736 | tf_op jit(solution)/shard_map/ppermute | solution.py:205
  44.6 0.0 copy-done.1
  44.6 2.1 %collective-permute-start.7 = (bf16[2,4,256,256]{3,2,1,0:T(8,128)(2,1)S(1)}, bf16[2,4,256,256]{3,2,1,0:T(8,128)(2,1)}, u32[]{:S(2)}, u32[]{:S(2)}) collective-permute-start(bf16[2,4,256,256]{3,2,1,0:T(8,128)(2,1)S(1)} %bitcast.19), channel_id=1, source_target_pairs={{0,1},{1,0},{2,3},{3,2},{4,5},{5,4},{6,7},{7,6},{8,9},{9,8},{10,11... | collective-permute-start | bytes 3145736 | tf_op jit(solution)/shard_map/ppermute | solution.py:205
  46.7 2.2 %collective-permute-start.8 = (bf16[256,2048]{1,0:T(8,128)(2,1)}, bf16[256,2048]{1,0:T(8,128)(2,1)}, u32[]{:S(2)}, u32[]{:S(2)}) collective-permute-start(bf16[256,2048]{1,0:T(8,128)(2,1)} %bitcast.26), channel_id=1, source_target_pairs={{0,1},{1,0},{2,3},{3,2},{4,5},{5,4},{6,7},{7,6},{8,9},{9,8},{10,11... | collective-permute-start | bytes 3145736 | tf_op jit(solution)/shard_map/ppermute | solution.py:205
  48.9 11.4 %all-to-all-done = bf16[64,8,512]{2,1,0:T(8,128)(2,1)S(1)} async-done(((bf16[64,8,512]{2,1,0:T(8,128)(2,1)}), bf16[64,8,512]{2,1,0:T(8,128)(2,1)S(1)}, u32[]{:S(2)}, u32[]{:S(2)}) %all-to-all-start) | async-done | bytes 524320 | tf_op jit(solution)/shard_map/all_to_all | solution.py:233
  60.4 1.9 %collective-permute-start.2 = (bf16[528,512]{1,0:T(8,128)(2,1)S(1)}, bf16[528,512]{1,0:T(8,128)(2,1)S(1)}, u32[]{:S(2)}, u32[]{:S(2)}) collective-permute-start(bf16[528,512]{1,0:T(8,128)(2,1)S(1)} %pad_maximum_fusion), channel_id=1, source_target_pairs={{0,2},{2,4},{4,6},{6,8},{8,10},{10,12},{12,14},{14,0},{1,3},{3,5},... | collective-permute-start | bytes 1622024 | tf_op jit(solution)/shard_map/ppermute | solution.py:202
  62.3 3.4 %collective-permute-start.3 = (bf16[528,512]{1,0:T(8,128)(2,1)S(1)}, bf16[528,512]{1,0:T(8,128)(2,1)S(1)}, u32[]{:S(2)}, u32[]{:S(2)}) collective-permute-start(bf16[528,512]{1,0:T(8,128)(2,1)S(1)} %pad_maximum_fusion), channel_id=1, source_target_pairs={{0,14},{2,0},{4,2},{6,4},{8,6},{10,8},{12,10},{14,12},{1,15},{3,1}... | collective-permute-start | bytes 1622024 | tf_op jit(solution)/shard_map/ppermute | solution.py:202
  65.7 1.0 shard_map.76
  66.7 8.0 %collective-permute-done.2.left = bf16[528,512]{1,0:T(8,128)(2,1)S(1)} collective-permute-done((bf16[528,512]{1,0:T(8,128)(2,1)S(1)}, bf16[528,512]{1,0:T(8,128)(2,1)S(1)}, u32[]{:S(2)}, u32[]{:S(2)}) %collective-permute-start.2) | collective-permute-done | bytes 540704 | tf_op jit(solution)/shard_map/ppermute | solution.py:202
  74.7 3.1 %collective-permute-done.3.right = bf16[528,512]{1,0:T(8,128)(2,1)S(1)} collective-permute-done((bf16[528,512]{1,0:T(8,128)(2,1)S(1)}, bf16[528,512]{1,0:T(8,128)(2,1)S(1)}, u32[]{:S(2)}, u32[]{:S(2)}) %collective-permute-start.3) | collective-permute-done | bytes 540704 | tf_op jit(solution)/shard_map/ppermute | solution.py:202
  77.9 1.9 %collective-permute-start.5 = (bf16[272,512]{1,0:T(8,128)(2,1)S(1)}, bf16[272,512]{1,0:T(8,128)(2,1)S(1)}, u32[]{:S(2)}, u32[]{:S(2)}) collective-permute-start(bf16[272,512]{1,0:T(8,128)(2,1)S(1)} %slice.7), channel_id=1, source_target_pairs={{0,14},{2,0},{4,2},{6,4},{8,6},{10,8},{12,10},{14,12},{1,15},{3,1}... | collective-permute-start | bytes 835592 | tf_op jit(solution)/shard_map/ppermute | solution.py:202
  79.8 4.6 %collective-permute-start.4 = (bf16[256,512]{1,0:T(8,128)(2,1)S(1)}, bf16[256,512]{1,0:T(8,128)(2,1)S(1)}, u32[]{:S(2)}, u32[]{:S(2)}) collective-permute-start(bf16[256,512]{1,0:T(8,128)(2,1)S(1)} %slice.6), channel_id=1, source_target_pairs={{0,2},{2,4},{4,6},{6,8},{8,10},{10,12},{12,14},{14,0},{1,3},{3,5},... | collective-permute-start | bytes 786440 | tf_op jit(solution)/shard_map/ppermute | solution.py:202
  84.4 0.0 collective-permute-done.6.wg2
  84.4 0.0 collective-permute-done.7.wu2
  84.4 0.0 copy-start.2
  84.4 3.2 %shard_map.77 = (f32[512,512]{1,0:T(8,128)S(1)}, f32[512,512]{1,0:T(8,128)S(1)}, f32[512,128]{1,0:T(8,128)S(1)}) custom-call(s32[3]{0:T(128)S(1)} %pad_add_fusion.pos, bf16[512,512]{1,0:T(8,128)(2,1)S(1)} %bitcast.25, bf16[16,512]{1,0:T(8,128)(2,1)S(1)} %get-tuple-element.37.gain.gain_m, bf16[528,512]{1,0:T(8,128)(2,1)S(1)} %collective-permute-done.2.left, ...), custom_call_target="tpu_custom_call" | custom-call | flops 1300000000 | bytes 4194304 | tf_op jit(solution)/shard_map/pallas_call | solution.py:249
  87.6 0.0 collective-permute-done.8.wd2
  87.6 0.1 collective-permute-done.4.left2
  87.7 0.0 collective-permute-done.5.right2
  87.7 0.0 copy-done.2
  87.7 3.1 %shard_map.78 = (bf16[256,512]{1,0:T(8,128)(2,1)S(1)}, bf16[256,512]{1,0:T(8,128)(2,1)S(1)}, bf16[512,512]{1,0:T(8,128)(2,1)S(1)}) custom-call(s32[3]{0:T(128)S(1)} %pad_add_fusion.pos, bf16[256,512]{1,0:T(8,128)(2,1)S(1)} %collective-permute-done.4.left2, bf16[272,512]{1,0:T(8,128)(2,1)S(1)} %collective-permute-done.5.right2, ...), custom_call_target="tpu_custom_call" | custom-call | flops 800000000 | bytes 4194304 | tf_op jit(solution)/shard_map/pallas_call | solution.py:252
  90.8 2.3 %collective-permute-start.10 = (bf16[256,512]{1,0:T(8,128)(2,1)S(1)}, bf16[256,512]{1,0:T(8,128)(2,1)S(1)}, u32[]{:S(2)}, u32[]{:S(2)}) collective-permute-start(bf16[256,512]{1,0:T(8,128)(2,1)S(1)} %get-tuple-element.52), channel_id=1, source_target_pairs={{0,14},{2,0},{4,2},{6,4},{8,6},{10,8},{12,10},{14,12},{1,15},{3,1}... | collective-permute-start | bytes 786440 | tf_op jit(solution)/shard_map/ppermute | solution.py:202
  93.1 4.6 %collective-permute-start.9 = (bf16[256,512]{1,0:T(8,128)(2,1)S(1)}, bf16[256,512]{1,0:T(8,128)(2,1)S(1)}, u32[]{:S(2)}, u32[]{:S(2)}) collective-permute-start(bf16[256,512]{1,0:T(8,128)(2,1)S(1)} %get-tuple-element.51), channel_id=1, source_target_pairs={{0,2},{2,4},{4,6},{6,8},{8,10},{10,12},{12,14},{14,0},{1,3},{3,5},... | collective-permute-start | bytes 786440 | tf_op jit(solution)/shard_map/ppermute | solution.py:202
  97.7 2.2 %shard_map.79 = (bf16[512,512]{1,0:T(8,128)(2,1)S(1)}, bf16[512,512]{1,0:T(8,128)(2,1)S(1)}, bf16[512,512]{1,0:T(8,128)(2,1)S(1)}) custom-call(s32[3]{0:T(128)S(1)} %pad_add_fusion.pos, bf16[512,512]{1,0:T(8,128)(2,1)S(1)} %get-tuple-element.47.hidden, bf16[256,2048]{1,0:T(8,128)(2,1)S(1)} %bitcast.28, bf16[256,2048]{1,0:T(8,128)(2,1)} %collective-permute-done.8.wd2), custom_call_target="tpu_custom_call" | custom-call | flops 800000000 | bytes 4194304 | tf_op jit(solution)/shard_map/pallas_call | solution.py:258
  100.0 0.0 collective-permute-done.10.got_b
  100.0 1.8 %collective-permute-done.9.got_a = bf16[256,512]{1,0:T(8,128)(2,1)S(1)} collective-permute-done((bf16[256,512]{1,0:T(8,128)(2,1)S(1)}, bf16[256,512]{1,0:T(8,128)(2,1)S(1)}, u32[]{:S(2)}, u32[]{:S(2)}) %collective-permute-start.9) | collective-permute-done | bytes 262176 | tf_op jit(solution)/shard_map/ppermute | solution.py:202
  101.8 0.2 shard_map.80
  101.9 4.3 %collective-permute-start.11 = (bf16[512,512]{1,0:T(8,128)(2,1)S(1)}, bf16[512,512]{1,0:T(8,128)(2,1)S(1)}, u32[]{:S(2)}, u32[]{:S(2)}) collective-permute-start(bf16[512,512]{1,0:T(8,128)(2,1)S(1)} %get-tuple-element.53), channel_id=1, source_target_pairs={{0,2},{2,4},{4,6},{6,8},{8,10},{10,12},{12,14},{14,0},{1,3},{3,5},... | collective-permute-start | bytes 1572872 | tf_op jit(solution)/shard_map/ppermute | solution.py:202
  106.2 1.9 %collective-permute-start.12 = (bf16[512,512]{1,0:T(8,128)(2,1)S(1)}, bf16[512,512]{1,0:T(8,128)(2,1)S(1)}, u32[]{:S(2)}, u32[]{:S(2)}) collective-permute-start(bf16[512,512]{1,0:T(8,128)(2,1)S(1)} %get-tuple-element.54), channel_id=1, source_target_pairs={{0,14},{2,0},{4,2},{6,4},{8,6},{10,8},{12,10},{14,12},{1,15},{3,1}... | collective-permute-start | bytes 1572872 | tf_op jit(solution)/shard_map/ppermute | solution.py:202
  108.2 5.2 %collective-permute-done.11.got_a = bf16[512,512]{1,0:T(8,128)(2,1)S(1)} collective-permute-done((bf16[512,512]{1,0:T(8,128)(2,1)S(1)}, bf16[512,512]{1,0:T(8,128)(2,1)S(1)}, u32[]{:S(2)}, u32[]{:S(2)}) %collective-permute-start.11) | collective-permute-done | bytes 524320 | tf_op jit(solution)/shard_map/ppermute | solution.py:202
  113.4 4.0 %collective-permute-done.12.got_b = bf16[512,512]{1,0:T(8,128)(2,1)S(1)} collective-permute-done((bf16[512,512]{1,0:T(8,128)(2,1)S(1)}, bf16[512,512]{1,0:T(8,128)(2,1)S(1)}, u32[]{:S(2)}, u32[]{:S(2)}) %collective-permute-start.12) | collective-permute-done | bytes 524320 | tf_op jit(solution)/shard_map/ppermute | solution.py:202
  117.4 1.0 shard_map.81
  118.3 0.0 copy-start.3
  118.3 9.1 %all-to-all-start.1 = ((bf16[64,8,512]{2,1,0:T(8,128)(2,1)}), bf16[64,8,512]{2,1,0:T(8,128)(2,1)S(1)}, u32[]{:S(2)}, u32[]{:S(2)}) async-start(bf16[64,8,512]{2,1,0:T(8,128)(2,1)} %bitcast.12), calls=%async_computation.1 | async-start | bytes 1048576 | tf_op jit(solution)/shard_map/all_to_all | solution.py:267
  127.4 0.0 copy-done.3
  127.5 0.1 shard_map.74
  127.6 14.5 %all-to-all-done.1 = bf16[64,8,512]{2,1,0:T(8,128)(2,1)S(1)} async-done(((bf16[64,8,512]{2,1,0:T(8,128)(2,1)}), bf16[64,8,512]{2,1,0:T(8,128)(2,1)S(1)}, u32[]{:S(2)}, u32[]{:S(2)}) %all-to-all-start.1) | async-done | bytes 524320 | tf_op jit(solution)/shard_map/all_to_all | solution.py:267
  142.1 1.0 shard_map.82
  143.2 8.2 %collective-permute-start.13 = (f32[2,256,128]{2,1,0:T(8,128)S(1)}, f32[2,256,128]{2,1,0:T(8,128)S(1)}, u32[]{:S(2)}, u32[]{:S(2)}) collective-permute-start(f32[2,256,128]{2,1,0:T(8,128)S(1)} %get-tuple-element.56), channel_id=1, source_target_pairs={{0,1},{1,0},{2,3},{3,2},{4,5},{5,4},{6,7},{7,6},{8,9},{9,8},{10,11... | collective-permute-start | bytes 786440 | tf_op jit(solution)/shard_map/ppermute | solution.py:205
  151.4 1.1 collective-permute-done.13.got
  152.5 6.1 %collective-permute-start.14 = (bf16[256,128]{1,0:T(8,128)(2,1)S(1)}, bf16[256,128]{1,0:T(8,128)(2,1)S(1)}, u32[]{:S(2)}, u32[]{:S(2)}) collective-permute-start(bf16[256,128]{1,0:T(8,128)(2,1)S(1)} %get-tuple-element.58), channel_id=1, source_target_pairs={{0,8},{1,9},{2,10},{3,11},{4,12},{5,13},{6,14},{7,15},{8,0},{9,1},... | collective-permute-start | bytes 196616 | tf_op jit(solution)/shard_map/ppermute | solution.py:205
  158.6 3.9 %collective-permute-done.14 = bf16[256,128]{1,0:T(8,128)(2,1)S(1)} collective-permute-done((bf16[256,128]{1,0:T(8,128)(2,1)S(1)}, bf16[256,128]{1,0:T(8,128)(2,1)S(1)}, u32[]{:S(2)}, u32[]{:S(2)}) %collective-permute-start.14) | collective-permute-done | bytes 65568 | tf_op jit(solution)/shard_map/ppermute | solution.py:205
  162.5 0.6 add_convert_fusion
  (6 shorter events, 0.1 us)
Async XLA Ops:
  0.0 44.6 %copy-start.1 = (bf16[1,2048,256]{2,1,0:T(8,128)(2,1)S(1)}, bf16[1,2048,256]{2,1,0:T(8,128)(2,1)}, u32[]{:S(2)}) copy-start(bf16[1,2048,256]{2,1,0:T(8,128)(2,1)} %param.12) | copy-start | bytes 3145732
  1.1 41.3 %copy-start = (bf16[1,2048,256]{2,1,0:T(8,128)(2,1)S(1)}, bf16[1,2048,256]{2,1,0:T(8,128)(2,1)}, u32[]{:S(2)}) copy-start(bf16[1,2048,256]{2,1,0:T(8,128)(2,1)} %param.11) | copy-start | bytes 3145732
  1.1 9.3 %collective-permute-start = (bf16[272,128]{1,0:T(8,128)(2,1)S(1)}, bf16[272,128]{1,0:T(8,128)(2,1)S(1)}, u32[]{:S(2)}, u32[]{:S(2)}) collective-permute-start(bf16[272,128]{1,0:T(8,128)(2,1)S(1)} %get-tuple-element.60), channel_id=1, source_target_pairs={{0,8},{1,9},{2,10},{3,11},{4,12},{5,13},{6,14},{7,15},{8,0},{9,1},... | collective-permute-start | bytes 208904 | tf_op jit(solution)/shard_map/ppermute | solution.py:205
  10.4 6.3 %collective-permute-start.1 = (bf16[2,272,128]{2,1,0:T(8,128)(2,1)S(1)}, bf16[2,272,128]{2,1,0:T(8,128)(2,1)S(1)}, u32[]{:S(2)}, u32[]{:S(2)}) collective-permute-start(bf16[2,272,128]{2,1,0:T(8,128)(2,1)S(1)} %pad_maximum_fusion.1.own), channel_id=1, source_target_pairs={{0,1},{1,0},{2,3},{3,2},{4,5},{5,4},{6,7},{7,6},{8,9},{9,8},{10,11... | collective-permute-start | bytes 417800 | tf_op jit(solution)/shard_map/ppermute | solution.py:205
  15.2 0.7 copy-start.4
  18.3 42.0 %all-to-all-start = ((bf16[64,8,512]{2,1,0:T(8,128)(2,1)}), bf16[64,8,512]{2,1,0:T(8,128)(2,1)S(1)}, u32[]{:S(2)}, u32[]{:S(2)}) async-start(bf16[64,8,512]{2,1,0:T(8,128)(2,1)} %bitcast.7), calls=%async_computation | async-start | bytes 1048576 | tf_op jit(solution)/shard_map/all_to_all | solution.py:233
  42.4 42.0 %collective-permute-start.6 = (bf16[2,4,256,256]{3,2,1,0:T(8,128)(2,1)S(1)}, bf16[2,4,256,256]{3,2,1,0:T(8,128)(2,1)}, u32[]{:S(2)}, u32[]{:S(2)}) collective-permute-start(bf16[2,4,256,256]{3,2,1,0:T(8,128)(2,1)S(1)} %bitcast.15), channel_id=1, source_target_pairs={{0,1},{1,0},{2,3},{3,2},{4,5},{5,4},{6,7},{7,6},{8,9},{9,8},{10,11... | collective-permute-start | bytes 3145736 | tf_op jit(solution)/shard_map/ppermute | solution.py:205
  44.6 39.8 %collective-permute-start.7 = (bf16[2,4,256,256]{3,2,1,0:T(8,128)(2,1)S(1)}, bf16[2,4,256,256]{3,2,1,0:T(8,128)(2,1)}, u32[]{:S(2)}, u32[]{:S(2)}) collective-permute-start(bf16[2,4,256,256]{3,2,1,0:T(8,128)(2,1)S(1)} %bitcast.19), channel_id=1, source_target_pairs={{0,1},{1,0},{2,3},{3,2},{4,5},{5,4},{6,7},{7,6},{8,9},{9,8},{10,11... | collective-permute-start | bytes 3145736 | tf_op jit(solution)/shard_map/ppermute | solution.py:205
  46.7 40.9 %collective-permute-start.8 = (bf16[256,2048]{1,0:T(8,128)(2,1)}, bf16[256,2048]{1,0:T(8,128)(2,1)}, u32[]{:S(2)}, u32[]{:S(2)}) collective-permute-start(bf16[256,2048]{1,0:T(8,128)(2,1)} %bitcast.26), channel_id=1, source_target_pairs={{0,1},{1,0},{2,3},{3,2},{4,5},{5,4},{6,7},{7,6},{8,9},{9,8},{10,11... | collective-permute-start | bytes 3145736 | tf_op jit(solution)/shard_map/ppermute | solution.py:205
  60.4 14.3 %collective-permute-start.2 = (bf16[528,512]{1,0:T(8,128)(2,1)S(1)}, bf16[528,512]{1,0:T(8,128)(2,1)S(1)}, u32[]{:S(2)}, u32[]{:S(2)}) collective-permute-start(bf16[528,512]{1,0:T(8,128)(2,1)S(1)} %pad_maximum_fusion), channel_id=1, source_target_pairs={{0,2},{2,4},{4,6},{6,8},{8,10},{10,12},{12,14},{14,0},{1,3},{3,5},... | collective-permute-start | bytes 1622024 | tf_op jit(solution)/shard_map/ppermute | solution.py:202
  62.3 15.5 %collective-permute-start.3 = (bf16[528,512]{1,0:T(8,128)(2,1)S(1)}, bf16[528,512]{1,0:T(8,128)(2,1)S(1)}, u32[]{:S(2)}, u32[]{:S(2)}) collective-permute-start(bf16[528,512]{1,0:T(8,128)(2,1)S(1)} %pad_maximum_fusion), channel_id=1, source_target_pairs={{0,14},{2,0},{4,2},{6,4},{8,6},{10,8},{12,10},{14,12},{1,15},{3,1}... | collective-permute-start | bytes 1622024 | tf_op jit(solution)/shard_map/ppermute | solution.py:202
  77.9 9.8 %collective-permute-start.5 = (bf16[272,512]{1,0:T(8,128)(2,1)S(1)}, bf16[272,512]{1,0:T(8,128)(2,1)S(1)}, u32[]{:S(2)}, u32[]{:S(2)}) collective-permute-start(bf16[272,512]{1,0:T(8,128)(2,1)S(1)} %slice.7), channel_id=1, source_target_pairs={{0,14},{2,0},{4,2},{6,4},{8,6},{10,8},{12,10},{14,12},{1,15},{3,1}... | collective-permute-start | bytes 835592 | tf_op jit(solution)/shard_map/ppermute | solution.py:202
  79.8 7.9 %collective-permute-start.4 = (bf16[256,512]{1,0:T(8,128)(2,1)S(1)}, bf16[256,512]{1,0:T(8,128)(2,1)S(1)}, u32[]{:S(2)}, u32[]{:S(2)}) collective-permute-start(bf16[256,512]{1,0:T(8,128)(2,1)S(1)} %slice.6), channel_id=1, source_target_pairs={{0,2},{2,4},{4,6},{6,8},{8,10},{10,12},{12,14},{14,0},{1,3},{3,5},... | collective-permute-start | bytes 786440 | tf_op jit(solution)/shard_map/ppermute | solution.py:202
  84.4 3.3 %copy-start.2 = (bf16[1,256,2048]{2,1,0:T(8,128)(2,1)S(1)}, bf16[1,256,2048]{2,1,0:T(8,128)(2,1)}, u32[]{:S(2)}) copy-start(bf16[1,256,2048]{2,1,0:T(8,128)(2,1)} %param.13) | copy-start | bytes 3145732
  90.8 9.2 %collective-permute-start.10 = (bf16[256,512]{1,0:T(8,128)(2,1)S(1)}, bf16[256,512]{1,0:T(8,128)(2,1)S(1)}, u32[]{:S(2)}, u32[]{:S(2)}) collective-permute-start(bf16[256,512]{1,0:T(8,128)(2,1)S(1)} %get-tuple-element.52), channel_id=1, source_target_pairs={{0,14},{2,0},{4,2},{6,4},{8,6},{10,8},{12,10},{14,12},{1,15},{3,1}... | collective-permute-start | bytes 786440 | tf_op jit(solution)/shard_map/ppermute | solution.py:202
  93.1 8.7 %collective-permute-start.9 = (bf16[256,512]{1,0:T(8,128)(2,1)S(1)}, bf16[256,512]{1,0:T(8,128)(2,1)S(1)}, u32[]{:S(2)}, u32[]{:S(2)}) collective-permute-start(bf16[256,512]{1,0:T(8,128)(2,1)S(1)} %get-tuple-element.51), channel_id=1, source_target_pairs={{0,2},{2,4},{4,6},{6,8},{8,10},{10,12},{12,14},{14,0},{1,3},{3,5},... | collective-permute-start | bytes 786440 | tf_op jit(solution)/shard_map/ppermute | solution.py:202
  101.9 11.4 %collective-permute-start.11 = (bf16[512,512]{1,0:T(8,128)(2,1)S(1)}, bf16[512,512]{1,0:T(8,128)(2,1)S(1)}, u32[]{:S(2)}, u32[]{:S(2)}) collective-permute-start(bf16[512,512]{1,0:T(8,128)(2,1)S(1)} %get-tuple-element.53), channel_id=1, source_target_pairs={{0,2},{2,4},{4,6},{6,8},{8,10},{10,12},{12,14},{14,0},{1,3},{3,5},... | collective-permute-start | bytes 1572872 | tf_op jit(solution)/shard_map/ppermute | solution.py:202
  106.2 11.1 %collective-permute-start.12 = (bf16[512,512]{1,0:T(8,128)(2,1)S(1)}, bf16[512,512]{1,0:T(8,128)(2,1)S(1)}, u32[]{:S(2)}, u32[]{:S(2)}) collective-permute-start(bf16[512,512]{1,0:T(8,128)(2,1)S(1)} %get-tuple-element.54), channel_id=1, source_target_pairs={{0,14},{2,0},{4,2},{6,4},{8,6},{10,8},{12,10},{14,12},{1,15},{3,1}... | collective-permute-start | bytes 1572872 | tf_op jit(solution)/shard_map/ppermute | solution.py:202
  118.3 9.1 %copy-start.3 = (f32[256,2]{0,1:T(2,128)S(1)}, f32[256,2]{0,1:T(2,128)}, u32[]{:S(2)}) copy-start(f32[256,2]{0,1:T(2,128)} %param.10) | copy-start | bytes 6148
  118.3 23.8 %all-to-all-start.1 = ((bf16[64,8,512]{2,1,0:T(8,128)(2,1)}), bf16[64,8,512]{2,1,0:T(8,128)(2,1)S(1)}, u32[]{:S(2)}, u32[]{:S(2)}) async-start(bf16[64,8,512]{2,1,0:T(8,128)(2,1)} %bitcast.12), calls=%async_computation.1 | async-start | bytes 1048576 | tf_op jit(solution)/shard_map/all_to_all | solution.py:267
  143.2 9.3 %collective-permute-start.13 = (f32[2,256,128]{2,1,0:T(8,128)S(1)}, f32[2,256,128]{2,1,0:T(8,128)S(1)}, u32[]{:S(2)}, u32[]{:S(2)}) collective-permute-start(f32[2,256,128]{2,1,0:T(8,128)S(1)} %get-tuple-element.56), channel_id=1, source_target_pairs={{0,1},{1,0},{2,3},{3,2},{4,5},{5,4},{6,7},{7,6},{8,9},{9,8},{10,11... | collective-permute-start | bytes 786440 | tf_op jit(solution)/shard_map/ppermute | solution.py:205
  152.5 10.0 %collective-permute-start.14 = (bf16[256,128]{1,0:T(8,128)(2,1)S(1)}, bf16[256,128]{1,0:T(8,128)(2,1)S(1)}, u32[]{:S(2)}, u32[]{:S(2)}) collective-permute-start(bf16[256,128]{1,0:T(8,128)(2,1)S(1)} %get-tuple-element.58), channel_id=1, source_target_pairs={{0,8},{1,9},{2,10},{3,11},{4,12},{5,13},{6,14},{7,15},{8,0},{9,1},... | collective-permute-start | bytes 196616 | tf_op jit(solution)/shard_map/ppermute | solution.py:205
